TPU v7x, 768 devices: a whole 4x8x12 slice. The times are simulated.
768 devices in a mesh: gr: 3 (over z_hi), sp: 32 (over z_lo, y), tp: 8 (over x, core).
Axes of the slice: x: 4, y: 8, z: 12 (z_hi: 3, z_lo: 4; z = z_hi * 4 + z_lo), core: 2. Of those that a mesh axis runs over, the one named last changes fastest.
Arguments:
- tokens: bfloat16 [6, 16384, 4096], P('gr', ('sp', 'tp')), parts along dimension 0, may hold values from -6 to 6
- norm_gain: bfloat16 [4096], replicated, may hold values from 0.099609375 to 1.8984375
- key_weight: bfloat16 [4096, 1024], P(None, 'tp'), may hold values from -0.09375 to 0.09375
- value_weight: bfloat16 [4096, 1024], P(None, 'tp'), may hold values from -0.09375 to 0.09375
- cum_gates: float32 [6, 16384, 16], P('gr', 'sp', 'tp'), parts along dimension 0, may hold values from -2733 to 0, as said below
- new_query: bfloat16 [6, 1024], P('gr', 'tp'), parts along dimension 0, may hold values from -240 to 240
- new_key: bfloat16 [6, 1024], P('gr', 'tp'), parts along dimension 0, may hold values from -6 to 6
- new_value: bfloat16 [6, 1024], P('gr', 'tp'), parts along dimension 0, may hold values from -6 to 6
- new_gate: float32 [6, 16], P('gr', 'tp'), parts along dimension 0, may hold values from -5 to -1.5
Outputs:
- key_cache: bfloat16 [6, 16384, 1024], P('gr', 'sp', 'tp'), parts along dimension 0
- value_cache: bfloat16 [6, 16384, 1024], P('gr', 'sp', 'tp'), parts along dimension 0
- readout: bfloat16 [6, 1024], P('gr', 'tp'), parts along dimension 0
There are 3 independent parts, one for each index of `gr`. A program takes and returns all parts, laid end to end along the dimension named above; an argument that names none is the same for every part. Nothing has to cross between parts.
Inputs may be any that keep to these rules, and one draw needn't show every extreme that they name: `cum_gates`: along positions, for each prompt and head, the values never rise.
All inputs are finite; a program needn't handle non-finite values.
Results may differ from a plain program's by a relative error of at most 0.005.
The roundings to bfloat16 on the way count: a program that leaves them out, or rounds other values in their place, can miss the bound.
Values may be sent and summed in bfloat16 or wider, within the bound.
No kernel may reach another device: no remote copies, remote signals or barrier semaphores. Data moves between devices by JAX's collectives and lax.ppermute only.
A program may use at most 64 MiB of HBM per device.

v0:
```python
import functools

import jax
import jax.numpy as jnp
from jax import lax
from jax.experimental import pallas as pl
from jax.experimental.pallas import tpu as pltpu
from jax.sharding import PartitionSpec as P


HD = 64
EPS = 1e-06
MASKED = -1e30


VMEM = pl.BlockSpec(memory_space=pltpu.VMEM)
ANY = pl.BlockSpec(memory_space=pl.ANY)

EARLY = ((0, 0), (0, 1), (3, 0), (3, 1), (1, 1), (1, 0))
LATE = ((2, 0), (2, 1))


def project_kernel(count, prior, *refs):
    xs, refs = refs[:count], refs[count:]
    before, (gain, wo, wp, own, par, n_s) = refs[: 2 * prior], refs[2 * prior :]
    width = xs[0].shape[1]
    half = own.shape[1]
    step = 16

    def normalize(x, base):
        def rows_of(i, carry):
            rows = pl.ds(pl.multiple_of(i * step, step), step)
            total = jnp.zeros((step, 128), jnp.float32)
            for c in range(width // 1024):
                part = x[rows, pl.ds(c * 1024, 1024)].astype(jnp.float32)
                part = part * part
                for j in range(8):
                    total = total + part[:, j * 128 : (j + 1) * 128]
            mean = jnp.sum(total, axis=-1, keepdims=True) * (1.0 / width)
            scale = lax.rsqrt(mean + EPS)
            out = pl.ds(pl.multiple_of(base + i * step, step), step)
            for c in range(width // 1024):
                at = pl.ds(c * 1024, 1024)
                part = x[rows, at].astype(jnp.float32)
                part = part * scale * gain[:, at].astype(jnp.float32)
                n_s[out, at] = part.astype(jnp.bfloat16)
            return carry

        lax.fori_loop(0, x.shape[0] // step, rows_of, 0, unroll=2)

    base = 0
    for x in xs:
        normalize(x, base)
        base += x.shape[0]
    for k, (w, out) in enumerate(((wo, own), (wp, par))):
        acc = jnp.dot(n_s[...], w[...], preferred_element_type=jnp.float32)
        done = before[k].shape[0] if prior else 0
        if prior:
            out[:done] = before[k][...]
        out[done:] = acc.astype(jnp.bfloat16).reshape(-1, half, out.shape[2])


def project(xs, gain, wo, wp, half, before=()):
    rows = sum(x.shape[0] for x in xs)
    width, cols = wo.shape
    done = before[0].shape[0] if before else 0
    out = jax.ShapeDtypeStruct((done + rows // half, half, cols), jnp.bfloat16)
    return pl.pallas_call(
        functools.partial(project_kernel, len(xs), bool(before)),
        out_shape=(out, out),
        in_specs=[VMEM] * (len(xs) + len(before) + 3),
        out_specs=(VMEM, VMEM),
        scratch_shapes=[pltpu.VMEM((rows, width), jnp.bfloat16)],
        compiler_params=pltpu.CompilerParams(vmem_limit_bytes=16 * 1024 * 1024),
        cost_estimate=pl.CostEstimate(
            flops=2 * rows * width * 2 * cols,
            bytes_accessed=6 * 1024 * 1024,
            transcendentals=0,
        ),
        name="project",
    )(*xs, *before, gain, wo, wp)


def prepare_kernel(cum, q, fk, fv, ng, gates, qm, small):
    block, cols = gates.shape[1:]
    shape = (cols, cols)
    same = lax.broadcasted_iota(jnp.int32, shape, 0) // HD == (
        lax.broadcasted_iota(jnp.int32, shape, 1) // HD
    )
    first = lax.broadcasted_iota(jnp.int32, (2, cols), 1) < HD
    for p in range(2):
        spread = [jnp.broadcast_to(cum[p, h : h + 1, :], (HD, block)) for h in range(2)]
        gates[p] = jnp.concatenate(spread, axis=0).T
        down = jnp.broadcast_to(q[p : p + 1, :].astype(jnp.float32), shape).T
        qm[p] = jnp.where(same, down, 0.0).astype(jnp.bfloat16)
        fresh = jnp.dot(fk[...], qm[p], preferred_element_type=jnp.float32)
        small[p : p + 1, :] = fresh[p : p + 1] * (HD**-0.5)
    small[2:4, :] = fv[...].astype(jnp.float32)
    small[4:6, :] = jnp.where(first, ng[:, 0:1], ng[:, 1:2])
    small[6:8, :] = jnp.zeros((2, cols), jnp.float32)


def prepare(cum, q, fk, fv, ng):
    block, cols = cum.shape[2], q.shape[1]
    return pl.pallas_call(
        prepare_kernel,
        out_shape=(
            jax.ShapeDtypeStruct((2, block, cols), jnp.float32),
            jax.ShapeDtypeStruct((2, cols, cols), jnp.bfloat16),
            jax.ShapeDtypeStruct((8, cols), jnp.float32),
        ),
        in_specs=[VMEM] * 5,
        out_specs=(VMEM,) * 3,
        compiler_params=pltpu.CompilerParams(vmem_limit_bytes=8 * 1024 * 1024),
        cost_estimate=pl.CostEstimate(
            flops=1024 * 1024, bytes_accessed=1024 * 1024, transcendentals=0
        ),
        name="prepare",
    )(cum, q, fk, fv, ng)


def halves(own, got, places):
    tp = lax.axis_index("tp")
    x, core = tp // 2, lax.rem(tp, 2)
    half = own.shape[1]
    found = []
    for side, ref in enumerate((own, got)):
        which = lax.rem(core + side, 2)
        for k, (off, p) in enumerate(places):
            place = lax.rem(x + jnp.where(which == 0, off, (4 - off) % 4), 4)
            found.append((ref, k, p, pl.multiple_of((place * 2 + which) * half, half)))
    return found


def stored(found, keys, values, sem):
    cols = keys.shape[2]
    copies = []
    for i, (ref, k, p, at) in enumerate(found):
        rows = pl.ds(at, ref.shape[1])
        for j, cache in enumerate((keys, values)):
            copies.append(
                pltpu.make_async_copy(
                    ref.at[k, :, pl.ds(j * cols, cols)], cache.at[p, rows, :], sem.at[i, j]
                )
            )
    for copy in copies:
        copy.start()
    return copies


def scored(found, p, gates, qm):
    cols = qm.shape[2]
    parts, seen = [], []
    for ref, k, prompt, at in found:
        if prompt == p:
            part = jnp.dot(ref[k, :, :cols], qm[p], preferred_element_type=jnp.float32)
            parts.append(part * (HD**-0.5) - gates[p, pl.ds(at, ref.shape[1]), :])
            seen.append(ref[k, :, cols:].astype(jnp.float32))
    return jnp.concatenate(parts, axis=0), jnp.concatenate(seen, axis=0)


def early_kernel(own, got, gates, qm, keys, values, state, sem):
    found = halves(own, got, EARLY)
    copies = stored(found, keys, values, sem)
    for p in range(2):
        scores, seen = scored(found, p, gates, qm)
        top = jnp.max(scores, axis=0, keepdims=True)
        weights = jnp.exp(scores - top)
        state[4 * p : 4 * p + 1, :] = top
        state[4 * p + 1 : 4 * p + 2, :] = jnp.sum(weights, axis=0, keepdims=True)
        state[4 * p + 2 : 4 * p + 3, :] = jnp.sum(weights * seen, axis=0, keepdims=True)
        state[4 * p + 3 : 4 * p + 4, :] = jnp.zeros_like(top)
    for copy in copies:
        copy.wait()


def early(own, got, gates, qm):
    block, cols = gates.shape[1:]
    cache = jax.ShapeDtypeStruct((2, block, cols), jnp.bfloat16)
    return pl.pallas_call(
        early_kernel,
        out_shape=(cache, cache, jax.ShapeDtypeStruct((8, cols), jnp.float32)),
        in_specs=[VMEM] * 4,
        out_specs=(ANY, ANY, VMEM),
        scratch_shapes=[pltpu.SemaphoreType.DMA((2 * len(EARLY), 2))],
        compiler_params=pltpu.CompilerParams(vmem_limit_bytes=8 * 1024 * 1024),
        cost_estimate=pl.CostEstimate(
            flops=64 * 1024 * 1024, bytes_accessed=2 * 1024 * 1024, transcendentals=0
        ),
        name="early",
    )(own, got, gates, qm)


def late_kernel(own, both, gates, qm, small, state, part):
    core = lax.rem(lax.axis_index("tp"), 2)
    found = halves(own, both.at[1 - core], LATE)
    members, _, cols = part.shape
    block = gates.shape[1]
    last = lax.axis_index("sp") == lax.axis_size("sp") - 1
    for p in range(2):
        scores, seen = scored(found, p, gates, qm)
        fresh = small[p : p + 1, :] - (
            gates[p, block - 1 : block, :] + small[4 + p : 5 + p, :]
        )
        fresh = jnp.where(last, fresh, MASKED)
        before = state[4 * p : 4 * p + 1, :]
        top = jnp.maximum(jnp.max(scores, axis=0, keepdims=True), fresh)
        top = jnp.maximum(top, before)
        weights = jnp.exp(scores - top)
        fresh_weight = jnp.exp(fresh - top)
        scale = jnp.exp(before - top)
        total = jnp.sum(weights, axis=0, keepdims=True) + fresh_weight
        total = total + scale * state[4 * p + 1 : 4 * p + 2, :]
        acc = jnp.sum(weights * seen, axis=0, keepdims=True)
        acc = acc + fresh_weight * small[2 + p : 3 + p, :]
        acc = acc + scale * state[4 * p + 2 : 4 * p + 3, :]
        for r, row in ((2 * p, top), (2 * p + 1, top), (2 * p + 4, total), (2 * p + 5, acc)):
            part[:, r : r + 1, :] = jnp.broadcast_to(row[None], (members, 1, cols))


def late(own, both, gates, qm, small, state, members):
    cols = gates.shape[2]
    return pl.pallas_call(
        late_kernel,
        out_shape=jax.ShapeDtypeStruct((members, 8, cols), jnp.float32),
        in_specs=[VMEM] * 6,
        out_specs=VMEM,
        compiler_params=pltpu.CompilerParams(vmem_limit_bytes=4 * 1024 * 1024),
        cost_estimate=pl.CostEstimate(
            flops=16 * 1024 * 1024, bytes_accessed=1024 * 1024, transcendentals=0
        ),
        name="late",
    )(own, both, gates, qm, small, state)


def merge_kernel(parts, own, both, k_in, v_in, keys, values, out, sem):
    core = lax.rem(lax.axis_index("tp"), 2)
    copies = stored(halves(own, both.at[1 - core], LATE), keys, values, sem)
    tops = parts[:, 0:4, :]
    scale = jnp.exp(tops - jnp.max(tops, axis=0, keepdims=True))
    sums = jnp.sum(scale * parts[:, 4:8, :], axis=0)
    for p in range(2):
        out[p : p + 1, :] = (
            sums[2 * p + 1 : 2 * p + 2] / sums[2 * p : 2 * p + 1]
        ).astype(jnp.bfloat16)
    for copy in copies:
        copy.wait()


def merge(parts, own, both, keys, values):
    cache = jax.ShapeDtypeStruct(keys.shape, keys.dtype)
    return pl.pallas_call(
        merge_kernel,
        out_shape=(cache, cache, jax.ShapeDtypeStruct((2, parts.shape[2]), jnp.bfloat16)),
        in_specs=[VMEM] * 3 + [ANY] * 2,
        out_specs=(ANY, ANY, VMEM),
        input_output_aliases={3: 0, 4: 1},
        scratch_shapes=[pltpu.SemaphoreType.DMA((2 * len(LATE), 2))],
        compiler_params=pltpu.CompilerParams(vmem_limit_bytes=4 * 1024 * 1024),
        name="merge",
    )(parts, own, both, keys, values)


def split_kernel(tokens, a, b):
    a[...] = tokens[0]
    b[...] = tokens[1]


def split(tokens):
    piece = jax.ShapeDtypeStruct(tokens.shape[1:], tokens.dtype)
    return pl.pallas_call(
        split_kernel,
        out_shape=(piece, piece),
        in_specs=[VMEM],
        out_specs=(VMEM, VMEM),
        compiler_params=pltpu.CompilerParams(vmem_limit_bytes=4 * 1024 * 1024),
        cost_estimate=pl.CostEstimate(
            flops=1024 * 1024, bytes_accessed=2 * 1024 * 1024, transcendentals=0
        ),
        name="split",
    )(tokens)


def shift(x, by):
    return lax.ppermute(x, "tp", by)


def body(
    tokens, norm_gain, key_weight, value_weight, cum_gates, new_query, new_key, new_value, new_gate
):
    members = lax.axis_size("sp")
    tps = lax.axis_size("tp")
    ahead = [(i, (i + 2 - 4 * (i % 2)) % tps) for i in range(tps)]
    back = [(i, (i - 2 + 4 * (i % 2)) % tps) for i in range(tps)]
    swap = [(i, i ^ 1) for i in range(tps)]
    gain = norm_gain.reshape(1, -1)
    half, width = tokens.shape[1:]
    from_3 = shift(tokens, ahead)
    a_0, b_0 = split(tokens)
    b_1 = shift(b_0, back)
    a_1 = shift(a_0, back)
    b_2 = shift(b_1, back)
    a_2 = shift(from_3[0], ahead)
    wo = jnp.concatenate([key_weight, value_weight], axis=1)
    wp = shift(wo, swap)

    made = prepare(
        jnp.swapaxes(cum_gates, 1, 2), new_query, new_key, new_value, new_gate
    )
    gain, wp, made = lax.optimization_barrier((gain, wp, made))
    gates, qm, small = made

    rows = (2 * half, width)
    done = project((tokens.reshape(rows),), gain, wo, wp, half)
    own1, par1 = project((from_3.reshape(rows), b_1, a_1), gain, wo, wp, half, done)
    got1 = shift(par1, swap)
    done = project((a_2,), gain, wo, wp, half)
    keys, values, state = early(own1, got1, gates, qm)
    own2, par2 = project((b_2,), gain, wo, wp, half, done)
    pairs = [[i, i + 1] for i in range(0, tps, 2)]
    both2 = lax.all_gather(par2, "tp", axis_index_groups=pairs)
    part = late(own2, both2, gates, qm, small, state, members)
    parts = lax.all_to_all(part, "sp", split_axis=0, concat_axis=0, tiled=True)
    return merge(parts, own2, both2, keys, values)


def solution(mesh):
    in_specs = (
        P("gr", ("sp", "tp"), None),
        P(),
        P(None, "tp"),
        P(None, "tp"),
        P("gr", "sp", "tp"),
        P("gr", "tp"),
        P("gr", "tp"),
        P("gr", "tp"),
        P("gr", "tp"),
    )
    out_specs = (P("gr", "sp", "tp"), P("gr", "sp", "tp"), P("gr", "tp"))
    return jax.shard_map(body, mesh=mesh, in_specs=in_specs, out_specs=out_specs, check_vma=False)
```

profile of v0, /device:TPU:1, one launch (start us, length us, event | category | flops | bytes accessed | tf_op | source)
XLA Modules:
  0.0 70.8 jit_solution(8672392528516682790)
XLA Ops:
  0.6 0.0 copy-start
  0.6 0.0 copy-start.6
  0.7 5.3 %collective-permute-start.2 = (bf16[2,64,4096]{2,1,0:T(8,128)(2,1)}, bf16[2,64,4096]{2,1,0:T(8,128)(2,1)S(1)}, u32[]{:S(2)}, u32[]{:S(2)}) collective-permute-start(bf16[2,64,4096]{2,1,0:T(8,128)(2,1)} %tokens.1), channel_id=1, source_target_pairs={{0,2},{1,7},{2,4},{3,1},{4,6},{5,3},{6,0},{7,5},{8,10},{9,15},{10,... | collective-permute-start | bytes 3145736 | tf_op jit(solution)/shard_map/ppermute | solution.py:285
  6.0 1.4 %constant_dynamic-update-slice_fusion.1 = bf16[4096,256]{1,0:T(8,128)(2,1)S(1)} fusion(bf16[4096,128]{1,0:T(8,128)(2,1)} %param.11), kind=kLoop, calls=%fused_computation.2 | loop fusion | bytes 2097152
  7.4 0.0 copy-done.6
  7.4 0.0 copy-start.7
  7.4 0.0 copy-start.1
  7.4 0.0 copy-start.2
  7.4 0.0 copy-start.3
  7.5 0.0 copy-start.4
  7.5 0.0 copy-start.5
  7.5 0.2 constant_dynamic-update-slice_fusion.refs_2_.refs_4_.refs_6_
  7.7 9.1 %collective-permute-start.4 = (bf16[4096,256]{1,0:T(8,128)(2,1)S(1)}, bf16[4096,256]{1,0:T(8,128)(2,1)S(1)}, u32[]{:S(2)}, u32[]{:S(2)}) collective-permute-start(bf16[4096,256]{1,0:T(8,128)(2,1)S(1)} %constant_dynamic-update-slice_fusion.refs_2_.refs_4_.refs_6_), channel_id=1, source_target_pairs={{0,1},{1,0},{2,3},{3,2},{4,5},{5,4},{6,7},{7,6},{8,9},{9,8},{10,11... | collective-permute-start | bytes 6291464 | tf_op jit(solution)/shard_map/ppermute | solution.py:285
  16.9 0.0 copy-done
  16.9 0.1 split.1
  16.9 1.9 %collective-permute-start = (bf16[64,4096]{1,0:T(8,128)(2,1)S(1)}, bf16[64,4096]{1,0:T(8,128)(2,1)S(1)}, u32[]{:S(2)}, u32[]{:S(2)}) collective-permute-start(bf16[64,4096]{1,0:T(8,128)(2,1)S(1)} %get-tuple-element.24), channel_id=1, source_target_pairs={{0,6},{1,3},{2,0},{3,5},{4,2},{5,7},{6,4},{7,1},{8,14},{9,11},{10,... | collective-permute-start | bytes 1572872 | tf_op jit(solution)/shard_map/ppermute | solution.py:285
  18.9 1.9 %collective-permute-start.5 = (bf16[64,4096]{1,0:T(8,128)(2,1)S(1)}, bf16[64,4096]{1,0:T(8,128)(2,1)S(1)}, u32[]{:S(2)}, u32[]{:S(2)}) collective-permute-start(bf16[64,4096]{1,0:T(8,128)(2,1)S(1)} %get-tuple-element.37), channel_id=1, source_target_pairs={{0,6},{1,3},{2,0},{3,5},{4,2},{5,7},{6,4},{7,1},{8,14},{9,11},{10,... | collective-permute-start | bytes 1572872 | tf_op jit(solution)/shard_map/ppermute | solution.py:285
  20.8 0.0 collective-permute-done.2
  20.9 4.9 %collective-permute-start.3 = (bf16[64,4096]{1,0:T(8,128)(2,1)S(1)}, bf16[64,4096]{1,0:T(8,128)(2,1)S(1)}, u32[]{:S(2)}, u32[]{:S(2)}) collective-permute-start(bf16[64,4096]{1,0:T(8,128)(2,1)S(1)} %slice_bitcast_fusion), channel_id=1, source_target_pairs={{0,2},{1,7},{2,4},{3,1},{4,6},{5,3},{6,0},{7,5},{8,10},{9,15},{10,... | collective-permute-start | bytes 1572872 | tf_op jit(solution)/shard_map/ppermute | solution.py:285
  25.7 8.6 %collective-permute-done.refs_1_ = bf16[64,4096]{1,0:T(8,128)(2,1)S(1)} collective-permute-done((bf16[64,4096]{1,0:T(8,128)(2,1)S(1)}, bf16[64,4096]{1,0:T(8,128)(2,1)S(1)}, u32[]{:S(2)}, u32[]{:S(2)}) %collective-permute-start) | collective-permute-done | bytes 524320 | tf_op jit(solution)/shard_map/ppermute | solution.py:285
  34.3 1.9 %collective-permute-start.1 = (bf16[64,4096]{1,0:T(8,128)(2,1)S(1)}, bf16[64,4096]{1,0:T(8,128)(2,1)S(1)}, u32[]{:S(2)}, u32[]{:S(2)}) collective-permute-start(bf16[64,4096]{1,0:T(8,128)(2,1)S(1)} %collective-permute-done.refs_1_), channel_id=1, source_target_pairs={{0,6},{1,3},{2,0},{3,5},{4,2},{5,7},{6,4},{7,1},{8,14},{9,11},{10,... | collective-permute-start | bytes 1572872 | tf_op jit(solution)/shard_map/ppermute | solution.py:285
  36.2 0.0 copy-done.7
  36.2 0.0 copy-done.1
  36.2 0.0 copy-done.2
  36.2 0.0 copy-done.3
  36.2 0.0 copy-done.4
  36.3 0.0 copy-done.5
  36.3 0.3 prepare.1
  36.5 0.0 collective-permute-done.4.refs_3_.refs_5_.refs_7_
  36.5 1.4 %project.6 = (bf16[2,64,256]{2,1,0:T(8,128)(2,1)S(1)}, bf16[2,64,256]{2,1,0:T(8,128)(2,1)S(1)}) custom-call(bf16[128,4096]{1,0:T(8,128)(2,1)S(1)} %bitcast.6, bf16[1,4096]{1,0:T(2,128)(2,1)S(1)} %reshape.15.refs_1_.refs_3_.refs_5_, bf16[4096,256]{1,0:T(8,128)(2,1)S(1)} %constant_dynamic-update-slice_fusion.refs_2_.refs_4_.refs_6_, ...), custom_call_target="tpu_custom_call" | custom-call | flops 536870912 | bytes 6291456 | tf_op jit(solution)/shard_map/project/pallas_call | solution.py:68
  38.0 1.9 %collective-permute-done.5.refs_2_ = bf16[64,4096]{1,0:T(8,128)(2,1)S(1)} collective-permute-done((bf16[64,4096]{1,0:T(8,128)(2,1)S(1)}, bf16[64,4096]{1,0:T(8,128)(2,1)S(1)}, u32[]{:S(2)}, u32[]{:S(2)}) %collective-permute-start.5) | collective-permute-done | bytes 524320 | tf_op jit(solution)/shard_map/ppermute | solution.py:285
  39.9 2.7 %project.7 = (bf16[6,64,256]{2,1,0:T(8,128)(2,1)S(1)}, bf16[6,64,256]{2,1,0:T(8,128)(2,1)S(1)}) custom-call(bf16[128,4096]{1,0:T(8,128)(2,1)S(1)} %bitcast.7, bf16[64,4096]{1,0:T(8,128)(2,1)S(1)} %collective-permute-done.refs_1_, bf16[64,4096]{1,0:T(8,128)(2,1)S(1)} %collective-permute-done.5.refs_2_, bf16[2,64,256]{2,1,0:T(8,128)(2,1)S(1)} %get-tuple-element.38.refs_3_, ...), custom_call_target="tpu_custom_call" | custom-call | flops 1073741824 | bytes 6291456 | tf_op jit(solution)/shard_map/project/pallas_call | solution.py:68
  42.6 6.2 %collective-permute-start.6 = (bf16[6,64,256]{2,1,0:T(8,128)(2,1)S(1)}, bf16[6,64,256]{2,1,0:T(8,128)(2,1)S(1)}, u32[]{:S(2)}, u32[]{:S(2)}) collective-permute-start(bf16[6,64,256]{2,1,0:T(8,128)(2,1)S(1)} %get-tuple-element.41), channel_id=1, source_target_pairs={{0,1},{1,0},{2,3},{3,2},{4,5},{5,4},{6,7},{7,6},{8,9},{9,8},{10,11... | collective-permute-start | bytes 589832 | tf_op jit(solution)/shard_map/ppermute | solution.py:285
  48.8 0.0 collective-permute-done.3.refs_0_
  48.8 1.2 %project.4 = (bf16[1,64,256]{2,1,0:T(8,128)(2,1)S(1)}, bf16[1,64,256]{2,1,0:T(8,128)(2,1)S(1)}) custom-call(bf16[64,4096]{1,0:T(8,128)(2,1)S(1)} %collective-permute-done.3.refs_0_, bf16[1,4096]{1,0:T(2,128)(2,1)S(1)} %reshape.15.refs_1_.refs_3_.refs_5_, bf16[4096,256]{1,0:T(8,128)(2,1)S(1)} %constant_dynamic-update-slice_fusion.refs_2_.refs_4_.refs_6_, ...), custom_call_target="tpu_custom_call" | custom-call | flops 268435456 | bytes 6291456 | tf_op jit(solution)/shard_map/project/pallas_call | solution.py:68
  50.0 0.0 collective-permute-done.1.refs_0_
  50.0 1.2 %project.5 = (bf16[2,64,256]{2,1,0:T(8,128)(2,1)S(1)}, bf16[2,64,256]{2,1,0:T(8,128)(2,1)S(1)}) custom-call(bf16[64,4096]{1,0:T(8,128)(2,1)S(1)} %collective-permute-done.1.refs_0_, bf16[1,64,256]{2,1,0:T(8,128)(2,1)S(1)} %get-tuple-element.30.refs_1_, bf16[1,64,256]{2,1,0:T(8,128)(2,1)S(1)} %get-tuple-element.31.refs_2_, ...), custom_call_target="tpu_custom_call" | custom-call | flops 268435456 | bytes 6291456 | tf_op jit(solution)/shard_map/project/pallas_call | solution.py:68
  51.2 4.5 %all-gather = bf16[4,64,256]{2,1,0:T(8,128)(2,1)S(1)} all-gather(bf16[2,64,256]{2,1,0:T(8,128)(2,1)S(1)} %get-tuple-element.33), channel_id=2, replica_groups={{0,1},{2,3},{4,5},{6,7},{8,9},{10,11},{12,13},{14,15},{16,17},{18,19},{..., dimensions={0}, use_global_device_ids=true | all-gather | bytes 196608 | tf_op jit(solution)/shard_map/all_gather | solution.py:321
  55.8 0.0 collective-permute-done.6.got
  55.8 1.2 %early.1 = (bf16[2,512,128]{2,1,0:T(8,128)(2,1)}, bf16[2,512,128]{2,1,0:T(8,128)(2,1)}, f32[8,128]{1,0:T(8,128)S(1)}) custom-call(bf16[6,64,256]{2,1,0:T(8,128)(2,1)S(1)} %get-tuple-element.40.own, bf16[6,64,256]{2,1,0:T(8,128)(2,1)S(1)} %collective-permute-done.6.got, f32[2,512,128]{2,1,0:T(8,128)S(1)} %get-tuple-element.34.gates, ...), custom_call_target="tpu_custom_call" | custom-call | flops 67108864 | bytes 2097152 | tf_op jit(solution)/shard_map/early/pallas_call | solution.py:180
  57.0 0.2 late.1
  57.2 12.3 %all_to_all.5.parts = f32[32,8,128]{2,1,0:T(8,128)S(1)} all-to-all(f32[32,8,128]{2,1,0:T(8,128)S(1)} %late.1), channel_id=1, replica_groups=mesh['gr'=3,'sp'=32,'tp'=8] {'sp'}, dimensions={0} | all-to-all | bytes 262144 | tf_op jit(solution)/shard_map/all_to_all | solution.py:323
  69.6 1.2 %merge.1 = (bf16[2,512,128]{2,1,0:T(8,128)(2,1)}, bf16[2,512,128]{2,1,0:T(8,128)(2,1)}, bf16[2,128]{1,0:T(2,128)(2,1)}) custom-call(f32[32,8,128]{2,1,0:T(8,128)S(1)} %all_to_all.5.parts, bf16[2,64,256]{2,1,0:T(8,128)(2,1)S(1)} %get-tuple-element.32.own, bf16[2,2,64,256]{3,2,1,0:T(8,128)(2,1)S(1)} %bitcast.9, ...), custom_call_target="tpu_custom_call", output_to_operand_aliasing={{0}: (3, {}), {1}: (4, {})} | custom-call | tf_op jit(solution)/shard_map/merge/pallas_call | solution.py:252
  (2 shorter events, 0.0 us)
Async XLA Ops:
  0.6 16.2 %copy-start = (bf16[2,64,4096]{2,1,0:T(8,128)(2,1)S(1)}, bf16[2,64,4096]{2,1,0:T(8,128)(2,1)}, u32[]{:S(2)}) copy-start(bf16[2,64,4096]{2,1,0:T(8,128)(2,1)} %tokens.1) | copy-start | bytes 3145732
  0.6 6.8 %copy-start.6 = (bf16[4096,128]{1,0:T(8,128)(2,1)S(1)}, bf16[4096,128]{1,0:T(8,128)(2,1)}, u32[]{:S(2)}) copy-start(bf16[4096,128]{1,0:T(8,128)(2,1)} %param.12) | copy-start | bytes 3145732
  0.7 20.1 %collective-permute-start.2 = (bf16[2,64,4096]{2,1,0:T(8,128)(2,1)}, bf16[2,64,4096]{2,1,0:T(8,128)(2,1)S(1)}, u32[]{:S(2)}, u32[]{:S(2)}) collective-permute-start(bf16[2,64,4096]{2,1,0:T(8,128)(2,1)} %tokens.1), channel_id=1, source_target_pairs={{0,2},{1,7},{2,4},{3,1},{4,6},{5,3},{6,0},{7,5},{8,10},{9,15},{10,... | collective-permute-start | bytes 3145736 | tf_op jit(solution)/shard_map/ppermute | solution.py:285
  7.4 28.8 %copy-start.7 = (bf16[4096]{0:T(1024)(128)(2,1)S(1)}, bf16[4096]{0:T(1024)(128)(2,1)}, u32[]{:S(2)}) copy-start(bf16[4096]{0:T(1024)(128)(2,1)} %param.10) | copy-start | bytes 24580
  7.4 28.8 %copy-start.1 = (f32[2,512,2]{1,2,0:T(2,128)S(1)}, f32[2,512,2]{1,2,0:T(2,128)}, u32[]{:S(2)}) copy-start(f32[2,512,2]{1,2,0:T(2,128)} %param.13) | copy-start | bytes 24580
  7.4 28.8 %copy-start.2 = (f32[2,2]{1,0:T(2,128)S(1)}, f32[2,2]{1,0:T(2,128)}, u32[]{:S(2)}) copy-start(f32[2,2]{1,0:T(2,128)} %ng.1) | copy-start | bytes 52
  7.4 28.8 %copy-start.3 = (bf16[2,128]{1,0:T(2,128)(2,1)S(1)}, bf16[2,128]{1,0:T(2,128)(2,1)}, u32[]{:S(2)}) copy-start(bf16[2,128]{1,0:T(2,128)(2,1)} %q.1) | copy-start | bytes 1540
  7.5 28.8 %copy-start.4 = (bf16[2,128]{1,0:T(2,128)(2,1)S(1)}, bf16[2,128]{1,0:T(2,128)(2,1)}, u32[]{:S(2)}) copy-start(bf16[2,128]{1,0:T(2,128)(2,1)} %fk.1) | copy-start | bytes 1540
  7.5 28.8 %copy-start.5 = (bf16[2,128]{1,0:T(2,128)(2,1)S(1)}, bf16[2,128]{1,0:T(2,128)(2,1)}, u32[]{:S(2)}) copy-start(bf16[2,128]{1,0:T(2,128)(2,1)} %fv.1) | copy-start | bytes 1540
  7.7 28.8 %collective-permute-start.4 = (bf16[4096,256]{1,0:T(8,128)(2,1)S(1)}, bf16[4096,256]{1,0:T(8,128)(2,1)S(1)}, u32[]{:S(2)}, u32[]{:S(2)}) collective-permute-start(bf16[4096,256]{1,0:T(8,128)(2,1)S(1)} %constant_dynamic-update-slice_fusion.refs_2_.refs_4_.refs_6_), channel_id=1, source_target_pairs={{0,1},{1,0},{2,3},{3,2},{4,5},{5,4},{6,7},{7,6},{8,9},{9,8},{10,11... | collective-permute-start | bytes 6291464 | tf_op jit(solution)/shard_map/ppermute | solution.py:285
  16.9 17.3 %collective-permute-start = (bf16[64,4096]{1,0:T(8,128)(2,1)S(1)}, bf16[64,4096]{1,0:T(8,128)(2,1)S(1)}, u32[]{:S(2)}, u32[]{:S(2)}) collective-permute-start(bf16[64,4096]{1,0:T(8,128)(2,1)S(1)} %get-tuple-element.24), channel_id=1, source_target_pairs={{0,6},{1,3},{2,0},{3,5},{4,2},{5,7},{6,4},{7,1},{8,14},{9,11},{10,... | collective-permute-start | bytes 1572872 | tf_op jit(solution)/shard_map/ppermute | solution.py:285
  18.9 21.0 %collective-permute-start.5 = (bf16[64,4096]{1,0:T(8,128)(2,1)S(1)}, bf16[64,4096]{1,0:T(8,128)(2,1)S(1)}, u32[]{:S(2)}, u32[]{:S(2)}) collective-permute-start(bf16[64,4096]{1,0:T(8,128)(2,1)S(1)} %get-tuple-element.37), channel_id=1, source_target_pairs={{0,6},{1,3},{2,0},{3,5},{4,2},{5,7},{6,4},{7,1},{8,14},{9,11},{10,... | collective-permute-start | bytes 1572872 | tf_op jit(solution)/shard_map/ppermute | solution.py:285
  20.9 28.0 %collective-permute-start.3 = (bf16[64,4096]{1,0:T(8,128)(2,1)S(1)}, bf16[64,4096]{1,0:T(8,128)(2,1)S(1)}, u32[]{:S(2)}, u32[]{:S(2)}) collective-permute-start(bf16[64,4096]{1,0:T(8,128)(2,1)S(1)} %slice_bitcast_fusion), channel_id=1, source_target_pairs={{0,2},{1,7},{2,4},{3,1},{4,6},{5,3},{6,0},{7,5},{8,10},{9,15},{10,... | collective-permute-start | bytes 1572872 | tf_op jit(solution)/shard_map/ppermute | solution.py:285
  34.3 15.8 %collective-permute-start.1 = (bf16[64,4096]{1,0:T(8,128)(2,1)S(1)}, bf16[64,4096]{1,0:T(8,128)(2,1)S(1)}, u32[]{:S(2)}, u32[]{:S(2)}) collective-permute-start(bf16[64,4096]{1,0:T(8,128)(2,1)S(1)} %collective-permute-done.refs_1_), channel_id=1, source_target_pairs={{0,6},{1,3},{2,0},{3,5},{4,2},{5,7},{6,4},{7,1},{8,14},{9,11},{10,... | collective-permute-start | bytes 1572872 | tf_op jit(solution)/shard_map/ppermute | solution.py:285
  42.6 13.2 %collective-permute-start.6 = (bf16[6,64,256]{2,1,0:T(8,128)(2,1)S(1)}, bf16[6,64,256]{2,1,0:T(8,128)(2,1)S(1)}, u32[]{:S(2)}, u32[]{:S(2)}) collective-permute-start(bf16[6,64,256]{2,1,0:T(8,128)(2,1)S(1)} %get-tuple-element.41), channel_id=1, source_target_pairs={{0,1},{1,0},{2,3},{3,2},{4,5},{5,4},{6,7},{7,6},{8,9},{9,8},{10,11... | collective-permute-start | bytes 589832 | tf_op jit(solution)/shard_map/ppermute | solution.py:285
where the time goes:
time: 71.2 us; the launch traced here: 70.8 us
  starting transfers between devices  31.3 us (44%)
  blocking collectives  16.9 us (24%)
  waiting for transfers between devices  10.5 us (15%)
  Pallas kernels  9.47 us (13%)
  local copies, waits for them, and re-layouts  1.75 us (2%)
  between operations  0.93 us (1%)
    ppermute x7, starting transfers between devices, shift(): return lax.ppermute(x, 'tp', by)  31.3 us
    all_to_all x1, blocking collectives, body(): parts = lax.all_to_all(part, 'sp', split_axis=0, concat_axis=0, tiled=True)  12.3 us
    ppermute x7, waiting for transfers between devices, shift(): return lax.ppermute(x, 'tp', by)  10.5 us
    pallas_call x4, Pallas kernels, project(): pl.pallas_call(functools.partial(project_kernel, len(xs), bool(before)),...  6.45 us
    all_gather x1, blocking collectives, body(): both2 = lax.all_gather(par2, 'tp', axis_index_groups=pairs)  4.55 us
    unnamed x17, local copies, waits for them, and re-layouts  1.45 us
  transfers between devices with their start and end apart: 7, of which 2 were waited for; matrix products, arithmetic and copies ran while one was open for 2% of the time, Pallas kernels for 10%

commit v1 on v0

--- a/solution.py
+++ b/solution.py
@@ -196,6 +196,7 @@
     found = halves(own, both.at[1 - core], LATE)
     members, _, cols = part.shape
     block = gates.shape[1]
+    low = lax.broadcasted_iota(jnp.int32, (1, cols), 1) % HD < HD // 2
     last = lax.axis_index("sp") == lax.axis_size("sp") - 1
     for p in range(2):
         scores, seen = scored(found, p, gates, qm)
@@ -214,7 +215,7 @@
         acc = jnp.sum(weights * seen, axis=0, keepdims=True)
         acc = acc + fresh_weight * small[2 + p : 3 + p, :]
         acc = acc + scale * state[4 * p + 2 : 4 * p + 3, :]
-        for r, row in ((2 * p, top), (2 * p + 1, top), (2 * p + 4, total), (2 * p + 5, acc)):
+        for r, row in ((p, jnp.where(low, top, total)), (p + 2, acc)):
             part[:, r : r + 1, :] = jnp.broadcast_to(row[None], (members, 1, cols))
 
 
@@ -222,7 +223,7 @@
     cols = gates.shape[2]
     return pl.pallas_call(
         late_kernel,
-        out_shape=jax.ShapeDtypeStruct((members, 8, cols), jnp.float32),
+        out_shape=jax.ShapeDtypeStruct((members, 4, cols), jnp.float32),
         in_specs=[VMEM] * 6,
         out_specs=VMEM,
         compiler_params=pltpu.CompilerParams(vmem_limit_bytes=4 * 1024 * 1024),
@@ -236,13 +237,16 @@
 def merge_kernel(parts, own, both, k_in, v_in, keys, values, out, sem):
     core = lax.rem(lax.axis_index("tp"), 2)
     copies = stored(halves(own, both.at[1 - core], LATE), keys, values, sem)
-    tops = parts[:, 0:4, :]
-    scale = jnp.exp(tops - jnp.max(tops, axis=0, keepdims=True))
-    sums = jnp.sum(scale * parts[:, 4:8, :], axis=0)
+    members, _, cols = parts.shape
+    low = lax.broadcasted_iota(jnp.int32, (members, cols), 1) % HD < HD // 2
     for p in range(2):
-        out[p : p + 1, :] = (
-            sums[2 * p + 1 : 2 * p + 2] / sums[2 * p : 2 * p + 1]
-        ).astype(jnp.bfloat16)
+        both_of = parts[:, p, :]
+        tops = jnp.where(low, both_of, pltpu.roll(both_of, HD // 2, 1))
+        totals = jnp.where(low, pltpu.roll(both_of, cols - HD // 2, 1), both_of)
+        scale = jnp.exp(tops - jnp.max(tops, axis=0, keepdims=True))
+        total = jnp.sum(scale * totals, axis=0, keepdims=True)
+        acc = jnp.sum(scale * parts[:, p + 2, :], axis=0, keepdims=True)
+        out[p : p + 1, :] = (acc / total).astype(jnp.bfloat16)
     for copy in copies:
         copy.wait()
 
@@ -314,9 +318,8 @@
     done = project((tokens.reshape(rows),), gain, wo, wp, half)
     own1, par1 = project((from_3.reshape(rows), b_1, a_1), gain, wo, wp, half, done)
     got1 = shift(par1, swap)
-    done = project((a_2,), gain, wo, wp, half)
     keys, values, state = early(own1, got1, gates, qm)
-    own2, par2 = project((b_2,), gain, wo, wp, half, done)
+    own2, par2 = project((a_2, b_2), gain, wo, wp, half)
     pairs = [[i, i + 1] for i in range(0, tps, 2)]
     both2 = lax.all_gather(par2, "tp", axis_index_groups=pairs)
     part = late(own2, both2, gates, qm, small, state, members)

time: 71.2 us -> 70.6 us (level)
  waiting for transfers between devices: 10.5 us -> 16.3 us
  starting transfers between devices: 31.3 us -> 26.7 us
  Pallas kernels: 9.47 us -> 8.54 us
  blocking collectives: 16.9 us -> 16 us
    ppermute x7, waiting for transfers between devices: 10.5 us -> 16.3 us  [shift(): return lax.ppermute(x, 'tp', by)]
    ppermute x7, starting transfers between devices: 31.3 us -> 26.7 us  [shift(): return lax.ppermute(x, 'tp', by)]
    all_gather x1, blocking collectives: 4.55 us -> 3.35 us  [body(): both2 = lax.all_gather(par2, 'tp', axis_index_groups=pairs)]
    pallas_call x4 -> x3, Pallas kernels: 6.45 us -> 5.51 us  [project(): pl.pallas_call(functools.partial(project_kernel, len(xs), bool(before)),...]
  transfers between devices with their start and end apart: 7 -> 7, of which waited for: 2 -> 2; matrix products, arithmetic and copies ran while one was open for 2% -> 2% of each run, Pallas kernels for 10% -> 8%
where the time goes in v1:
time: 70.6 us; the launch traced here: 70.1 us
  starting transfers between devices  26.7 us (38%)
  waiting for transfers between devices  16.3 us (23%)
  blocking collectives  16 us (23%)
  Pallas kernels  8.54 us (12%)
  local copies, waits for them, and re-layouts  1.75 us (2%)
  between operations  0.92 us (1%)
    ppermute x7, starting transfers between devices, shift(): return lax.ppermute(x, 'tp', by)  26.7 us
    ppermute x7, waiting for transfers between devices, shift(): return lax.ppermute(x, 'tp', by)  16.3 us
    all_to_all x1, blocking collectives, body(): parts = lax.all_to_all(part, 'sp', split_axis=0, concat_axis=0, tiled=True)  12.6 us
    pallas_call x3, Pallas kernels, project(): pl.pallas_call(functools.partial(project_kernel, len(xs), bool(before)),...  5.51 us
    all_gather x1, blocking collectives, body(): both2 = lax.all_gather(par2, 'tp', axis_index_groups=pairs)  3.35 us
    unnamed x17, local copies, waits for them, and re-layouts  1.45 us
  transfers between devices with their start and end apart: 7, of which 2 were waited for; matrix products, arithmetic and copies ran while one was open for 2% of the time, Pallas kernels for 8%

profile of v1, /device:TPU:1, one launch (start us, length us, event | category | flops | bytes accessed | tf_op | source)
XLA Modules:
  0.0 70.1 jit_solution(12061089725741280519)
XLA Ops:
  0.6 0.0 copy-start
  0.6 0.0 copy-start.6
  0.7 5.3 %collective-permute-start = (bf16[2,64,4096]{2,1,0:T(8,128)(2,1)}, bf16[2,64,4096]{2,1,0:T(8,128)(2,1)S(1)}, u32[]{:S(2)}, u32[]{:S(2)}) collective-permute-start(bf16[2,64,4096]{2,1,0:T(8,128)(2,1)} %tokens.1), channel_id=1, source_target_pairs={{0,2},{1,7},{2,4},{3,1},{4,6},{5,3},{6,0},{7,5},{8,10},{9,15},{10,... | collective-permute-start | bytes 3145736 | tf_op jit(solution)/shard_map/ppermute | solution.py:289
  6.0 1.4 %constant_dynamic-update-slice_fusion.1 = bf16[4096,256]{1,0:T(8,128)(2,1)S(1)} fusion(bf16[4096,128]{1,0:T(8,128)(2,1)} %param.11), kind=kLoop, calls=%fused_computation.2 | loop fusion | bytes 2097152
  7.4 0.0 copy-done.6
  7.4 0.0 copy-start.7
  7.4 0.0 copy-start.1
  7.4 0.0 copy-start.2
  7.4 0.0 copy-start.3
  7.5 0.0 copy-start.4
  7.5 0.0 copy-start.5
  7.5 0.2 constant_dynamic-update-slice_fusion.refs_3_.refs_2_.refs_6_
  7.7 9.1 %collective-permute-start.4 = (bf16[4096,256]{1,0:T(8,128)(2,1)S(1)}, bf16[4096,256]{1,0:T(8,128)(2,1)S(1)}, u32[]{:S(2)}, u32[]{:S(2)}) collective-permute-start(bf16[4096,256]{1,0:T(8,128)(2,1)S(1)} %constant_dynamic-update-slice_fusion.refs_3_.refs_2_.refs_6_), channel_id=1, source_target_pairs={{0,1},{1,0},{2,3},{3,2},{4,5},{5,4},{6,7},{7,6},{8,9},{9,8},{10,11... | collective-permute-start | bytes 6291464 | tf_op jit(solution)/shard_map/ppermute | solution.py:289
  16.9 0.0 copy-done
  16.9 0.1 split.1
  16.9 1.9 %collective-permute-start.2 = (bf16[64,4096]{1,0:T(8,128)(2,1)S(1)}, bf16[64,4096]{1,0:T(8,128)(2,1)S(1)}, u32[]{:S(2)}, u32[]{:S(2)}) collective-permute-start(bf16[64,4096]{1,0:T(8,128)(2,1)S(1)} %get-tuple-element.22), channel_id=1, source_target_pairs={{0,6},{1,3},{2,0},{3,5},{4,2},{5,7},{6,4},{7,1},{8,14},{9,11},{10,... | collective-permute-start | bytes 1572872 | tf_op jit(solution)/shard_map/ppermute | solution.py:289
  18.9 1.9 %collective-permute-start.5 = (bf16[64,4096]{1,0:T(8,128)(2,1)S(1)}, bf16[64,4096]{1,0:T(8,128)(2,1)S(1)}, u32[]{:S(2)}, u32[]{:S(2)}) collective-permute-start(bf16[64,4096]{1,0:T(8,128)(2,1)S(1)} %get-tuple-element.33), channel_id=1, source_target_pairs={{0,6},{1,3},{2,0},{3,5},{4,2},{5,7},{6,4},{7,1},{8,14},{9,11},{10,... | collective-permute-start | bytes 1572872 | tf_op jit(solution)/shard_map/ppermute | solution.py:289
  20.8 13.5 %collective-permute-done.2.refs_1_ = bf16[64,4096]{1,0:T(8,128)(2,1)S(1)} collective-permute-done((bf16[64,4096]{1,0:T(8,128)(2,1)S(1)}, bf16[64,4096]{1,0:T(8,128)(2,1)S(1)}, u32[]{:S(2)}, u32[]{:S(2)}) %collective-permute-start.2) | collective-permute-done | bytes 524320 | tf_op jit(solution)/shard_map/ppermute | solution.py:289
  34.3 1.9 %collective-permute-start.3 = (bf16[64,4096]{1,0:T(8,128)(2,1)S(1)}, bf16[64,4096]{1,0:T(8,128)(2,1)S(1)}, u32[]{:S(2)}, u32[]{:S(2)}) collective-permute-start(bf16[64,4096]{1,0:T(8,128)(2,1)S(1)} %collective-permute-done.2.refs_1_), channel_id=1, source_target_pairs={{0,6},{1,3},{2,0},{3,5},{4,2},{5,7},{6,4},{7,1},{8,14},{9,11},{10,... | collective-permute-start | bytes 1572872 | tf_op jit(solution)/shard_map/ppermute | solution.py:289
  36.2 0.0 collective-permute-done
  36.2 4.6 %collective-permute-start.1 = (bf16[64,4096]{1,0:T(8,128)(2,1)S(1)}, bf16[64,4096]{1,0:T(8,128)(2,1)S(1)}, u32[]{:S(2)}, u32[]{:S(2)}) collective-permute-start(bf16[64,4096]{1,0:T(8,128)(2,1)S(1)} %slice_bitcast_fusion), channel_id=1, source_target_pairs={{0,2},{1,7},{2,4},{3,1},{4,6},{5,3},{6,0},{7,5},{8,10},{9,15},{10,... | collective-permute-start | bytes 1572872 | tf_op jit(solution)/shard_map/ppermute | solution.py:289
  40.8 0.0 copy-done.7
  40.8 0.0 copy-done.1
  40.9 0.0 copy-done.2
  40.9 0.0 copy-done.3
  40.9 0.0 copy-done.4
  40.9 0.0 copy-done.5
  40.9 0.3 prepare.1
  41.2 0.0 collective-permute-done.4.refs_4_.refs_3_.refs_7_
  41.2 1.4 %project.4 = (bf16[2,64,256]{2,1,0:T(8,128)(2,1)S(1)}, bf16[2,64,256]{2,1,0:T(8,128)(2,1)S(1)}) custom-call(bf16[128,4096]{1,0:T(8,128)(2,1)S(1)} %bitcast.6, bf16[1,4096]{1,0:T(2,128)(2,1)S(1)} %reshape.15.refs_2_.refs_1_.refs_5_, bf16[4096,256]{1,0:T(8,128)(2,1)S(1)} %constant_dynamic-update-slice_fusion.refs_3_.refs_2_.refs_6_, ...), custom_call_target="tpu_custom_call" | custom-call | flops 536870912 | bytes 6291456 | tf_op jit(solution)/shard_map/project/pallas_call | solution.py:68
  42.6 0.0 collective-permute-done.5.refs_2_
  42.6 2.7 %project.5 = (bf16[6,64,256]{2,1,0:T(8,128)(2,1)S(1)}, bf16[6,64,256]{2,1,0:T(8,128)(2,1)S(1)}) custom-call(bf16[128,4096]{1,0:T(8,128)(2,1)S(1)} %bitcast.7, bf16[64,4096]{1,0:T(8,128)(2,1)S(1)} %collective-permute-done.2.refs_1_, bf16[64,4096]{1,0:T(8,128)(2,1)S(1)} %collective-permute-done.5.refs_2_, bf16[2,64,256]{2,1,0:T(8,128)(2,1)S(1)} %get-tuple-element.34.refs_3_, ...), custom_call_target="tpu_custom_call" | custom-call | flops 1073741824 | bytes 6291456 | tf_op jit(solution)/shard_map/project/pallas_call | solution.py:68
  45.3 1.9 %collective-permute-start.6 = (bf16[6,64,256]{2,1,0:T(8,128)(2,1)S(1)}, bf16[6,64,256]{2,1,0:T(8,128)(2,1)S(1)}, u32[]{:S(2)}, u32[]{:S(2)}) collective-permute-start(bf16[6,64,256]{2,1,0:T(8,128)(2,1)S(1)} %get-tuple-element.37), channel_id=1, source_target_pairs={{0,1},{1,0},{2,3},{3,2},{4,5},{5,4},{6,7},{7,6},{8,9},{9,8},{10,11... | collective-permute-start | bytes 589832 | tf_op jit(solution)/shard_map/ppermute | solution.py:289
  47.2 2.8 %collective-permute-done.3.refs_1_ = bf16[64,4096]{1,0:T(8,128)(2,1)S(1)} collective-permute-done((bf16[64,4096]{1,0:T(8,128)(2,1)S(1)}, bf16[64,4096]{1,0:T(8,128)(2,1)S(1)}, u32[]{:S(2)}, u32[]{:S(2)}) %collective-permute-start.3) | collective-permute-done | bytes 524320 | tf_op jit(solution)/shard_map/ppermute | solution.py:289
  50.0 0.0 collective-permute-done.1.refs_0_
  50.0 1.4 %project.3 = (bf16[2,64,256]{2,1,0:T(8,128)(2,1)S(1)}, bf16[2,64,256]{2,1,0:T(8,128)(2,1)S(1)}) custom-call(bf16[64,4096]{1,0:T(8,128)(2,1)S(1)} %collective-permute-done.1.refs_0_, bf16[64,4096]{1,0:T(8,128)(2,1)S(1)} %collective-permute-done.3.refs_1_, bf16[1,4096]{1,0:T(2,128)(2,1)S(1)} %reshape.15.refs_2_.refs_1_.refs_5_, ...), custom_call_target="tpu_custom_call" | custom-call | flops 536870912 | bytes 6291456 | tf_op jit(solution)/shard_map/project/pallas_call | solution.py:68
  51.5 3.4 %all-gather = bf16[4,64,256]{2,1,0:T(8,128)(2,1)S(1)} all-gather(bf16[2,64,256]{2,1,0:T(8,128)(2,1)S(1)} %get-tuple-element.29), channel_id=2, replica_groups={{0,1},{2,3},{4,5},{6,7},{8,9},{10,11},{12,13},{14,15},{16,17},{18,19},{..., dimensions={0}, use_global_device_ids=true | all-gather | bytes 196608 | tf_op jit(solution)/shard_map/all_gather | solution.py:324
  54.8 0.0 collective-permute-done.6.got
  54.8 1.2 %early.1 = (bf16[2,512,128]{2,1,0:T(8,128)(2,1)}, bf16[2,512,128]{2,1,0:T(8,128)(2,1)}, f32[8,128]{1,0:T(8,128)S(1)}) custom-call(bf16[6,64,256]{2,1,0:T(8,128)(2,1)S(1)} %get-tuple-element.36.own, bf16[6,64,256]{2,1,0:T(8,128)(2,1)S(1)} %collective-permute-done.6.got, f32[2,512,128]{2,1,0:T(8,128)S(1)} %get-tuple-element.30.gates, ...), custom_call_target="tpu_custom_call" | custom-call | flops 67108864 | bytes 2097152 | tf_op jit(solution)/shard_map/early/pallas_call | solution.py:180
  56.0 0.2 late.1
  56.3 12.6 %all_to_all.5.parts = f32[32,4,128]{2,1,0:T(4,128)S(1)} all-to-all(f32[32,4,128]{2,1,0:T(4,128)S(1)} %late.1), channel_id=1, replica_groups=mesh['gr'=3,'sp'=32,'tp'=8] {'sp'}, dimensions={0} | all-to-all | bytes 131072 | tf_op jit(solution)/shard_map/all_to_all | solution.py:326
  68.9 1.3 %merge.1 = (bf16[2,512,128]{2,1,0:T(8,128)(2,1)}, bf16[2,512,128]{2,1,0:T(8,128)(2,1)}, bf16[2,128]{1,0:T(2,128)(2,1)}) custom-call(f32[32,4,128]{2,1,0:T(4,128)S(1)} %all_to_all.5.parts, bf16[2,64,256]{2,1,0:T(8,128)(2,1)S(1)} %get-tuple-element.28.own, bf16[2,2,64,256]{3,2,1,0:T(8,128)(2,1)S(1)} %bitcast.9, ...), custom_call_target="tpu_custom_call", output_to_operand_aliasing={{0}: (3, {}), {1}: (4, {})} | custom-call | tf_op jit(solution)/shard_map/merge/pallas_call | solution.py:256
  (2 shorter events, 0.0 us)
Async XLA Ops:
  0.6 16.2 %copy-start = (bf16[2,64,4096]{2,1,0:T(8,128)(2,1)S(1)}, bf16[2,64,4096]{2,1,0:T(8,128)(2,1)}, u32[]{:S(2)}) copy-start(bf16[2,64,4096]{2,1,0:T(8,128)(2,1)} %tokens.1) | copy-start | bytes 3145732
  0.6 6.8 %copy-start.6 = (bf16[4096,128]{1,0:T(8,128)(2,1)S(1)}, bf16[4096,128]{1,0:T(8,128)(2,1)}, u32[]{:S(2)}) copy-start(bf16[4096,128]{1,0:T(8,128)(2,1)} %param.12) | copy-start | bytes 3145732
  0.7 35.5 %collective-permute-start = (bf16[2,64,4096]{2,1,0:T(8,128)(2,1)}, bf16[2,64,4096]{2,1,0:T(8,128)(2,1)S(1)}, u32[]{:S(2)}, u32[]{:S(2)}) collective-permute-start(bf16[2,64,4096]{2,1,0:T(8,128)(2,1)} %tokens.1), channel_id=1, source_target_pairs={{0,2},{1,7},{2,4},{3,1},{4,6},{5,3},{6,0},{7,5},{8,10},{9,15},{10,... | collective-permute-start | bytes 3145736 | tf_op jit(solution)/shard_map/ppermute | solution.py:289
  7.4 33.4 %copy-start.7 = (bf16[4096]{0:T(1024)(128)(2,1)S(1)}, bf16[4096]{0:T(1024)(128)(2,1)}, u32[]{:S(2)}) copy-start(bf16[4096]{0:T(1024)(128)(2,1)} %param.10) | copy-start | bytes 24580
  7.4 33.4 %copy-start.1 = (f32[2,512,2]{1,2,0:T(2,128)S(1)}, f32[2,512,2]{1,2,0:T(2,128)}, u32[]{:S(2)}) copy-start(f32[2,512,2]{1,2,0:T(2,128)} %param.13) | copy-start | bytes 24580
  7.4 33.4 %copy-start.2 = (f32[2,2]{1,0:T(2,128)S(1)}, f32[2,2]{1,0:T(2,128)}, u32[]{:S(2)}) copy-start(f32[2,2]{1,0:T(2,128)} %ng.1) | copy-start | bytes 52
  7.4 33.4 %copy-start.3 = (bf16[2,128]{1,0:T(2,128)(2,1)S(1)}, bf16[2,128]{1,0:T(2,128)(2,1)}, u32[]{:S(2)}) copy-start(bf16[2,128]{1,0:T(2,128)(2,1)} %q.1) | copy-start | bytes 1540
  7.5 33.4 %copy-start.4 = (bf16[2,128]{1,0:T(2,128)(2,1)S(1)}, bf16[2,128]{1,0:T(2,128)(2,1)}, u32[]{:S(2)}) copy-start(bf16[2,128]{1,0:T(2,128)(2,1)} %fk.1) | copy-start | bytes 1540
  7.5 33.4 %copy-start.5 = (bf16[2,128]{1,0:T(2,128)(2,1)S(1)}, bf16[2,128]{1,0:T(2,128)(2,1)}, u32[]{:S(2)}) copy-start(bf16[2,128]{1,0:T(2,128)(2,1)} %fv.1) | copy-start | bytes 1540
  7.7 33.4 %collective-permute-start.4 = (bf16[4096,256]{1,0:T(8,128)(2,1)S(1)}, bf16[4096,256]{1,0:T(8,128)(2,1)S(1)}, u32[]{:S(2)}, u32[]{:S(2)}) collective-permute-start(bf16[4096,256]{1,0:T(8,128)(2,1)S(1)} %constant_dynamic-update-slice_fusion.refs_3_.refs_2_.refs_6_), channel_id=1, source_target_pairs={{0,1},{1,0},{2,3},{3,2},{4,5},{5,4},{6,7},{7,6},{8,9},{9,8},{10,11... | collective-permute-start | bytes 6291464 | tf_op jit(solution)/shard_map/ppermute | solution.py:289
  16.9 17.3 %collective-permute-start.2 = (bf16[64,4096]{1,0:T(8,128)(2,1)S(1)}, bf16[64,4096]{1,0:T(8,128)(2,1)S(1)}, u32[]{:S(2)}, u32[]{:S(2)}) collective-permute-start(bf16[64,4096]{1,0:T(8,128)(2,1)S(1)} %get-tuple-element.22), channel_id=1, source_target_pairs={{0,6},{1,3},{2,0},{3,5},{4,2},{5,7},{6,4},{7,1},{8,14},{9,11},{10,... | collective-permute-start | bytes 1572872 | tf_op jit(solution)/shard_map/ppermute | solution.py:289
  18.9 23.7 %collective-permute-start.5 = (bf16[64,4096]{1,0:T(8,128)(2,1)S(1)}, bf16[64,4096]{1,0:T(8,128)(2,1)S(1)}, u32[]{:S(2)}, u32[]{:S(2)}) collective-permute-start(bf16[64,4096]{1,0:T(8,128)(2,1)S(1)} %get-tuple-element.33), channel_id=1, source_target_pairs={{0,6},{1,3},{2,0},{3,5},{4,2},{5,7},{6,4},{7,1},{8,14},{9,11},{10,... | collective-permute-start | bytes 1572872 | tf_op jit(solution)/shard_map/ppermute | solution.py:289
  34.3 15.8 %collective-permute-start.3 = (bf16[64,4096]{1,0:T(8,128)(2,1)S(1)}, bf16[64,4096]{1,0:T(8,128)(2,1)S(1)}, u32[]{:S(2)}, u32[]{:S(2)}) collective-permute-start(bf16[64,4096]{1,0:T(8,128)(2,1)S(1)} %collective-permute-done.2.refs_1_), channel_id=1, source_target_pairs={{0,6},{1,3},{2,0},{3,5},{4,2},{5,7},{6,4},{7,1},{8,14},{9,11},{10,... | collective-permute-start | bytes 1572872 | tf_op jit(solution)/shard_map/ppermute | solution.py:289
  36.2 13.8 %collective-permute-start.1 = (bf16[64,4096]{1,0:T(8,128)(2,1)S(1)}, bf16[64,4096]{1,0:T(8,128)(2,1)S(1)}, u32[]{:S(2)}, u32[]{:S(2)}) collective-permute-start(bf16[64,4096]{1,0:T(8,128)(2,1)S(1)} %slice_bitcast_fusion), channel_id=1, source_target_pairs={{0,2},{1,7},{2,4},{3,1},{4,6},{5,3},{6,0},{7,5},{8,10},{9,15},{10,... | collective-permute-start | bytes 1572872 | tf_op jit(solution)/shard_map/ppermute | solution.py:289
  45.3 9.5 %collective-permute-start.6 = (bf16[6,64,256]{2,1,0:T(8,128)(2,1)S(1)}, bf16[6,64,256]{2,1,0:T(8,128)(2,1)S(1)}, u32[]{:S(2)}, u32[]{:S(2)}) collective-permute-start(bf16[6,64,256]{2,1,0:T(8,128)(2,1)S(1)} %get-tuple-element.37), channel_id=1, source_target_pairs={{0,1},{1,0},{2,3},{3,2},{4,5},{5,4},{6,7},{7,6},{8,9},{9,8},{10,11... | collective-permute-start | bytes 589832 | tf_op jit(solution)/shard_map/ppermute | solution.py:289

commit v2 on v1

--- a/solution.py
+++ b/solution.py
@@ -11,6 +11,7 @@
 HD = 64
 EPS = 1e-06
 MASKED = -1e30
+CHUNKS = 4
 
 
 VMEM = pl.BlockSpec(memory_space=pltpu.VMEM)
@@ -60,6 +61,51 @@
         out[done:] = acc.astype(jnp.bfloat16).reshape(-1, half, out.shape[2])
 
 
+def finish_kernel(xa, xb, gain, wo, wp, own, par, n_s):
+    half, width = xa.shape
+    cols = wo.shape[1]
+    piece = width // CHUNKS
+    scales = []
+    for x in (xa, xb):
+        total = jnp.zeros((half, 128), jnp.float32)
+        for j in range(width // 128):
+            part = x[:, j * 128 : (j + 1) * 128].astype(jnp.float32)
+            total = total + part * part
+        mean = jnp.sum(total, axis=-1, keepdims=True) * (1.0 / width)
+        scales.append(lax.rsqrt(mean + EPS))
+    sums = [jnp.zeros((2 * half, cols), jnp.float32) for _ in range(2)]
+    for c in range(CHUNKS):
+        at = slice(c * piece, (c + 1) * piece)
+        factor = gain[:, at].astype(jnp.float32)
+        for k, x in enumerate((xa, xb)):
+            part = x[:, at].astype(jnp.float32) * scales[k] * factor
+            n_s[k * half : (k + 1) * half, at] = part.astype(jnp.bfloat16)
+        for k, w in enumerate((wo, wp)):
+            sums[k] = sums[k] + jnp.dot(
+                n_s[:, at], w[at, :], preferred_element_type=jnp.float32
+            )
+    for out, acc in zip((own, par), sums):
+        out[...] = acc.astype(jnp.bfloat16).reshape(out.shape)
+
+
+def finish(xa, xb, gain, wo, wp):
+    half, width = xa.shape
+    cols = wo.shape[1]
+    out = jax.ShapeDtypeStruct((2, half, cols), jnp.bfloat16)
+    return pl.pallas_call(
+        finish_kernel,
+        out_shape=(out, out),
+        in_specs=[VMEM] * 5,
+        out_specs=(VMEM, VMEM),
+        scratch_shapes=[pltpu.VMEM((2 * half, width), jnp.bfloat16)],
+        compiler_params=pltpu.CompilerParams(vmem_limit_bytes=16 * 1024 * 1024),
+        cost_estimate=pl.CostEstimate(
+            flops=8 * half * width * cols, bytes_accessed=6 * 1024 * 1024, transcendentals=0
+        ),
+        name="finish",
+    )(xa, xb, gain, wo, wp)
+
+
 def project(xs, gain, wo, wp, half, before=()):
     rows = sum(x.shape[0] for x in xs)
     width, cols = wo.shape
@@ -194,9 +240,10 @@
 def late_kernel(own, both, gates, qm, small, state, part):
     core = lax.rem(lax.axis_index("tp"), 2)
     found = halves(own, both.at[1 - core], LATE)
-    members, _, cols = part.shape
+    members, cols = part.shape[0], gates.shape[2]
     block = gates.shape[1]
-    low = lax.broadcasted_iota(jnp.int32, (1, cols), 1) % HD < HD // 2
+    packed = jnp.zeros((1, cols), jnp.float32)
+    quarter = lax.broadcasted_iota(jnp.int32, (1, cols), 1) % HD // (HD // 4)
     last = lax.axis_index("sp") == lax.axis_size("sp") - 1
     for p in range(2):
         scores, seen = scored(found, p, gates, qm)
@@ -215,15 +262,19 @@
         acc = jnp.sum(weights * seen, axis=0, keepdims=True)
         acc = acc + fresh_weight * small[2 + p : 3 + p, :]
         acc = acc + scale * state[4 * p + 2 : 4 * p + 3, :]
-        for r, row in ((p, jnp.where(low, top, total)), (p + 2, acc)):
-            part[:, r : r + 1, :] = jnp.broadcast_to(row[None], (members, 1, cols))
+        packed = jnp.where(quarter == 2 * p, top, packed)
+        packed = jnp.where(quarter == 2 * p + 1, total, packed)
+        part[:, :, p * cols : (p + 1) * cols] = jnp.broadcast_to(
+            acc[None], (members, 1, cols)
+        )
+    part[:, :, 2 * cols :] = jnp.broadcast_to(packed[None], (members, 1, cols))
 
 
 def late(own, both, gates, qm, small, state, members):
     cols = gates.shape[2]
     return pl.pallas_call(
         late_kernel,
-        out_shape=jax.ShapeDtypeStruct((members, 4, cols), jnp.float32),
+        out_shape=jax.ShapeDtypeStruct((members, 1, 3 * cols), jnp.float32),
         in_specs=[VMEM] * 6,
         out_specs=VMEM,
         compiler_params=pltpu.CompilerParams(vmem_limit_bytes=4 * 1024 * 1024),
@@ -237,15 +288,24 @@
 def merge_kernel(parts, own, both, k_in, v_in, keys, values, out, sem):
     core = lax.rem(lax.axis_index("tp"), 2)
     copies = stored(halves(own, both.at[1 - core], LATE), keys, values, sem)
-    members, _, cols = parts.shape
-    low = lax.broadcasted_iota(jnp.int32, (members, cols), 1) % HD < HD // 2
+    members, cols = parts.shape[0], out.shape[1]
+    packed = parts[:, 0, 2 * cols :]
+    quarter = lax.broadcasted_iota(jnp.int32, (members, cols), 1) % HD // (HD // 4)
+
+    def spread(which):
+        only = jnp.where(quarter == which, packed, 0.0)
+        found = only
+        for to in range(4):
+            if to != which:
+                found = found + pltpu.roll(only, (to - which) * (HD // 4) % cols, 1)
+        return found
+
     for p in range(2):
-        both_of = parts[:, p, :]
-        tops = jnp.where(low, both_of, pltpu.roll(both_of, HD // 2, 1))
-        totals = jnp.where(low, pltpu.roll(both_of, cols - HD // 2, 1), both_of)
+        tops = spread(2 * p)
         scale = jnp.exp(tops - jnp.max(tops, axis=0, keepdims=True))
-        total = jnp.sum(scale * totals, axis=0, keepdims=True)
-        acc = jnp.sum(scale * parts[:, p + 2, :], axis=0, keepdims=True)
+        total = jnp.sum(scale * spread(2 * p + 1), axis=0, keepdims=True)
+        acc = parts[:, 0, p * cols : (p + 1) * cols]
+        acc = jnp.sum(scale * acc, axis=0, keepdims=True)
         out[p : p + 1, :] = (acc / total).astype(jnp.bfloat16)
     for copy in copies:
         copy.wait()
@@ -255,7 +315,7 @@
     cache = jax.ShapeDtypeStruct(keys.shape, keys.dtype)
     return pl.pallas_call(
         merge_kernel,
-        out_shape=(cache, cache, jax.ShapeDtypeStruct((2, parts.shape[2]), jnp.bfloat16)),
+        out_shape=(cache, cache, jax.ShapeDtypeStruct((2, keys.shape[2]), jnp.bfloat16)),
         in_specs=[VMEM] * 3 + [ANY] * 2,
         out_specs=(ANY, ANY, VMEM),
         input_output_aliases={3: 0, 4: 1},
@@ -319,7 +379,7 @@
     own1, par1 = project((from_3.reshape(rows), b_1, a_1), gain, wo, wp, half, done)
     got1 = shift(par1, swap)
     keys, values, state = early(own1, got1, gates, qm)
-    own2, par2 = project((a_2, b_2), gain, wo, wp, half)
+    own2, par2 = finish(a_2, b_2, gain, wo, wp)
     pairs = [[i, i + 1] for i in range(0, tps, 2)]
     both2 = lax.all_gather(par2, "tp", axis_index_groups=pairs)
     part = late(own2, both2, gates, qm, small, state, members)

time: 70.6 us -> 70.1 us (level)
    pallas_call x3 -> x2, Pallas kernels: 5.51 us -> 4.09 us  [project(): pl.pallas_call(functools.partial(project_kernel, len(xs), bool(before)),...]
    pallas_call x1 -> x2, Pallas kernels: 0.24 us -> 1.2 us  [the longest x1 0.96 us: finish(): pl.pallas_call(finish_kernel, out_shape=(out, out), in_specs=[VMEM] * 5,...]
where the time goes in v2:
time: 70.1 us; the launch traced here: 69.7 us
  starting transfers between devices  26.7 us (38%)
  waiting for transfers between devices  16.3 us (23%)
  blocking collectives  15.9 us (23%)
  Pallas kernels  8.11 us (12%)
  local copies, waits for them, and re-layouts  1.75 us (2%)
  between operations  0.92 us (1%)
    ppermute x7, starting transfers between devices, shift(): return lax.ppermute(x, 'tp', by)  26.7 us
    ppermute x7, waiting for transfers between devices, shift(): return lax.ppermute(x, 'tp', by)  16.3 us
    all_to_all x1, blocking collectives, body(): parts = lax.all_to_all(part, 'sp', split_axis=0, concat_axis=0, tiled=True)  12.6 us
    pallas_call x2, Pallas kernels, project(): pl.pallas_call(functools.partial(project_kernel, len(xs), bool(before)),...  4.09 us
    all_gather x1, blocking collectives, body(): both2 = lax.all_gather(par2, 'tp', axis_index_groups=pairs)  3.35 us
    unnamed x17, local copies, waits for them, and re-layouts  1.45 us
  transfers between devices with their start and end apart: 7, of which 2 were waited for; matrix products, arithmetic and copies ran while one was open for 2% of the time, Pallas kernels for 8%

profile of v2, /device:TPU:1, one launch (start us, length us, event | category | flops | bytes accessed | tf_op | source)
XLA Modules:
  0.0 69.7 jit_solution(17917215230181759516)
XLA Ops:
  0.6 0.0 copy-start
  0.6 0.0 copy-start.6
  0.7 5.3 %collective-permute-start = (bf16[2,64,4096]{2,1,0:T(8,128)(2,1)}, bf16[2,64,4096]{2,1,0:T(8,128)(2,1)S(1)}, u32[]{:S(2)}, u32[]{:S(2)}) collective-permute-start(bf16[2,64,4096]{2,1,0:T(8,128)(2,1)} %tokens.1), channel_id=1, source_target_pairs={{0,2},{1,7},{2,4},{3,1},{4,6},{5,3},{6,0},{7,5},{8,10},{9,15},{10,... | collective-permute-start | bytes 3145736 | tf_op jit(solution)/shard_map/ppermute | solution.py:349
  6.0 1.4 %constant_dynamic-update-slice_fusion.1 = bf16[4096,256]{1,0:T(8,128)(2,1)S(1)} fusion(bf16[4096,128]{1,0:T(8,128)(2,1)} %param.11), kind=kLoop, calls=%fused_computation.2 | loop fusion | bytes 2097152
  7.4 0.0 copy-done.6
  7.4 0.0 copy-start.7
  7.4 0.0 copy-start.1
  7.4 0.0 copy-start.2
  7.4 0.0 copy-start.3
  7.5 0.0 copy-start.4
  7.5 0.0 copy-start.5
  7.5 0.2 constant_dynamic-update-slice_fusion.wo.refs_2_.refs_6_
  7.7 9.1 %collective-permute-start.4 = (bf16[4096,256]{1,0:T(8,128)(2,1)S(1)}, bf16[4096,256]{1,0:T(8,128)(2,1)S(1)}, u32[]{:S(2)}, u32[]{:S(2)}) collective-permute-start(bf16[4096,256]{1,0:T(8,128)(2,1)S(1)} %constant_dynamic-update-slice_fusion.wo.refs_2_.refs_6_), channel_id=1, source_target_pairs={{0,1},{1,0},{2,3},{3,2},{4,5},{5,4},{6,7},{7,6},{8,9},{9,8},{10,11... | collective-permute-start | bytes 6291464 | tf_op jit(solution)/shard_map/ppermute | solution.py:349
  16.9 0.0 copy-done
  16.9 0.1 split.1
  16.9 1.9 %collective-permute-start.2 = (bf16[64,4096]{1,0:T(8,128)(2,1)S(1)}, bf16[64,4096]{1,0:T(8,128)(2,1)S(1)}, u32[]{:S(2)}, u32[]{:S(2)}) collective-permute-start(bf16[64,4096]{1,0:T(8,128)(2,1)S(1)} %get-tuple-element.22), channel_id=1, source_target_pairs={{0,6},{1,3},{2,0},{3,5},{4,2},{5,7},{6,4},{7,1},{8,14},{9,11},{10,... | collective-permute-start | bytes 1572872 | tf_op jit(solution)/shard_map/ppermute | solution.py:349
  18.9 1.9 %collective-permute-start.5 = (bf16[64,4096]{1,0:T(8,128)(2,1)S(1)}, bf16[64,4096]{1,0:T(8,128)(2,1)S(1)}, u32[]{:S(2)}, u32[]{:S(2)}) collective-permute-start(bf16[64,4096]{1,0:T(8,128)(2,1)S(1)} %get-tuple-element.33), channel_id=1, source_target_pairs={{0,6},{1,3},{2,0},{3,5},{4,2},{5,7},{6,4},{7,1},{8,14},{9,11},{10,... | collective-permute-start | bytes 1572872 | tf_op jit(solution)/shard_map/ppermute | solution.py:349
  20.8 13.5 %collective-permute-done.2.refs_1_ = bf16[64,4096]{1,0:T(8,128)(2,1)S(1)} collective-permute-done((bf16[64,4096]{1,0:T(8,128)(2,1)S(1)}, bf16[64,4096]{1,0:T(8,128)(2,1)S(1)}, u32[]{:S(2)}, u32[]{:S(2)}) %collective-permute-start.2) | collective-permute-done | bytes 524320 | tf_op jit(solution)/shard_map/ppermute | solution.py:349
  34.3 1.9 %collective-permute-start.3 = (bf16[64,4096]{1,0:T(8,128)(2,1)S(1)}, bf16[64,4096]{1,0:T(8,128)(2,1)S(1)}, u32[]{:S(2)}, u32[]{:S(2)}) collective-permute-start(bf16[64,4096]{1,0:T(8,128)(2,1)S(1)} %collective-permute-done.2.refs_1_), channel_id=1, source_target_pairs={{0,6},{1,3},{2,0},{3,5},{4,2},{5,7},{6,4},{7,1},{8,14},{9,11},{10,... | collective-permute-start | bytes 1572872 | tf_op jit(solution)/shard_map/ppermute | solution.py:349
  36.2 0.0 collective-permute-done
  36.2 4.6 %collective-permute-start.1 = (bf16[64,4096]{1,0:T(8,128)(2,1)S(1)}, bf16[64,4096]{1,0:T(8,128)(2,1)S(1)}, u32[]{:S(2)}, u32[]{:S(2)}) collective-permute-start(bf16[64,4096]{1,0:T(8,128)(2,1)S(1)} %slice_bitcast_fusion), channel_id=1, source_target_pairs={{0,2},{1,7},{2,4},{3,1},{4,6},{5,3},{6,0},{7,5},{8,10},{9,15},{10,... | collective-permute-start | bytes 1572872 | tf_op jit(solution)/shard_map/ppermute | solution.py:349
  40.8 0.0 copy-done.7
  40.8 0.0 copy-done.1
  40.9 0.0 copy-done.2
  40.9 0.0 copy-done.3
  40.9 0.0 copy-done.4
  40.9 0.0 copy-done.5
  40.9 0.3 prepare.1
  41.2 0.0 collective-permute-done.4.wp.refs_3_.refs_7_
  41.2 1.4 %project.2 = (bf16[2,64,256]{2,1,0:T(8,128)(2,1)S(1)}, bf16[2,64,256]{2,1,0:T(8,128)(2,1)S(1)}) custom-call(bf16[128,4096]{1,0:T(8,128)(2,1)S(1)} %bitcast.6, bf16[1,4096]{1,0:T(2,128)(2,1)S(1)} %reshape.15.gain.refs_1_.refs_5_, bf16[4096,256]{1,0:T(8,128)(2,1)S(1)} %constant_dynamic-update-slice_fusion.wo.refs_2_.refs_6_, ...), custom_call_target="tpu_custom_call" | custom-call | flops 536870912 | bytes 6291456 | tf_op jit(solution)/shard_map/project/pallas_call | solution.py:114
  42.6 0.0 collective-permute-done.5.refs_2_
  42.6 2.7 %project.3 = (bf16[6,64,256]{2,1,0:T(8,128)(2,1)S(1)}, bf16[6,64,256]{2,1,0:T(8,128)(2,1)S(1)}) custom-call(bf16[128,4096]{1,0:T(8,128)(2,1)S(1)} %bitcast.7, bf16[64,4096]{1,0:T(8,128)(2,1)S(1)} %collective-permute-done.2.refs_1_, bf16[64,4096]{1,0:T(8,128)(2,1)S(1)} %collective-permute-done.5.refs_2_, bf16[2,64,256]{2,1,0:T(8,128)(2,1)S(1)} %get-tuple-element.34.refs_3_, ...), custom_call_target="tpu_custom_call" | custom-call | flops 1073741824 | bytes 6291456 | tf_op jit(solution)/shard_map/project/pallas_call | solution.py:114
  45.3 1.9 %collective-permute-start.6 = (bf16[6,64,256]{2,1,0:T(8,128)(2,1)S(1)}, bf16[6,64,256]{2,1,0:T(8,128)(2,1)S(1)}, u32[]{:S(2)}, u32[]{:S(2)}) collective-permute-start(bf16[6,64,256]{2,1,0:T(8,128)(2,1)S(1)} %get-tuple-element.37), channel_id=1, source_target_pairs={{0,1},{1,0},{2,3},{3,2},{4,5},{5,4},{6,7},{7,6},{8,9},{9,8},{10,11... | collective-permute-start | bytes 589832 | tf_op jit(solution)/shard_map/ppermute | solution.py:349
  47.2 2.8 %collective-permute-done.3.xb = bf16[64,4096]{1,0:T(8,128)(2,1)S(1)} collective-permute-done((bf16[64,4096]{1,0:T(8,128)(2,1)S(1)}, bf16[64,4096]{1,0:T(8,128)(2,1)S(1)}, u32[]{:S(2)}, u32[]{:S(2)}) %collective-permute-start.3) | collective-permute-done | bytes 524320 | tf_op jit(solution)/shard_map/ppermute | solution.py:349
  50.0 0.0 collective-permute-done.1.xa
  50.0 1.0 %finish.1 = (bf16[2,64,256]{2,1,0:T(8,128)(2,1)S(1)}, bf16[2,64,256]{2,1,0:T(8,128)(2,1)S(1)}) custom-call(bf16[64,4096]{1,0:T(8,128)(2,1)S(1)} %collective-permute-done.1.xa, bf16[64,4096]{1,0:T(8,128)(2,1)S(1)} %collective-permute-done.3.xb, bf16[1,4096]{1,0:T(2,128)(2,1)S(1)} %reshape.15.gain.refs_1_.refs_5_, ...), custom_call_target="tpu_custom_call" | custom-call | flops 536870912 | bytes 6291456 | tf_op jit(solution)/shard_map/finish/pallas_call | solution.py:95
  51.0 3.3 %all-gather = bf16[4,64,256]{2,1,0:T(8,128)(2,1)S(1)} all-gather(bf16[2,64,256]{2,1,0:T(8,128)(2,1)S(1)} %get-tuple-element.29), channel_id=2, replica_groups={{0,1},{2,3},{4,5},{6,7},{8,9},{10,11},{12,13},{14,15},{16,17},{18,19},{..., dimensions={0}, use_global_device_ids=true | all-gather | bytes 196608 | tf_op jit(solution)/shard_map/all_gather | solution.py:384
  54.4 0.0 collective-permute-done.6.got
  54.4 1.2 %early.1 = (bf16[2,512,128]{2,1,0:T(8,128)(2,1)}, bf16[2,512,128]{2,1,0:T(8,128)(2,1)}, f32[8,128]{1,0:T(8,128)S(1)}) custom-call(bf16[6,64,256]{2,1,0:T(8,128)(2,1)S(1)} %get-tuple-element.36.own, bf16[6,64,256]{2,1,0:T(8,128)(2,1)S(1)} %collective-permute-done.6.got, f32[2,512,128]{2,1,0:T(8,128)S(1)} %get-tuple-element.30.gates, ...), custom_call_target="tpu_custom_call" | custom-call | flops 67108864 | bytes 2097152 | tf_op jit(solution)/shard_map/early/pallas_call | solution.py:226
  55.6 0.2 late.1
  55.8 12.6 %all_to_all.5.parts = f32[32,1,384]{2,1,0:T(1,128)S(1)} all-to-all(f32[32,1,384]{2,1,0:T(1,128)S(1)} %late.1), channel_id=1, replica_groups=mesh['gr'=3,'sp'=32,'tp'=8] {'sp'}, dimensions={0} | all-to-all | bytes 98304 | tf_op jit(solution)/shard_map/all_to_all | solution.py:386
  68.4 1.3 %merge.1 = (bf16[2,512,128]{2,1,0:T(8,128)(2,1)}, bf16[2,512,128]{2,1,0:T(8,128)(2,1)}, bf16[2,128]{1,0:T(2,128)(2,1)}) custom-call(f32[32,1,384]{2,1,0:T(1,128)S(1)} %all_to_all.5.parts, bf16[2,64,256]{2,1,0:T(8,128)(2,1)S(1)} %get-tuple-element.28.own, bf16[2,2,64,256]{3,2,1,0:T(8,128)(2,1)S(1)} %bitcast.9, ...), custom_call_target="tpu_custom_call", output_to_operand_aliasing={{0}: (3, {}), {1}: (4, {})} | custom-call | tf_op jit(solution)/shard_map/merge/pallas_call | solution.py:316
  (2 shorter events, 0.0 us)
Async XLA Ops:
  0.6 16.2 %copy-start = (bf16[2,64,4096]{2,1,0:T(8,128)(2,1)S(1)}, bf16[2,64,4096]{2,1,0:T(8,128)(2,1)}, u32[]{:S(2)}) copy-start(bf16[2,64,4096]{2,1,0:T(8,128)(2,1)} %tokens.1) | copy-start | bytes 3145732
  0.6 6.8 %copy-start.6 = (bf16[4096,128]{1,0:T(8,128)(2,1)S(1)}, bf16[4096,128]{1,0:T(8,128)(2,1)}, u32[]{:S(2)}) copy-start(bf16[4096,128]{1,0:T(8,128)(2,1)} %param.12) | copy-start | bytes 3145732
  0.7 35.5 %collective-permute-start = (bf16[2,64,4096]{2,1,0:T(8,128)(2,1)}, bf16[2,64,4096]{2,1,0:T(8,128)(2,1)S(1)}, u32[]{:S(2)}, u32[]{:S(2)}) collective-permute-start(bf16[2,64,4096]{2,1,0:T(8,128)(2,1)} %tokens.1), channel_id=1, source_target_pairs={{0,2},{1,7},{2,4},{3,1},{4,6},{5,3},{6,0},{7,5},{8,10},{9,15},{10,... | collective-permute-start | bytes 3145736 | tf_op jit(solution)/shard_map/ppermute | solution.py:349
  7.4 33.4 %copy-start.7 = (bf16[4096]{0:T(1024)(128)(2,1)S(1)}, bf16[4096]{0:T(1024)(128)(2,1)}, u32[]{:S(2)}) copy-start(bf16[4096]{0:T(1024)(128)(2,1)} %param.10) | copy-start | bytes 24580
  7.4 33.4 %copy-start.1 = (f32[2,512,2]{1,2,0:T(2,128)S(1)}, f32[2,512,2]{1,2,0:T(2,128)}, u32[]{:S(2)}) copy-start(f32[2,512,2]{1,2,0:T(2,128)} %param.13) | copy-start | bytes 24580
  7.4 33.4 %copy-start.2 = (f32[2,2]{1,0:T(2,128)S(1)}, f32[2,2]{1,0:T(2,128)}, u32[]{:S(2)}) copy-start(f32[2,2]{1,0:T(2,128)} %ng.1) | copy-start | bytes 52
  7.4 33.4 %copy-start.3 = (bf16[2,128]{1,0:T(2,128)(2,1)S(1)}, bf16[2,128]{1,0:T(2,128)(2,1)}, u32[]{:S(2)}) copy-start(bf16[2,128]{1,0:T(2,128)(2,1)} %q.1) | copy-start | bytes 1540
  7.5 33.4 %copy-start.4 = (bf16[2,128]{1,0:T(2,128)(2,1)S(1)}, bf16[2,128]{1,0:T(2,128)(2,1)}, u32[]{:S(2)}) copy-start(bf16[2,128]{1,0:T(2,128)(2,1)} %fk.1) | copy-start | bytes 1540
  7.5 33.4 %copy-start.5 = (bf16[2,128]{1,0:T(2,128)(2,1)S(1)}, bf16[2,128]{1,0:T(2,128)(2,1)}, u32[]{:S(2)}) copy-start(bf16[2,128]{1,0:T(2,128)(2,1)} %fv.1) | copy-start | bytes 1540
  7.7 33.4 %collective-permute-start.4 = (bf16[4096,256]{1,0:T(8,128)(2,1)S(1)}, bf16[4096,256]{1,0:T(8,128)(2,1)S(1)}, u32[]{:S(2)}, u32[]{:S(2)}) collective-permute-start(bf16[4096,256]{1,0:T(8,128)(2,1)S(1)} %constant_dynamic-update-slice_fusion.wo.refs_2_.refs_6_), channel_id=1, source_target_pairs={{0,1},{1,0},{2,3},{3,2},{4,5},{5,4},{6,7},{7,6},{8,9},{9,8},{10,11... | collective-permute-start | bytes 6291464 | tf_op jit(solution)/shard_map/ppermute | solution.py:349
  16.9 17.3 %collective-permute-start.2 = (bf16[64,4096]{1,0:T(8,128)(2,1)S(1)}, bf16[64,4096]{1,0:T(8,128)(2,1)S(1)}, u32[]{:S(2)}, u32[]{:S(2)}) collective-permute-start(bf16[64,4096]{1,0:T(8,128)(2,1)S(1)} %get-tuple-element.22), channel_id=1, source_target_pairs={{0,6},{1,3},{2,0},{3,5},{4,2},{5,7},{6,4},{7,1},{8,14},{9,11},{10,... | collective-permute-start | bytes 1572872 | tf_op jit(solution)/shard_map/ppermute | solution.py:349
  18.9 23.7 %collective-permute-start.5 = (bf16[64,4096]{1,0:T(8,128)(2,1)S(1)}, bf16[64,4096]{1,0:T(8,128)(2,1)S(1)}, u32[]{:S(2)}, u32[]{:S(2)}) collective-permute-start(bf16[64,4096]{1,0:T(8,128)(2,1)S(1)} %get-tuple-element.33), channel_id=1, source_target_pairs={{0,6},{1,3},{2,0},{3,5},{4,2},{5,7},{6,4},{7,1},{8,14},{9,11},{10,... | collective-permute-start | bytes 1572872 | tf_op jit(solution)/shard_map/ppermute | solution.py:349
  34.3 15.8 %collective-permute-start.3 = (bf16[64,4096]{1,0:T(8,128)(2,1)S(1)}, bf16[64,4096]{1,0:T(8,128)(2,1)S(1)}, u32[]{:S(2)}, u32[]{:S(2)}) collective-permute-start(bf16[64,4096]{1,0:T(8,128)(2,1)S(1)} %collective-permute-done.2.refs_1_), channel_id=1, source_target_pairs={{0,6},{1,3},{2,0},{3,5},{4,2},{5,7},{6,4},{7,1},{8,14},{9,11},{10,... | collective-permute-start | bytes 1572872 | tf_op jit(solution)/shard_map/ppermute | solution.py:349
  36.2 13.8 %collective-permute-start.1 = (bf16[64,4096]{1,0:T(8,128)(2,1)S(1)}, bf16[64,4096]{1,0:T(8,128)(2,1)S(1)}, u32[]{:S(2)}, u32[]{:S(2)}) collective-permute-start(bf16[64,4096]{1,0:T(8,128)(2,1)S(1)} %slice_bitcast_fusion), channel_id=1, source_target_pairs={{0,2},{1,7},{2,4},{3,1},{4,6},{5,3},{6,0},{7,5},{8,10},{9,15},{10,... | collective-permute-start | bytes 1572872 | tf_op jit(solution)/shard_map/ppermute | solution.py:349
  45.3 9.1 %collective-permute-start.6 = (bf16[6,64,256]{2,1,0:T(8,128)(2,1)S(1)}, bf16[6,64,256]{2,1,0:T(8,128)(2,1)S(1)}, u32[]{:S(2)}, u32[]{:S(2)}) collective-permute-start(bf16[6,64,256]{2,1,0:T(8,128)(2,1)S(1)} %get-tuple-element.37), channel_id=1, source_target_pairs={{0,1},{1,0},{2,3},{3,2},{4,5},{5,4},{6,7},{7,6},{8,9},{9,8},{10,11... | collective-permute-start | bytes 589832 | tf_op jit(solution)/shard_map/ppermute | solution.py:349

commit v3 on v2

--- a/solution.py
+++ b/solution.py
@@ -189,8 +189,6 @@
                     ref.at[k, :, pl.ds(j * cols, cols)], cache.at[p, rows, :], sem.at[i, j]
                 )
             )
-    for copy in copies:
-        copy.start()
     return copies
 
 
@@ -208,6 +206,8 @@
 def early_kernel(own, got, gates, qm, keys, values, state, sem):
     found = halves(own, got, EARLY)
     copies = stored(found, keys, values, sem)
+    for copy in copies:
+        copy.start()
     for p in range(2):
         scores, seen = scored(found, p, gates, qm)
         top = jnp.max(scores, axis=0, keepdims=True)
@@ -237,9 +237,28 @@
     )(own, got, gates, qm)
 
 
-def late_kernel(own, both, gates, qm, small, state, part):
+def started(copies):
+    for copy in copies:
+        copy.start()
+
+
+def awaited(copies):
+    for copy in copies:
+        copy.wait()
+
+
+def at_turn(turn, act):
+    first = lax.axis_index("sp") < lax.axis_size("sp") // 2
+    pl.when(first if turn == 0 else jnp.logical_not(first))(act)
+
+
+def late_kernel(
+    own, both, gates, qm, small, state, k_in, v_in, keys, values, part, sem
+):
     core = lax.rem(lax.axis_index("tp"), 2)
     found = halves(own, both.at[1 - core], LATE)
+    copies = stored(found, keys, values, sem)
+    at_turn(0, lambda: started(copies))
     members, cols = part.shape[0], gates.shape[2]
     block = gates.shape[1]
     packed = jnp.zeros((1, cols), jnp.float32)
@@ -268,26 +287,35 @@
             acc[None], (members, 1, cols)
         )
     part[:, :, 2 * cols :] = jnp.broadcast_to(packed[None], (members, 1, cols))
-
-
-def late(own, both, gates, qm, small, state, members):
+    at_turn(0, lambda: awaited(copies))
+
+
+def late(own, both, gates, qm, small, state, keys, values, members):
     cols = gates.shape[2]
+    cache = jax.ShapeDtypeStruct(keys.shape, keys.dtype)
     return pl.pallas_call(
         late_kernel,
-        out_shape=jax.ShapeDtypeStruct((members, 1, 3 * cols), jnp.float32),
-        in_specs=[VMEM] * 6,
-        out_specs=VMEM,
+        out_shape=(
+            cache,
+            cache,
+            jax.ShapeDtypeStruct((members, 1, 3 * cols), jnp.float32),
+        ),
+        in_specs=[VMEM] * 6 + [ANY] * 2,
+        out_specs=(ANY, ANY, VMEM),
+        input_output_aliases={6: 0, 7: 1},
+        scratch_shapes=[pltpu.SemaphoreType.DMA((2 * len(LATE), 2))],
         compiler_params=pltpu.CompilerParams(vmem_limit_bytes=4 * 1024 * 1024),
         cost_estimate=pl.CostEstimate(
             flops=16 * 1024 * 1024, bytes_accessed=1024 * 1024, transcendentals=0
         ),
         name="late",
-    )(own, both, gates, qm, small, state)
+    )(own, both, gates, qm, small, state, keys, values)
 
 
 def merge_kernel(parts, own, both, k_in, v_in, keys, values, out, sem):
     core = lax.rem(lax.axis_index("tp"), 2)
     copies = stored(halves(own, both.at[1 - core], LATE), keys, values, sem)
+    at_turn(1, lambda: started(copies))
     members, cols = parts.shape[0], out.shape[1]
     packed = parts[:, 0, 2 * cols :]
     quarter = lax.broadcasted_iota(jnp.int32, (members, cols), 1) % HD // (HD // 4)
@@ -307,8 +335,7 @@
         acc = parts[:, 0, p * cols : (p + 1) * cols]
         acc = jnp.sum(scale * acc, axis=0, keepdims=True)
         out[p : p + 1, :] = (acc / total).astype(jnp.bfloat16)
-    for copy in copies:
-        copy.wait()
+    at_turn(1, lambda: awaited(copies))
 
 
 def merge(parts, own, both, keys, values):
@@ -382,7 +409,9 @@
     own2, par2 = finish(a_2, b_2, gain, wo, wp)
     pairs = [[i, i + 1] for i in range(0, tps, 2)]
     both2 = lax.all_gather(par2, "tp", axis_index_groups=pairs)
-    part = late(own2, both2, gates, qm, small, state, members)
+    keys, values, part = late(
+        own2, both2, gates, qm, small, state, keys, values, members
+    )
     parts = lax.all_to_all(part, "sp", split_axis=0, concat_axis=0, tiled=True)
     return merge(parts, own2, both2, keys, values)
 

time: 70.1 us -> 69.6 us (level)
  no operation moved by 1% of the time
where the time goes in v3:
time: 69.6 us; the launch traced here: 69.2 us
  starting transfers between devices  26.7 us (38%)
  waiting for transfers between devices  16.3 us (23%)
  blocking collectives  15.4 us (22%)
  Pallas kernels  8.17 us (12%)
  local copies, waits for them, and re-layouts  1.75 us (3%)
  between operations  0.92 us (1%)
    ppermute x7, starting transfers between devices, shift(): return lax.ppermute(x, 'tp', by)  26.7 us
    ppermute x7, waiting for transfers between devices, shift(): return lax.ppermute(x, 'tp', by)  16.3 us
    all_to_all x1, blocking collectives, body(): parts = lax.all_to_all(part, 'sp', split_axis=0, concat_axis=0, tiled=True)  12.1 us
    pallas_call x2, Pallas kernels, project(): pl.pallas_call(functools.partial(project_kernel, len(xs), bool(before)),...  4.09 us
    all_gather x1, blocking collectives, body(): both2 = lax.all_gather(par2, 'tp', axis_index_groups=pairs)  3.35 us
    unnamed x17, local copies, waits for them, and re-layouts  1.45 us
  transfers between devices with their start and end apart: 7, of which 2 were waited for; matrix products, arithmetic and copies ran while one was open for 2% of the time, Pallas kernels for 8%

profile of v3, /device:TPU:1, one launch (start us, length us, event | category | flops | bytes accessed | tf_op | source)
XLA Modules:
  0.0 69.2 jit_solution(12530894058683745557)
XLA Ops:
  0.6 0.0 copy-start
  0.6 0.0 copy-start.6
  0.7 5.3 %collective-permute-start = (bf16[2,64,4096]{2,1,0:T(8,128)(2,1)}, bf16[2,64,4096]{2,1,0:T(8,128)(2,1)S(1)}, u32[]{:S(2)}, u32[]{:S(2)}) collective-permute-start(bf16[2,64,4096]{2,1,0:T(8,128)(2,1)} %tokens.1), channel_id=1, source_target_pairs={{0,2},{1,7},{2,4},{3,1},{4,6},{5,3},{6,0},{7,5},{8,10},{9,15},{10,... | collective-permute-start | bytes 3145736 | tf_op jit(solution)/shard_map/ppermute | solution.py:376
  6.0 1.4 %constant_dynamic-update-slice_fusion.1 = bf16[4096,256]{1,0:T(8,128)(2,1)S(1)} fusion(bf16[4096,128]{1,0:T(8,128)(2,1)} %param.11), kind=kLoop, calls=%fused_computation.2 | loop fusion | bytes 2097152
  7.4 0.0 copy-done.6
  7.4 0.0 copy-start.7
  7.4 0.0 copy-start.1
  7.4 0.0 copy-start.2
  7.4 0.0 copy-start.3
  7.5 0.0 copy-start.4
  7.5 0.0 copy-start.5
  7.5 0.2 constant_dynamic-update-slice_fusion.wo.refs_2_.refs_6_
  7.7 9.1 %collective-permute-start.4 = (bf16[4096,256]{1,0:T(8,128)(2,1)S(1)}, bf16[4096,256]{1,0:T(8,128)(2,1)S(1)}, u32[]{:S(2)}, u32[]{:S(2)}) collective-permute-start(bf16[4096,256]{1,0:T(8,128)(2,1)S(1)} %constant_dynamic-update-slice_fusion.wo.refs_2_.refs_6_), channel_id=1, source_target_pairs={{0,1},{1,0},{2,3},{3,2},{4,5},{5,4},{6,7},{7,6},{8,9},{9,8},{10,11... | collective-permute-start | bytes 6291464 | tf_op jit(solution)/shard_map/ppermute | solution.py:376
  16.9 0.0 copy-done
  16.9 0.1 split.1
  16.9 1.9 %collective-permute-start.2 = (bf16[64,4096]{1,0:T(8,128)(2,1)S(1)}, bf16[64,4096]{1,0:T(8,128)(2,1)S(1)}, u32[]{:S(2)}, u32[]{:S(2)}) collective-permute-start(bf16[64,4096]{1,0:T(8,128)(2,1)S(1)} %get-tuple-element.25), channel_id=1, source_target_pairs={{0,6},{1,3},{2,0},{3,5},{4,2},{5,7},{6,4},{7,1},{8,14},{9,11},{10,... | collective-permute-start | bytes 1572872 | tf_op jit(solution)/shard_map/ppermute | solution.py:376
  18.9 1.9 %collective-permute-start.5 = (bf16[64,4096]{1,0:T(8,128)(2,1)S(1)}, bf16[64,4096]{1,0:T(8,128)(2,1)S(1)}, u32[]{:S(2)}, u32[]{:S(2)}) collective-permute-start(bf16[64,4096]{1,0:T(8,128)(2,1)S(1)} %get-tuple-element.36), channel_id=1, source_target_pairs={{0,6},{1,3},{2,0},{3,5},{4,2},{5,7},{6,4},{7,1},{8,14},{9,11},{10,... | collective-permute-start | bytes 1572872 | tf_op jit(solution)/shard_map/ppermute | solution.py:376
  20.8 13.5 %collective-permute-done.2.refs_1_ = bf16[64,4096]{1,0:T(8,128)(2,1)S(1)} collective-permute-done((bf16[64,4096]{1,0:T(8,128)(2,1)S(1)}, bf16[64,4096]{1,0:T(8,128)(2,1)S(1)}, u32[]{:S(2)}, u32[]{:S(2)}) %collective-permute-start.2) | collective-permute-done | bytes 524320 | tf_op jit(solution)/shard_map/ppermute | solution.py:376
  34.3 1.9 %collective-permute-start.3 = (bf16[64,4096]{1,0:T(8,128)(2,1)S(1)}, bf16[64,4096]{1,0:T(8,128)(2,1)S(1)}, u32[]{:S(2)}, u32[]{:S(2)}) collective-permute-start(bf16[64,4096]{1,0:T(8,128)(2,1)S(1)} %collective-permute-done.2.refs_1_), channel_id=1, source_target_pairs={{0,6},{1,3},{2,0},{3,5},{4,2},{5,7},{6,4},{7,1},{8,14},{9,11},{10,... | collective-permute-start | bytes 1572872 | tf_op jit(solution)/shard_map/ppermute | solution.py:376
  36.2 0.0 collective-permute-done
  36.2 4.6 %collective-permute-start.1 = (bf16[64,4096]{1,0:T(8,128)(2,1)S(1)}, bf16[64,4096]{1,0:T(8,128)(2,1)S(1)}, u32[]{:S(2)}, u32[]{:S(2)}) collective-permute-start(bf16[64,4096]{1,0:T(8,128)(2,1)S(1)} %slice_bitcast_fusion), channel_id=1, source_target_pairs={{0,2},{1,7},{2,4},{3,1},{4,6},{5,3},{6,0},{7,5},{8,10},{9,15},{10,... | collective-permute-start | bytes 1572872 | tf_op jit(solution)/shard_map/ppermute | solution.py:376
  40.8 0.0 copy-done.7
  40.8 0.0 copy-done.1
  40.9 0.0 copy-done.2
  40.9 0.0 copy-done.3
  40.9 0.0 copy-done.4
  40.9 0.0 copy-done.5
  40.9 0.3 prepare.1
  41.2 0.0 collective-permute-done.4.wp.refs_3_.refs_7_
  41.2 1.4 %project.2 = (bf16[2,64,256]{2,1,0:T(8,128)(2,1)S(1)}, bf16[2,64,256]{2,1,0:T(8,128)(2,1)S(1)}) custom-call(bf16[128,4096]{1,0:T(8,128)(2,1)S(1)} %bitcast.6, bf16[1,4096]{1,0:T(2,128)(2,1)S(1)} %reshape.15.gain.refs_1_.refs_5_, bf16[4096,256]{1,0:T(8,128)(2,1)S(1)} %constant_dynamic-update-slice_fusion.wo.refs_2_.refs_6_, ...), custom_call_target="tpu_custom_call" | custom-call | flops 536870912 | bytes 6291456 | tf_op jit(solution)/shard_map/project/pallas_call | solution.py:114
  42.6 0.0 collective-permute-done.5.refs_2_
  42.6 2.7 %project.3 = (bf16[6,64,256]{2,1,0:T(8,128)(2,1)S(1)}, bf16[6,64,256]{2,1,0:T(8,128)(2,1)S(1)}) custom-call(bf16[128,4096]{1,0:T(8,128)(2,1)S(1)} %bitcast.7, bf16[64,4096]{1,0:T(8,128)(2,1)S(1)} %collective-permute-done.2.refs_1_, bf16[64,4096]{1,0:T(8,128)(2,1)S(1)} %collective-permute-done.5.refs_2_, bf16[2,64,256]{2,1,0:T(8,128)(2,1)S(1)} %get-tuple-element.37.refs_3_, ...), custom_call_target="tpu_custom_call" | custom-call | flops 1073741824 | bytes 6291456 | tf_op jit(solution)/shard_map/project/pallas_call | solution.py:114
  45.3 1.9 %collective-permute-start.6 = (bf16[6,64,256]{2,1,0:T(8,128)(2,1)S(1)}, bf16[6,64,256]{2,1,0:T(8,128)(2,1)S(1)}, u32[]{:S(2)}, u32[]{:S(2)}) collective-permute-start(bf16[6,64,256]{2,1,0:T(8,128)(2,1)S(1)} %get-tuple-element.40), channel_id=1, source_target_pairs={{0,1},{1,0},{2,3},{3,2},{4,5},{5,4},{6,7},{7,6},{8,9},{9,8},{10,11... | collective-permute-start | bytes 589832 | tf_op jit(solution)/shard_map/ppermute | solution.py:376
  47.2 2.8 %collective-permute-done.3.xb = bf16[64,4096]{1,0:T(8,128)(2,1)S(1)} collective-permute-done((bf16[64,4096]{1,0:T(8,128)(2,1)S(1)}, bf16[64,4096]{1,0:T(8,128)(2,1)S(1)}, u32[]{:S(2)}, u32[]{:S(2)}) %collective-permute-start.3) | collective-permute-done | bytes 524320 | tf_op jit(solution)/shard_map/ppermute | solution.py:376
  50.0 0.0 collective-permute-done.1.xa
  50.0 1.0 %finish.1 = (bf16[2,64,256]{2,1,0:T(8,128)(2,1)S(1)}, bf16[2,64,256]{2,1,0:T(8,128)(2,1)S(1)}) custom-call(bf16[64,4096]{1,0:T(8,128)(2,1)S(1)} %collective-permute-done.1.xa, bf16[64,4096]{1,0:T(8,128)(2,1)S(1)} %collective-permute-done.3.xb, bf16[1,4096]{1,0:T(2,128)(2,1)S(1)} %reshape.15.gain.refs_1_.refs_5_, ...), custom_call_target="tpu_custom_call" | custom-call | flops 536870912 | bytes 6291456 | tf_op jit(solution)/shard_map/finish/pallas_call | solution.py:95
  51.0 3.3 %all-gather = bf16[4,64,256]{2,1,0:T(8,128)(2,1)S(1)} all-gather(bf16[2,64,256]{2,1,0:T(8,128)(2,1)S(1)} %get-tuple-element.32), channel_id=2, replica_groups={{0,1},{2,3},{4,5},{6,7},{8,9},{10,11},{12,13},{14,15},{16,17},{18,19},{..., dimensions={0}, use_global_device_ids=true | all-gather | bytes 196608 | tf_op jit(solution)/shard_map/all_gather | solution.py:411
  54.4 0.0 collective-permute-done.6.got
  54.4 1.2 %early.1 = (bf16[2,512,128]{2,1,0:T(8,128)(2,1)}, bf16[2,512,128]{2,1,0:T(8,128)(2,1)}, f32[8,128]{1,0:T(8,128)S(1)}) custom-call(bf16[6,64,256]{2,1,0:T(8,128)(2,1)S(1)} %get-tuple-element.39.own, bf16[6,64,256]{2,1,0:T(8,128)(2,1)S(1)} %collective-permute-done.6.got, f32[2,512,128]{2,1,0:T(8,128)S(1)} %get-tuple-element.33.gates, ...), custom_call_target="tpu_custom_call" | custom-call | flops 67108864 | bytes 2097152 | tf_op jit(solution)/shard_map/early/pallas_call | solution.py:226
  55.6 0.8 %late.1 = (bf16[2,512,128]{2,1,0:T(8,128)(2,1)}, bf16[2,512,128]{2,1,0:T(8,128)(2,1)}, f32[32,1,384]{2,1,0:T(1,128)S(1)}) custom-call(bf16[2,64,256]{2,1,0:T(8,128)(2,1)S(1)} %get-tuple-element.31.own, bf16[2,2,64,256]{3,2,1,0:T(8,128)(2,1)S(1)} %bitcast.8, ...), custom_call_target="tpu_custom_call", output_to_operand_aliasing={{0}: (6, {}), {1}: (7, {})} | custom-call | flops 16777216 | bytes 1048576 | tf_op jit(solution)/shard_map/late/pallas_call | solution.py:296
  56.4 12.1 %all_to_all.5.parts = f32[32,1,384]{2,1,0:T(1,128)S(1)} all-to-all(f32[32,1,384]{2,1,0:T(1,128)S(1)} %get-tuple-element.44), channel_id=1, replica_groups=mesh['gr'=3,'sp'=32,'tp'=8] {'sp'}, dimensions={0} | all-to-all | bytes 98304 | tf_op jit(solution)/shard_map/all_to_all | solution.py:415
  68.5 0.7 %merge.1 = (bf16[2,512,128]{2,1,0:T(8,128)(2,1)}, bf16[2,512,128]{2,1,0:T(8,128)(2,1)}, bf16[2,128]{1,0:T(2,128)(2,1)}) custom-call(f32[32,1,384]{2,1,0:T(1,128)S(1)} %all_to_all.5.parts, bf16[2,64,256]{2,1,0:T(8,128)(2,1)S(1)} %get-tuple-element.31.own, bf16[2,2,64,256]{3,2,1,0:T(8,128)(2,1)S(1)} %bitcast.9, ...), custom_call_target="tpu_custom_call", output_to_operand_aliasing={{0}: (3, {}), {1}: (4, {})} | custom-call | tf_op jit(solution)/shard_map/merge/pallas_call | solution.py:343
  (2 shorter events, 0.0 us)
Async XLA Ops:
  0.6 16.2 %copy-start = (bf16[2,64,4096]{2,1,0:T(8,128)(2,1)S(1)}, bf16[2,64,4096]{2,1,0:T(8,128)(2,1)}, u32[]{:S(2)}) copy-start(bf16[2,64,4096]{2,1,0:T(8,128)(2,1)} %tokens.1) | copy-start | bytes 3145732
  0.6 6.8 %copy-start.6 = (bf16[4096,128]{1,0:T(8,128)(2,1)S(1)}, bf16[4096,128]{1,0:T(8,128)(2,1)}, u32[]{:S(2)}) copy-start(bf16[4096,128]{1,0:T(8,128)(2,1)} %param.12) | copy-start | bytes 3145732
  0.7 35.5 %collective-permute-start = (bf16[2,64,4096]{2,1,0:T(8,128)(2,1)}, bf16[2,64,4096]{2,1,0:T(8,128)(2,1)S(1)}, u32[]{:S(2)}, u32[]{:S(2)}) collective-permute-start(bf16[2,64,4096]{2,1,0:T(8,128)(2,1)} %tokens.1), channel_id=1, source_target_pairs={{0,2},{1,7},{2,4},{3,1},{4,6},{5,3},{6,0},{7,5},{8,10},{9,15},{10,... | collective-permute-start | bytes 3145736 | tf_op jit(solution)/shard_map/ppermute | solution.py:376
  7.4 33.4 %copy-start.7 = (bf16[4096]{0:T(1024)(128)(2,1)S(1)}, bf16[4096]{0:T(1024)(128)(2,1)}, u32[]{:S(2)}) copy-start(bf16[4096]{0:T(1024)(128)(2,1)} %param.10) | copy-start | bytes 24580
  7.4 33.4 %copy-start.1 = (f32[2,512,2]{1,2,0:T(2,128)S(1)}, f32[2,512,2]{1,2,0:T(2,128)}, u32[]{:S(2)}) copy-start(f32[2,512,2]{1,2,0:T(2,128)} %param.13) | copy-start | bytes 24580
  7.4 33.4 %copy-start.2 = (f32[2,2]{1,0:T(2,128)S(1)}, f32[2,2]{1,0:T(2,128)}, u32[]{:S(2)}) copy-start(f32[2,2]{1,0:T(2,128)} %ng.1) | copy-start | bytes 52
  7.4 33.4 %copy-start.3 = (bf16[2,128]{1,0:T(2,128)(2,1)S(1)}, bf16[2,128]{1,0:T(2,128)(2,1)}, u32[]{:S(2)}) copy-start(bf16[2,128]{1,0:T(2,128)(2,1)} %q.1) | copy-start | bytes 1540
  7.5 33.4 %copy-start.4 = (bf16[2,128]{1,0:T(2,128)(2,1)S(1)}, bf16[2,128]{1,0:T(2,128)(2,1)}, u32[]{:S(2)}) copy-start(bf16[2,128]{1,0:T(2,128)(2,1)} %fk.1) | copy-start | bytes 1540
  7.5 33.4 %copy-start.5 = (bf16[2,128]{1,0:T(2,128)(2,1)S(1)}, bf16[2,128]{1,0:T(2,128)(2,1)}, u32[]{:S(2)}) copy-start(bf16[2,128]{1,0:T(2,128)(2,1)} %fv.1) | copy-start | bytes 1540
  7.7 33.4 %collective-permute-start.4 = (bf16[4096,256]{1,0:T(8,128)(2,1)S(1)}, bf16[4096,256]{1,0:T(8,128)(2,1)S(1)}, u32[]{:S(2)}, u32[]{:S(2)}) collective-permute-start(bf16[4096,256]{1,0:T(8,128)(2,1)S(1)} %constant_dynamic-update-slice_fusion.wo.refs_2_.refs_6_), channel_id=1, source_target_pairs={{0,1},{1,0},{2,3},{3,2},{4,5},{5,4},{6,7},{7,6},{8,9},{9,8},{10,11... | collective-permute-start | bytes 6291464 | tf_op jit(solution)/shard_map/ppermute | solution.py:376
  16.9 17.3 %collective-permute-start.2 = (bf16[64,4096]{1,0:T(8,128)(2,1)S(1)}, bf16[64,4096]{1,0:T(8,128)(2,1)S(1)}, u32[]{:S(2)}, u32[]{:S(2)}) collective-permute-start(bf16[64,4096]{1,0:T(8,128)(2,1)S(1)} %get-tuple-element.25), channel_id=1, source_target_pairs={{0,6},{1,3},{2,0},{3,5},{4,2},{5,7},{6,4},{7,1},{8,14},{9,11},{10,... | collective-permute-start | bytes 1572872 | tf_op jit(solution)/shard_map/ppermute | solution.py:376
  18.9 23.7 %collective-permute-start.5 = (bf16[64,4096]{1,0:T(8,128)(2,1)S(1)}, bf16[64,4096]{1,0:T(8,128)(2,1)S(1)}, u32[]{:S(2)}, u32[]{:S(2)}) collective-permute-start(bf16[64,4096]{1,0:T(8,128)(2,1)S(1)} %get-tuple-element.36), channel_id=1, source_target_pairs={{0,6},{1,3},{2,0},{3,5},{4,2},{5,7},{6,4},{7,1},{8,14},{9,11},{10,... | collective-permute-start | bytes 1572872 | tf_op jit(solution)/shard_map/ppermute | solution.py:376
  34.3 15.8 %collective-permute-start.3 = (bf16[64,4096]{1,0:T(8,128)(2,1)S(1)}, bf16[64,4096]{1,0:T(8,128)(2,1)S(1)}, u32[]{:S(2)}, u32[]{:S(2)}) collective-permute-start(bf16[64,4096]{1,0:T(8,128)(2,1)S(1)} %collective-permute-done.2.refs_1_), channel_id=1, source_target_pairs={{0,6},{1,3},{2,0},{3,5},{4,2},{5,7},{6,4},{7,1},{8,14},{9,11},{10,... | collective-permute-start | bytes 1572872 | tf_op jit(solution)/shard_map/ppermute | solution.py:376
  36.2 13.8 %collective-permute-start.1 = (bf16[64,4096]{1,0:T(8,128)(2,1)S(1)}, bf16[64,4096]{1,0:T(8,128)(2,1)S(1)}, u32[]{:S(2)}, u32[]{:S(2)}) collective-permute-start(bf16[64,4096]{1,0:T(8,128)(2,1)S(1)} %slice_bitcast_fusion), channel_id=1, source_target_pairs={{0,2},{1,7},{2,4},{3,1},{4,6},{5,3},{6,0},{7,5},{8,10},{9,15},{10,... | collective-permute-start | bytes 1572872 | tf_op jit(solution)/shard_map/ppermute | solution.py:376
  45.3 9.1 %collective-permute-start.6 = (bf16[6,64,256]{2,1,0:T(8,128)(2,1)S(1)}, bf16[6,64,256]{2,1,0:T(8,128)(2,1)S(1)}, u32[]{:S(2)}, u32[]{:S(2)}) collective-permute-start(bf16[6,64,256]{2,1,0:T(8,128)(2,1)S(1)} %get-tuple-element.40), channel_id=1, source_target_pairs={{0,1},{1,0},{2,3},{3,2},{4,5},{5,4},{6,7},{7,6},{8,9},{9,8},{10,11... | collective-permute-start | bytes 589832 | tf_op jit(solution)/shard_map/ppermute | solution.py:376

commit v4 on v3

--- a/solution.py
+++ b/solution.py
@@ -17,8 +17,8 @@
 VMEM = pl.BlockSpec(memory_space=pltpu.VMEM)
 ANY = pl.BlockSpec(memory_space=pl.ANY)
 
-EARLY = ((0, 0), (0, 1), (3, 0), (3, 1), (1, 1), (1, 0))
-LATE = ((2, 0), (2, 1))
+EARLY = ((0, 0), (0, 1), (3, 0), (3, 1), (1, 1))
+LATE = ((1, 0), (2, 0), (2, 1))
 
 
 def project_kernel(count, prior, *refs):
@@ -61,7 +61,7 @@
         out[done:] = acc.astype(jnp.bfloat16).reshape(-1, half, out.shape[2])
 
 
-def finish_kernel(xa, xb, gain, wo, wp, own, par, n_s):
+def finish_kernel(xa, xb, own_in, par_in, gain, wo, wp, own, par, n_s):
     half, width = xa.shape
     cols = wo.shape[1]
     piece = width // CHUNKS
@@ -84,18 +84,20 @@
             sums[k] = sums[k] + jnp.dot(
                 n_s[:, at], w[at, :], preferred_element_type=jnp.float32
             )
-    for out, acc in zip((own, par), sums):
-        out[...] = acc.astype(jnp.bfloat16).reshape(out.shape)
-
-
-def finish(xa, xb, gain, wo, wp):
+    done = own_in.shape[0]
+    for out, before, acc in zip((own, par), (own_in, par_in), sums):
+        out[:done] = before[...]
+        out[done:] = acc.astype(jnp.bfloat16).reshape(-1, half, cols)
+
+
+def finish(xa, xb, own, par, gain, wo, wp):
     half, width = xa.shape
     cols = wo.shape[1]
-    out = jax.ShapeDtypeStruct((2, half, cols), jnp.bfloat16)
+    out = jax.ShapeDtypeStruct((2 + own.shape[0], half, cols), jnp.bfloat16)
     return pl.pallas_call(
         finish_kernel,
         out_shape=(out, out),
-        in_specs=[VMEM] * 5,
+        in_specs=[VMEM] * 7,
         out_specs=(VMEM, VMEM),
         scratch_shapes=[pltpu.VMEM((2 * half, width), jnp.bfloat16)],
         compiler_params=pltpu.CompilerParams(vmem_limit_bytes=16 * 1024 * 1024),
@@ -103,7 +105,7 @@
             flops=8 * half * width * cols, bytes_accessed=6 * 1024 * 1024, transcendentals=0
         ),
         name="finish",
-    )(xa, xb, gain, wo, wp)
+    )(xa, xb, own, par, gain, wo, wp)
 
 
 def project(xs, gain, wo, wp, half, before=()):
@@ -391,7 +393,8 @@
     b_1 = shift(b_0, back)
     a_1 = shift(a_0, back)
     b_2 = shift(b_1, back)
-    a_2 = shift(from_3[0], ahead)
+    a_3 = from_3[0]
+    a_2 = shift(a_3, ahead)
     wo = jnp.concatenate([key_weight, value_weight], axis=1)
     wp = shift(wo, swap)
 
@@ -403,10 +406,13 @@
 
     rows = (2 * half, width)
     done = project((tokens.reshape(rows),), gain, wo, wp, half)
-    own1, par1 = project((from_3.reshape(rows), b_1, a_1), gain, wo, wp, half, done)
+    own1, par1 = project(
+        (from_3.reshape(rows), b_1), gain, wo, wp, half, done
+    )
     got1 = shift(par1, swap)
+    done = project((a_1,), gain, wo, wp, half)
     keys, values, state = early(own1, got1, gates, qm)
-    own2, par2 = finish(a_2, b_2, gain, wo, wp)
+    own2, par2 = finish(a_2, b_2, *done, gain, wo, wp)
     pairs = [[i, i + 1] for i in range(0, tps, 2)]
     both2 = lax.all_gather(par2, "tp", axis_index_groups=pairs)
     keys, values, part = late(

time: 69.6 us -> 69.8 us (level)
    pallas_call x2 -> x3, Pallas kernels: 4.09 us -> 4.66 us  [project(): pl.pallas_call(functools.partial(project_kernel, len(xs), bool(before)),...]
  transfers between devices with their start and end apart: 7 -> 7, of which waited for: 2 -> 2; matrix products, arithmetic and copies ran while one was open for 2% -> 2% of each run, Pallas kernels for 8% -> 9%
where the time goes in v4:
time: 69.8 us; the launch traced here: 69.4 us
  starting transfers between devices  26.7 us (38%)
  waiting for transfers between devices  15.7 us (22%)
  blocking collectives  15.6 us (22%)
  Pallas kernels  8.78 us (13%)
  local copies, waits for them, and re-layouts  1.75 us (3%)
  between operations  0.93 us (1%)
    ppermute x7, starting transfers between devices, shift(): return lax.ppermute(x, 'tp', by)  26.7 us
    ppermute x7, waiting for transfers between devices, shift(): return lax.ppermute(x, 'tp', by)  15.7 us
    all_to_all x1, blocking collectives, body(): parts = lax.all_to_all(part, 'sp', split_axis=0, concat_axis=0, tiled=True)  12.2 us
    pallas_call x3, Pallas kernels, project(): pl.pallas_call(functools.partial(project_kernel, len(xs), bool(before)),...  4.66 us
    all_gather x1, blocking collectives, body(): both2 = lax.all_gather(par2, 'tp', axis_index_groups=pairs)  3.39 us
    unnamed x17, local copies, waits for them, and re-layouts  1.45 us
  transfers between devices with their start and end apart: 7, of which 2 were waited for; matrix products, arithmetic and copies ran while one was open for 2% of the time, Pallas kernels for 9%

profile of v4, /device:TPU:1, one launch (start us, length us, event | category | flops | bytes accessed | tf_op | source)
XLA Modules:
  0.0 69.4 jit_solution(16964272797503524898)
XLA Ops:
  0.6 0.0 copy-start
  0.6 0.0 copy-start.6
  0.7 5.3 %collective-permute-start = (bf16[2,64,4096]{2,1,0:T(8,128)(2,1)}, bf16[2,64,4096]{2,1,0:T(8,128)(2,1)S(1)}, u32[]{:S(2)}, u32[]{:S(2)}) collective-permute-start(bf16[2,64,4096]{2,1,0:T(8,128)(2,1)} %tokens.1), channel_id=1, source_target_pairs={{0,2},{1,7},{2,4},{3,1},{4,6},{5,3},{6,0},{7,5},{8,10},{9,15},{10,... | collective-permute-start | bytes 3145736 | tf_op jit(solution)/shard_map/ppermute | solution.py:378
  6.0 1.4 %constant_dynamic-update-slice_fusion.1 = bf16[4096,256]{1,0:T(8,128)(2,1)S(1)} fusion(bf16[4096,128]{1,0:T(8,128)(2,1)} %param.11), kind=kLoop, calls=%fused_computation.2 | loop fusion | bytes 2097152
  7.4 0.0 copy-done.6
  7.4 0.0 copy-start.7
  7.4 0.0 copy-start.1
  7.4 0.0 copy-start.2
  7.4 0.0 copy-start.3
  7.5 0.0 copy-start.4
  7.5 0.0 copy-start.5
  7.5 0.2 constant_dynamic-update-slice_fusion.refs_2_.wo.refs_5_
  7.7 9.1 %collective-permute-start.5 = (bf16[4096,256]{1,0:T(8,128)(2,1)S(1)}, bf16[4096,256]{1,0:T(8,128)(2,1)S(1)}, u32[]{:S(2)}, u32[]{:S(2)}) collective-permute-start(bf16[4096,256]{1,0:T(8,128)(2,1)S(1)} %constant_dynamic-update-slice_fusion.refs_2_.wo.refs_5_), channel_id=1, source_target_pairs={{0,1},{1,0},{2,3},{3,2},{4,5},{5,4},{6,7},{7,6},{8,9},{9,8},{10,11... | collective-permute-start | bytes 6291464 | tf_op jit(solution)/shard_map/ppermute | solution.py:378
  16.9 0.0 copy-done
  16.9 0.1 split.1
  16.9 1.9 %collective-permute-start.2 = (bf16[64,4096]{1,0:T(8,128)(2,1)S(1)}, bf16[64,4096]{1,0:T(8,128)(2,1)S(1)}, u32[]{:S(2)}, u32[]{:S(2)}) collective-permute-start(bf16[64,4096]{1,0:T(8,128)(2,1)S(1)} %get-tuple-element.27), channel_id=1, source_target_pairs={{0,6},{1,3},{2,0},{3,5},{4,2},{5,7},{6,4},{7,1},{8,14},{9,11},{10,... | collective-permute-start | bytes 1572872 | tf_op jit(solution)/shard_map/ppermute | solution.py:378
  18.9 1.9 %collective-permute-start.4 = (bf16[64,4096]{1,0:T(8,128)(2,1)S(1)}, bf16[64,4096]{1,0:T(8,128)(2,1)S(1)}, u32[]{:S(2)}, u32[]{:S(2)}) collective-permute-start(bf16[64,4096]{1,0:T(8,128)(2,1)S(1)} %get-tuple-element.28), channel_id=1, source_target_pairs={{0,6},{1,3},{2,0},{3,5},{4,2},{5,7},{6,4},{7,1},{8,14},{9,11},{10,... | collective-permute-start | bytes 1572872 | tf_op jit(solution)/shard_map/ppermute | solution.py:378
  20.8 13.5 %collective-permute-done.2.refs_1_ = bf16[64,4096]{1,0:T(8,128)(2,1)S(1)} collective-permute-done((bf16[64,4096]{1,0:T(8,128)(2,1)S(1)}, bf16[64,4096]{1,0:T(8,128)(2,1)S(1)}, u32[]{:S(2)}, u32[]{:S(2)}) %collective-permute-start.2) | collective-permute-done | bytes 524320 | tf_op jit(solution)/shard_map/ppermute | solution.py:378
  34.3 1.9 %collective-permute-start.3 = (bf16[64,4096]{1,0:T(8,128)(2,1)S(1)}, bf16[64,4096]{1,0:T(8,128)(2,1)S(1)}, u32[]{:S(2)}, u32[]{:S(2)}) collective-permute-start(bf16[64,4096]{1,0:T(8,128)(2,1)S(1)} %collective-permute-done.2.refs_1_), channel_id=1, source_target_pairs={{0,6},{1,3},{2,0},{3,5},{4,2},{5,7},{6,4},{7,1},{8,14},{9,11},{10,... | collective-permute-start | bytes 1572872 | tf_op jit(solution)/shard_map/ppermute | solution.py:378
  36.2 0.0 collective-permute-done
  36.2 4.6 %collective-permute-start.1 = (bf16[64,4096]{1,0:T(8,128)(2,1)S(1)}, bf16[64,4096]{1,0:T(8,128)(2,1)S(1)}, u32[]{:S(2)}, u32[]{:S(2)}) collective-permute-start(bf16[64,4096]{1,0:T(8,128)(2,1)S(1)} %slice_bitcast_fusion), channel_id=1, source_target_pairs={{0,2},{1,7},{2,4},{3,1},{4,6},{5,3},{6,0},{7,5},{8,10},{9,15},{10,... | collective-permute-start | bytes 1572872 | tf_op jit(solution)/shard_map/ppermute | solution.py:378
  40.8 0.0 copy-done.7
  40.8 0.0 copy-done.1
  40.9 0.0 copy-done.2
  40.9 0.0 copy-done.3
  40.9 0.0 copy-done.4
  40.9 0.0 copy-done.5
  40.9 0.3 prepare.1
  41.2 0.0 collective-permute-done.5.refs_3_.wp.refs_6_
  41.2 1.4 %project.4 = (bf16[2,64,256]{2,1,0:T(8,128)(2,1)S(1)}, bf16[2,64,256]{2,1,0:T(8,128)(2,1)S(1)}) custom-call(bf16[128,4096]{1,0:T(8,128)(2,1)S(1)} %bitcast.6, bf16[1,4096]{1,0:T(2,128)(2,1)S(1)} %reshape.15.refs_1_.gain.refs_4_, bf16[4096,256]{1,0:T(8,128)(2,1)S(1)} %constant_dynamic-update-slice_fusion.refs_2_.wo.refs_5_, ...), custom_call_target="tpu_custom_call" | custom-call | flops 536870912 | bytes 6291456 | tf_op jit(solution)/shard_map/project/pallas_call | solution.py:116
  42.6 2.0 %project.5 = (bf16[5,64,256]{2,1,0:T(8,128)(2,1)S(1)}, bf16[5,64,256]{2,1,0:T(8,128)(2,1)S(1)}) custom-call(bf16[128,4096]{1,0:T(8,128)(2,1)S(1)} %bitcast.7, bf16[64,4096]{1,0:T(8,128)(2,1)S(1)} %collective-permute-done.2.refs_1_, bf16[2,64,256]{2,1,0:T(8,128)(2,1)S(1)} %get-tuple-element.41.refs_2_, bf16[2,64,256]{2,1,0:T(8,128)(2,1)S(1)} %get-tuple-element.42.refs_3_, ...), custom_call_target="tpu_custom_call" | custom-call | flops 805306368 | bytes 6291456 | tf_op jit(solution)/shard_map/project/pallas_call | solution.py:116
  44.7 1.9 %collective-permute-start.6 = (bf16[5,64,256]{2,1,0:T(8,128)(2,1)S(1)}, bf16[5,64,256]{2,1,0:T(8,128)(2,1)S(1)}, u32[]{:S(2)}, u32[]{:S(2)}) collective-permute-start(bf16[5,64,256]{2,1,0:T(8,128)(2,1)S(1)} %get-tuple-element.44), channel_id=1, source_target_pairs={{0,1},{1,0},{2,3},{3,2},{4,5},{5,4},{6,7},{7,6},{8,9},{9,8},{10,11... | collective-permute-start | bytes 491528 | tf_op jit(solution)/shard_map/ppermute | solution.py:378
  46.6 0.0 collective-permute-done.4.refs_0_
  46.6 1.2 %project.3 = (bf16[1,64,256]{2,1,0:T(8,128)(2,1)S(1)}, bf16[1,64,256]{2,1,0:T(8,128)(2,1)S(1)}) custom-call(bf16[64,4096]{1,0:T(8,128)(2,1)S(1)} %collective-permute-done.4.refs_0_, bf16[1,4096]{1,0:T(2,128)(2,1)S(1)} %reshape.15.refs_1_.gain.refs_4_, bf16[4096,256]{1,0:T(8,128)(2,1)S(1)} %constant_dynamic-update-slice_fusion.refs_2_.wo.refs_5_, ...), custom_call_target="tpu_custom_call" | custom-call | flops 268435456 | bytes 6291456 | tf_op jit(solution)/shard_map/project/pallas_call | solution.py:116
  47.8 2.2 %collective-permute-done.3.xb = bf16[64,4096]{1,0:T(8,128)(2,1)S(1)} collective-permute-done((bf16[64,4096]{1,0:T(8,128)(2,1)S(1)}, bf16[64,4096]{1,0:T(8,128)(2,1)S(1)}, u32[]{:S(2)}, u32[]{:S(2)}) %collective-permute-start.3) | collective-permute-done | bytes 524320 | tf_op jit(solution)/shard_map/ppermute | solution.py:378
  50.0 0.0 collective-permute-done.1.xa
  50.0 1.0 %finish.1 = (bf16[3,64,256]{2,1,0:T(8,128)(2,1)S(1)}, bf16[3,64,256]{2,1,0:T(8,128)(2,1)S(1)}) custom-call(bf16[64,4096]{1,0:T(8,128)(2,1)S(1)} %collective-permute-done.1.xa, bf16[64,4096]{1,0:T(8,128)(2,1)S(1)} %collective-permute-done.3.xb, bf16[1,64,256]{2,1,0:T(8,128)(2,1)S(1)} %get-tuple-element.34.own_in, ...), custom_call_target="tpu_custom_call" | custom-call | flops 536870912 | bytes 6291456 | tf_op jit(solution)/shard_map/finish/pallas_call | solution.py:97
  51.0 3.4 %all-gather = bf16[6,64,256]{2,1,0:T(8,128)(2,1)S(1)} all-gather(bf16[3,64,256]{2,1,0:T(8,128)(2,1)S(1)} %get-tuple-element.37), channel_id=2, replica_groups={{0,1},{2,3},{4,5},{6,7},{8,9},{10,11},{12,13},{14,15},{16,17},{18,19},{..., dimensions={0}, use_global_device_ids=true | all-gather | bytes 294912 | tf_op jit(solution)/shard_map/all_gather | solution.py:417
  54.4 0.0 collective-permute-done.6.got
  54.4 1.1 %early.1 = (bf16[2,512,128]{2,1,0:T(8,128)(2,1)}, bf16[2,512,128]{2,1,0:T(8,128)(2,1)}, f32[8,128]{1,0:T(8,128)S(1)}) custom-call(bf16[5,64,256]{2,1,0:T(8,128)(2,1)S(1)} %get-tuple-element.43.own, bf16[5,64,256]{2,1,0:T(8,128)(2,1)S(1)} %collective-permute-done.6.got, f32[2,512,128]{2,1,0:T(8,128)S(1)} %get-tuple-element.38.gates, ...), custom_call_target="tpu_custom_call" | custom-call | flops 67108864 | bytes 2097152 | tf_op jit(solution)/shard_map/early/pallas_call | solution.py:228
  55.5 1.0 %late.1 = (bf16[2,512,128]{2,1,0:T(8,128)(2,1)}, bf16[2,512,128]{2,1,0:T(8,128)(2,1)}, f32[32,1,384]{2,1,0:T(1,128)S(1)}) custom-call(bf16[3,64,256]{2,1,0:T(8,128)(2,1)S(1)} %get-tuple-element.36.own, bf16[2,3,64,256]{3,2,1,0:T(8,128)(2,1)S(1)} %bitcast.8, ...), custom_call_target="tpu_custom_call", output_to_operand_aliasing={{0}: (6, {}), {1}: (7, {})} | custom-call | flops 16777216 | bytes 1048576 | tf_op jit(solution)/shard_map/late/pallas_call | solution.py:298
  56.5 12.2 %all_to_all.5.parts = f32[32,1,384]{2,1,0:T(1,128)S(1)} all-to-all(f32[32,1,384]{2,1,0:T(1,128)S(1)} %get-tuple-element.48), channel_id=1, replica_groups=mesh['gr'=3,'sp'=32,'tp'=8] {'sp'}, dimensions={0} | all-to-all | bytes 98304 | tf_op jit(solution)/shard_map/all_to_all | solution.py:421
  68.6 0.8 %merge.1 = (bf16[2,512,128]{2,1,0:T(8,128)(2,1)}, bf16[2,512,128]{2,1,0:T(8,128)(2,1)}, bf16[2,128]{1,0:T(2,128)(2,1)}) custom-call(f32[32,1,384]{2,1,0:T(1,128)S(1)} %all_to_all.5.parts, bf16[3,64,256]{2,1,0:T(8,128)(2,1)S(1)} %get-tuple-element.36.own, bf16[2,3,64,256]{3,2,1,0:T(8,128)(2,1)S(1)} %bitcast.9, ...), custom_call_target="tpu_custom_call", output_to_operand_aliasing={{0}: (3, {}), {1}: (4, {})} | custom-call | tf_op jit(solution)/shard_map/merge/pallas_call | solution.py:345
  (2 shorter events, 0.0 us)
Async XLA Ops:
  0.6 16.2 %copy-start = (bf16[2,64,4096]{2,1,0:T(8,128)(2,1)S(1)}, bf16[2,64,4096]{2,1,0:T(8,128)(2,1)}, u32[]{:S(2)}) copy-start(bf16[2,64,4096]{2,1,0:T(8,128)(2,1)} %tokens.1) | copy-start | bytes 3145732
  0.6 6.8 %copy-start.6 = (bf16[4096,128]{1,0:T(8,128)(2,1)S(1)}, bf16[4096,128]{1,0:T(8,128)(2,1)}, u32[]{:S(2)}) copy-start(bf16[4096,128]{1,0:T(8,128)(2,1)} %param.12) | copy-start | bytes 3145732
  0.7 35.5 %collective-permute-start = (bf16[2,64,4096]{2,1,0:T(8,128)(2,1)}, bf16[2,64,4096]{2,1,0:T(8,128)(2,1)S(1)}, u32[]{:S(2)}, u32[]{:S(2)}) collective-permute-start(bf16[2,64,4096]{2,1,0:T(8,128)(2,1)} %tokens.1), channel_id=1, source_target_pairs={{0,2},{1,7},{2,4},{3,1},{4,6},{5,3},{6,0},{7,5},{8,10},{9,15},{10,... | collective-permute-start | bytes 3145736 | tf_op jit(solution)/shard_map/ppermute | solution.py:378
  7.4 33.4 %copy-start.7 = (bf16[4096]{0:T(1024)(128)(2,1)S(1)}, bf16[4096]{0:T(1024)(128)(2,1)}, u32[]{:S(2)}) copy-start(bf16[4096]{0:T(1024)(128)(2,1)} %param.10) | copy-start | bytes 24580
  7.4 33.4 %copy-start.1 = (f32[2,512,2]{1,2,0:T(2,128)S(1)}, f32[2,512,2]{1,2,0:T(2,128)}, u32[]{:S(2)}) copy-start(f32[2,512,2]{1,2,0:T(2,128)} %param.13) | copy-start | bytes 24580
  7.4 33.4 %copy-start.2 = (f32[2,2]{1,0:T(2,128)S(1)}, f32[2,2]{1,0:T(2,128)}, u32[]{:S(2)}) copy-start(f32[2,2]{1,0:T(2,128)} %ng.1) | copy-start | bytes 52
  7.4 33.4 %copy-start.3 = (bf16[2,128]{1,0:T(2,128)(2,1)S(1)}, bf16[2,128]{1,0:T(2,128)(2,1)}, u32[]{:S(2)}) copy-start(bf16[2,128]{1,0:T(2,128)(2,1)} %q.1) | copy-start | bytes 1540
  7.5 33.4 %copy-start.4 = (bf16[2,128]{1,0:T(2,128)(2,1)S(1)}, bf16[2,128]{1,0:T(2,128)(2,1)}, u32[]{:S(2)}) copy-start(bf16[2,128]{1,0:T(2,128)(2,1)} %fk.1) | copy-start | bytes 1540
  7.5 33.4 %copy-start.5 = (bf16[2,128]{1,0:T(2,128)(2,1)S(1)}, bf16[2,128]{1,0:T(2,128)(2,1)}, u32[]{:S(2)}) copy-start(bf16[2,128]{1,0:T(2,128)(2,1)} %fv.1) | copy-start | bytes 1540
  7.7 33.4 %collective-permute-start.5 = (bf16[4096,256]{1,0:T(8,128)(2,1)S(1)}, bf16[4096,256]{1,0:T(8,128)(2,1)S(1)}, u32[]{:S(2)}, u32[]{:S(2)}) collective-permute-start(bf16[4096,256]{1,0:T(8,128)(2,1)S(1)} %constant_dynamic-update-slice_fusion.refs_2_.wo.refs_5_), channel_id=1, source_target_pairs={{0,1},{1,0},{2,3},{3,2},{4,5},{5,4},{6,7},{7,6},{8,9},{9,8},{10,11... | collective-permute-start | bytes 6291464 | tf_op jit(solution)/shard_map/ppermute | solution.py:378
  16.9 17.3 %collective-permute-start.2 = (bf16[64,4096]{1,0:T(8,128)(2,1)S(1)}, bf16[64,4096]{1,0:T(8,128)(2,1)S(1)}, u32[]{:S(2)}, u32[]{:S(2)}) collective-permute-start(bf16[64,4096]{1,0:T(8,128)(2,1)S(1)} %get-tuple-element.27), channel_id=1, source_target_pairs={{0,6},{1,3},{2,0},{3,5},{4,2},{5,7},{6,4},{7,1},{8,14},{9,11},{10,... | collective-permute-start | bytes 1572872 | tf_op jit(solution)/shard_map/ppermute | solution.py:378
  18.9 27.7 %collective-permute-start.4 = (bf16[64,4096]{1,0:T(8,128)(2,1)S(1)}, bf16[64,4096]{1,0:T(8,128)(2,1)S(1)}, u32[]{:S(2)}, u32[]{:S(2)}) collective-permute-start(bf16[64,4096]{1,0:T(8,128)(2,1)S(1)} %get-tuple-element.28), channel_id=1, source_target_pairs={{0,6},{1,3},{2,0},{3,5},{4,2},{5,7},{6,4},{7,1},{8,14},{9,11},{10,... | collective-permute-start | bytes 1572872 | tf_op jit(solution)/shard_map/ppermute | solution.py:378
  34.3 15.8 %collective-permute-start.3 = (bf16[64,4096]{1,0:T(8,128)(2,1)S(1)}, bf16[64,4096]{1,0:T(8,128)(2,1)S(1)}, u32[]{:S(2)}, u32[]{:S(2)}) collective-permute-start(bf16[64,4096]{1,0:T(8,128)(2,1)S(1)} %collective-permute-done.2.refs_1_), channel_id=1, source_target_pairs={{0,6},{1,3},{2,0},{3,5},{4,2},{5,7},{6,4},{7,1},{8,14},{9,11},{10,... | collective-permute-start | bytes 1572872 | tf_op jit(solution)/shard_map/ppermute | solution.py:378
  36.2 13.8 %collective-permute-start.1 = (bf16[64,4096]{1,0:T(8,128)(2,1)S(1)}, bf16[64,4096]{1,0:T(8,128)(2,1)S(1)}, u32[]{:S(2)}, u32[]{:S(2)}) collective-permute-start(bf16[64,4096]{1,0:T(8,128)(2,1)S(1)} %slice_bitcast_fusion), channel_id=1, source_target_pairs={{0,2},{1,7},{2,4},{3,1},{4,6},{5,3},{6,0},{7,5},{8,10},{9,15},{10,... | collective-permute-start | bytes 1572872 | tf_op jit(solution)/shard_map/ppermute | solution.py:378
  44.7 9.7 %collective-permute-start.6 = (bf16[5,64,256]{2,1,0:T(8,128)(2,1)S(1)}, bf16[5,64,256]{2,1,0:T(8,128)(2,1)S(1)}, u32[]{:S(2)}, u32[]{:S(2)}) collective-permute-start(bf16[5,64,256]{2,1,0:T(8,128)(2,1)S(1)} %get-tuple-element.44), channel_id=1, source_target_pairs={{0,1},{1,0},{2,3},{3,2},{4,5},{5,4},{6,7},{7,6},{8,9},{9,8},{10,11... | collective-permute-start | bytes 491528 | tf_op jit(solution)/shard_map/ppermute | solution.py:378

commit v5 on v4

--- a/solution.py
+++ b/solution.py
@@ -11,14 +11,14 @@
 HD = 64
 EPS = 1e-06
 MASKED = -1e30
-CHUNKS = 4
+CHUNKS = 16
 
 
 VMEM = pl.BlockSpec(memory_space=pltpu.VMEM)
 ANY = pl.BlockSpec(memory_space=pl.ANY)
 
-EARLY = ((0, 0), (0, 1), (3, 0), (3, 1), (1, 1))
-LATE = ((1, 0), (2, 0), (2, 1))
+EARLY = ((0, 0), (0, 1), (1, 1), (3, 0), (3, 1))
+LATE = ((1, 0), (2, 1), (2, 0))
 
 
 def project_kernel(count, prior, *refs):
@@ -61,23 +61,24 @@
         out[done:] = acc.astype(jnp.bfloat16).reshape(-1, half, out.shape[2])
 
 
-def finish_kernel(xa, xb, own_in, par_in, gain, wo, wp, own, par, n_s):
-    half, width = xa.shape
+def finish_kernel(count, *refs):
+    xs, (own_in, par_in, gain, wo, wp, own, par, n_s) = refs[:count], refs[count:]
+    half, width = xs[0].shape
     cols = wo.shape[1]
     piece = width // CHUNKS
     scales = []
-    for x in (xa, xb):
+    for x in xs:
         total = jnp.zeros((half, 128), jnp.float32)
         for j in range(width // 128):
             part = x[:, j * 128 : (j + 1) * 128].astype(jnp.float32)
             total = total + part * part
         mean = jnp.sum(total, axis=-1, keepdims=True) * (1.0 / width)
         scales.append(lax.rsqrt(mean + EPS))
-    sums = [jnp.zeros((2 * half, cols), jnp.float32) for _ in range(2)]
+    sums = [jnp.zeros((count * half, cols), jnp.float32) for _ in range(2)]
     for c in range(CHUNKS):
         at = slice(c * piece, (c + 1) * piece)
         factor = gain[:, at].astype(jnp.float32)
-        for k, x in enumerate((xa, xb)):
+        for k, x in enumerate(xs):
             part = x[:, at].astype(jnp.float32) * scales[k] * factor
             n_s[k * half : (k + 1) * half, at] = part.astype(jnp.bfloat16)
         for k, w in enumerate((wo, wp)):
@@ -87,25 +88,27 @@
     done = own_in.shape[0]
     for out, before, acc in zip((own, par), (own_in, par_in), sums):
         out[:done] = before[...]
-        out[done:] = acc.astype(jnp.bfloat16).reshape(-1, half, cols)
-
-
-def finish(xa, xb, own, par, gain, wo, wp):
-    half, width = xa.shape
+        out[done:] = acc.astype(jnp.bfloat16).reshape(count, half, cols)
+
+
+def finish(xs, own, par, gain, wo, wp):
+    count, (half, width) = len(xs), xs[0].shape
     cols = wo.shape[1]
-    out = jax.ShapeDtypeStruct((2 + own.shape[0], half, cols), jnp.bfloat16)
-    return pl.pallas_call(
-        finish_kernel,
+    out = jax.ShapeDtypeStruct((count + own.shape[0], half, cols), jnp.bfloat16)
+    return pl.pallas_call(
+        functools.partial(finish_kernel, count),
         out_shape=(out, out),
-        in_specs=[VMEM] * 7,
+        in_specs=[VMEM] * (count + 5),
         out_specs=(VMEM, VMEM),
-        scratch_shapes=[pltpu.VMEM((2 * half, width), jnp.bfloat16)],
+        scratch_shapes=[pltpu.VMEM((count * half, width), jnp.bfloat16)],
         compiler_params=pltpu.CompilerParams(vmem_limit_bytes=16 * 1024 * 1024),
         cost_estimate=pl.CostEstimate(
-            flops=8 * half * width * cols, bytes_accessed=6 * 1024 * 1024, transcendentals=0
+            flops=4 * count * half * width * cols,
+            bytes_accessed=6 * 1024 * 1024,
+            transcendentals=0,
         ),
         name="finish",
-    )(xa, xb, own, par, gain, wo, wp)
+    )(*xs, own, par, gain, wo, wp)
 
 
 def project(xs, gain, wo, wp, half, before=()):
@@ -405,14 +408,14 @@
     gates, qm, small = made
 
     rows = (2 * half, width)
-    done = project((tokens.reshape(rows),), gain, wo, wp, half)
+    done = project((tokens.reshape(rows), b_1), gain, wo, wp, half)
     own1, par1 = project(
-        (from_3.reshape(rows), b_1), gain, wo, wp, half, done
+        (from_3.reshape(rows),), gain, wo, wp, half, done
     )
     got1 = shift(par1, swap)
-    done = project((a_1,), gain, wo, wp, half)
+    done = project((a_1, b_2), gain, wo, wp, half)
     keys, values, state = early(own1, got1, gates, qm)
-    own2, par2 = finish(a_2, b_2, *done, gain, wo, wp)
+    own2, par2 = finish((a_2,), *done, gain, wo, wp)
     pairs = [[i, i + 1] for i in range(0, tps, 2)]
     both2 = lax.all_gather(par2, "tp", axis_index_groups=pairs)
     keys, values, part = late(

time: 69.8 us -> 69.7 us (level)
  blocking collectives: 15.6 us -> 14 us
  waiting for transfers between devices: 15.7 us -> 16.9 us
    all_gather x1, blocking collectives: 3.39 us -> 1.96 us  [body(): both2 = lax.all_gather(par2, 'tp', axis_index_groups=pairs)]
    ppermute x7, waiting for transfers between devices: 15.7 us -> 16.9 us  [shift(): return lax.ppermute(x, 'tp', by)]
where the time goes in v5:
time: 69.7 us; the launch traced here: 69.3 us
  starting transfers between devices  26.7 us (38%)
  waiting for transfers between devices  16.9 us (24%)
  blocking collectives  14 us (20%)
  Pallas kernels  9.02 us (13%)
  local copies, waits for them, and re-layouts  1.75 us (3%)
  between operations  0.94 us (1%)
    ppermute x7, starting transfers between devices, shift(): return lax.ppermute(x, 'tp', by)  26.7 us
    ppermute x7, waiting for transfers between devices, shift(): return lax.ppermute(x, 'tp', by)  16.9 us
    all_to_all x1, blocking collectives, body(): parts = lax.all_to_all(part, 'sp', split_axis=0, concat_axis=0, tiled=True)  12.1 us
    pallas_call x3, Pallas kernels, project(): pl.pallas_call(functools.partial(project_kernel, len(xs), bool(before)),...  4.89 us
    all_gather x1, blocking collectives, body(): both2 = lax.all_gather(par2, 'tp', axis_index_groups=pairs)  1.96 us
    unnamed x17, local copies, waits for them, and re-layouts  1.45 us
  transfers between devices with their start and end apart: 7, of which 2 were waited for; matrix products, arithmetic and copies ran while one was open for 2% of the time, Pallas kernels for 9%

profile of v5, /device:TPU:1, one launch (start us, length us, event | category | flops | bytes accessed | tf_op | source)
XLA Modules:
  0.0 69.3 jit_solution(5619957648012399176)
XLA Ops:
  0.6 0.0 copy-start
  0.6 0.0 copy-start.6
  0.7 5.3 %collective-permute-start = (bf16[2,64,4096]{2,1,0:T(8,128)(2,1)}, bf16[2,64,4096]{2,1,0:T(8,128)(2,1)S(1)}, u32[]{:S(2)}, u32[]{:S(2)}) collective-permute-start(bf16[2,64,4096]{2,1,0:T(8,128)(2,1)} %tokens.1), channel_id=1, source_target_pairs={{0,2},{1,7},{2,4},{3,1},{4,6},{5,3},{6,0},{7,5},{8,10},{9,15},{10,... | collective-permute-start | bytes 3145736 | tf_op jit(solution)/shard_map/ppermute | solution.py:381
  6.0 1.4 %constant_dynamic-update-slice_fusion.1 = bf16[4096,256]{1,0:T(8,128)(2,1)S(1)} fusion(bf16[4096,128]{1,0:T(8,128)(2,1)} %param.11), kind=kLoop, calls=%fused_computation.2 | loop fusion | bytes 2097152
  7.4 0.0 copy-done.6
  7.4 0.0 copy-start.7
  7.4 0.0 copy-start.1
  7.4 0.0 copy-start.2
  7.4 0.0 copy-start.3
  7.5 0.0 copy-start.4
  7.5 0.0 copy-start.5
  7.5 0.2 constant_dynamic-update-slice_fusion.refs_3_.refs_4_
  7.7 9.1 %collective-permute-start.5 = (bf16[4096,256]{1,0:T(8,128)(2,1)S(1)}, bf16[4096,256]{1,0:T(8,128)(2,1)S(1)}, u32[]{:S(2)}, u32[]{:S(2)}) collective-permute-start(bf16[4096,256]{1,0:T(8,128)(2,1)S(1)} %constant_dynamic-update-slice_fusion.refs_3_.refs_4_), channel_id=1, source_target_pairs={{0,1},{1,0},{2,3},{3,2},{4,5},{5,4},{6,7},{7,6},{8,9},{9,8},{10,11... | collective-permute-start | bytes 6291464 | tf_op jit(solution)/shard_map/ppermute | solution.py:381
  16.9 0.0 copy-done
  16.9 0.1 split.1
  16.9 1.9 %collective-permute-start.3 = (bf16[64,4096]{1,0:T(8,128)(2,1)S(1)}, bf16[64,4096]{1,0:T(8,128)(2,1)S(1)}, u32[]{:S(2)}, u32[]{:S(2)}) collective-permute-start(bf16[64,4096]{1,0:T(8,128)(2,1)S(1)} %get-tuple-element.28), channel_id=1, source_target_pairs={{0,6},{1,3},{2,0},{3,5},{4,2},{5,7},{6,4},{7,1},{8,14},{9,11},{10,... | collective-permute-start | bytes 1572872 | tf_op jit(solution)/shard_map/ppermute | solution.py:381
  18.9 1.9 %collective-permute-start.2 = (bf16[64,4096]{1,0:T(8,128)(2,1)S(1)}, bf16[64,4096]{1,0:T(8,128)(2,1)S(1)}, u32[]{:S(2)}, u32[]{:S(2)}) collective-permute-start(bf16[64,4096]{1,0:T(8,128)(2,1)S(1)} %get-tuple-element.27), channel_id=1, source_target_pairs={{0,6},{1,3},{2,0},{3,5},{4,2},{5,7},{6,4},{7,1},{8,14},{9,11},{10,... | collective-permute-start | bytes 1572872 | tf_op jit(solution)/shard_map/ppermute | solution.py:381
  20.8 13.5 %collective-permute-done.3.refs_1_ = bf16[64,4096]{1,0:T(8,128)(2,1)S(1)} collective-permute-done((bf16[64,4096]{1,0:T(8,128)(2,1)S(1)}, bf16[64,4096]{1,0:T(8,128)(2,1)S(1)}, u32[]{:S(2)}, u32[]{:S(2)}) %collective-permute-start.3) | collective-permute-done | bytes 524320 | tf_op jit(solution)/shard_map/ppermute | solution.py:381
  34.3 1.9 %collective-permute-start.4 = (bf16[64,4096]{1,0:T(8,128)(2,1)S(1)}, bf16[64,4096]{1,0:T(8,128)(2,1)S(1)}, u32[]{:S(2)}, u32[]{:S(2)}) collective-permute-start(bf16[64,4096]{1,0:T(8,128)(2,1)S(1)} %collective-permute-done.3.refs_1_), channel_id=1, source_target_pairs={{0,6},{1,3},{2,0},{3,5},{4,2},{5,7},{6,4},{7,1},{8,14},{9,11},{10,... | collective-permute-start | bytes 1572872 | tf_op jit(solution)/shard_map/ppermute | solution.py:381
  36.2 0.0 collective-permute-done
  36.2 4.6 %collective-permute-start.1 = (bf16[64,4096]{1,0:T(8,128)(2,1)S(1)}, bf16[64,4096]{1,0:T(8,128)(2,1)S(1)}, u32[]{:S(2)}, u32[]{:S(2)}) collective-permute-start(bf16[64,4096]{1,0:T(8,128)(2,1)S(1)} %slice_bitcast_fusion), channel_id=1, source_target_pairs={{0,2},{1,7},{2,4},{3,1},{4,6},{5,3},{6,0},{7,5},{8,10},{9,15},{10,... | collective-permute-start | bytes 1572872 | tf_op jit(solution)/shard_map/ppermute | solution.py:381
  40.8 0.0 copy-done.7
  40.8 0.0 copy-done.1
  40.9 0.0 copy-done.2
  40.9 0.0 copy-done.3
  40.9 0.0 copy-done.4
  40.9 0.0 copy-done.5
  40.9 0.3 prepare.1
  41.2 0.0 collective-permute-done.5.refs_4_.refs_5_
  41.2 2.1 %project.4 = (bf16[3,64,256]{2,1,0:T(8,128)(2,1)S(1)}, bf16[3,64,256]{2,1,0:T(8,128)(2,1)S(1)}) custom-call(bf16[128,4096]{1,0:T(8,128)(2,1)S(1)} %bitcast.6, bf16[64,4096]{1,0:T(8,128)(2,1)S(1)} %collective-permute-done.3.refs_1_, bf16[1,4096]{1,0:T(2,128)(2,1)S(1)} %reshape.15.refs_2_.refs_3_, ...), custom_call_target="tpu_custom_call" | custom-call | flops 805306368 | bytes 6291456 | tf_op jit(solution)/shard_map/project/pallas_call | solution.py:119
  43.2 1.4 %project.5 = (bf16[5,64,256]{2,1,0:T(8,128)(2,1)S(1)}, bf16[5,64,256]{2,1,0:T(8,128)(2,1)S(1)}) custom-call(bf16[128,4096]{1,0:T(8,128)(2,1)S(1)} %bitcast.7, bf16[3,64,256]{2,1,0:T(8,128)(2,1)S(1)} %get-tuple-element.41.refs_1_, bf16[3,64,256]{2,1,0:T(8,128)(2,1)S(1)} %get-tuple-element.42.refs_2_, bf16[1,4096]{1,0:T(2,128)(2,1)S(1)} %reshape.15.refs_2_.refs_3_, ...), custom_call_target="tpu_custom_call" | custom-call | flops 536870912 | bytes 6291456 | tf_op jit(solution)/shard_map/project/pallas_call | solution.py:119
  44.7 1.9 %collective-permute-start.6 = (bf16[5,64,256]{2,1,0:T(8,128)(2,1)S(1)}, bf16[5,64,256]{2,1,0:T(8,128)(2,1)S(1)}, u32[]{:S(2)}, u32[]{:S(2)}) collective-permute-start(bf16[5,64,256]{2,1,0:T(8,128)(2,1)S(1)} %get-tuple-element.44), channel_id=1, source_target_pairs={{0,1},{1,0},{2,3},{3,2},{4,5},{5,4},{6,7},{7,6},{8,9},{9,8},{10,11... | collective-permute-start | bytes 491528 | tf_op jit(solution)/shard_map/ppermute | solution.py:381
  46.6 0.0 collective-permute-done.2.refs_0_
  46.6 3.4 %collective-permute-done.4.refs_1_ = bf16[64,4096]{1,0:T(8,128)(2,1)S(1)} collective-permute-done((bf16[64,4096]{1,0:T(8,128)(2,1)S(1)}, bf16[64,4096]{1,0:T(8,128)(2,1)S(1)}, u32[]{:S(2)}, u32[]{:S(2)}) %collective-permute-start.4) | collective-permute-done | bytes 524320 | tf_op jit(solution)/shard_map/ppermute | solution.py:381
  50.0 1.4 %project.3 = (bf16[2,64,256]{2,1,0:T(8,128)(2,1)S(1)}, bf16[2,64,256]{2,1,0:T(8,128)(2,1)S(1)}) custom-call(bf16[64,4096]{1,0:T(8,128)(2,1)S(1)} %collective-permute-done.2.refs_0_, bf16[64,4096]{1,0:T(8,128)(2,1)S(1)} %collective-permute-done.4.refs_1_, bf16[1,4096]{1,0:T(2,128)(2,1)S(1)} %reshape.15.refs_2_.refs_3_, ...), custom_call_target="tpu_custom_call" | custom-call | flops 536870912 | bytes 6291456 | tf_op jit(solution)/shard_map/project/pallas_call | solution.py:119
  51.5 0.0 collective-permute-done.1.refs_0_
  51.5 1.0 %finish.1 = (bf16[3,64,256]{2,1,0:T(8,128)(2,1)S(1)}, bf16[3,64,256]{2,1,0:T(8,128)(2,1)S(1)}) custom-call(bf16[64,4096]{1,0:T(8,128)(2,1)S(1)} %collective-permute-done.1.refs_0_, bf16[2,64,256]{2,1,0:T(8,128)(2,1)S(1)} %get-tuple-element.34.refs_1_, bf16[2,64,256]{2,1,0:T(8,128)(2,1)S(1)} %get-tuple-element.35.refs_2_, ...), custom_call_target="tpu_custom_call" | custom-call | flops 268435456 | bytes 6291456 | tf_op jit(solution)/shard_map/finish/pallas_call | solution.py:98
  52.4 2.0 %all-gather = bf16[6,64,256]{2,1,0:T(8,128)(2,1)S(1)} all-gather(bf16[3,64,256]{2,1,0:T(8,128)(2,1)S(1)} %get-tuple-element.37), channel_id=2, replica_groups={{0,1},{2,3},{4,5},{6,7},{8,9},{10,11},{12,13},{14,15},{16,17},{18,19},{..., dimensions={0}, use_global_device_ids=true | all-gather | bytes 294912 | tf_op jit(solution)/shard_map/all_gather | solution.py:420
  54.4 0.0 collective-permute-done.6.got
  54.4 1.1 %early.1 = (bf16[2,512,128]{2,1,0:T(8,128)(2,1)}, bf16[2,512,128]{2,1,0:T(8,128)(2,1)}, f32[8,128]{1,0:T(8,128)S(1)}) custom-call(bf16[5,64,256]{2,1,0:T(8,128)(2,1)S(1)} %get-tuple-element.43.own, bf16[5,64,256]{2,1,0:T(8,128)(2,1)S(1)} %collective-permute-done.6.got, f32[2,512,128]{2,1,0:T(8,128)S(1)} %get-tuple-element.38.gates, ...), custom_call_target="tpu_custom_call" | custom-call | flops 67108864 | bytes 2097152 | tf_op jit(solution)/shard_map/early/pallas_call | solution.py:231
  55.5 1.0 %late.1 = (bf16[2,512,128]{2,1,0:T(8,128)(2,1)}, bf16[2,512,128]{2,1,0:T(8,128)(2,1)}, f32[32,1,384]{2,1,0:T(1,128)S(1)}) custom-call(bf16[3,64,256]{2,1,0:T(8,128)(2,1)S(1)} %get-tuple-element.36.own, bf16[2,3,64,256]{3,2,1,0:T(8,128)(2,1)S(1)} %bitcast.8, ...), custom_call_target="tpu_custom_call", output_to_operand_aliasing={{0}: (6, {}), {1}: (7, {})} | custom-call | flops 16777216 | bytes 1048576 | tf_op jit(solution)/shard_map/late/pallas_call | solution.py:301
  56.5 12.1 %all_to_all.5.parts = f32[32,1,384]{2,1,0:T(1,128)S(1)} all-to-all(f32[32,1,384]{2,1,0:T(1,128)S(1)} %get-tuple-element.48), channel_id=1, replica_groups=mesh['gr'=3,'sp'=32,'tp'=8] {'sp'}, dimensions={0} | all-to-all | bytes 98304 | tf_op jit(solution)/shard_map/all_to_all | solution.py:424
  68.6 0.8 %merge.1 = (bf16[2,512,128]{2,1,0:T(8,128)(2,1)}, bf16[2,512,128]{2,1,0:T(8,128)(2,1)}, bf16[2,128]{1,0:T(2,128)(2,1)}) custom-call(f32[32,1,384]{2,1,0:T(1,128)S(1)} %all_to_all.5.parts, bf16[3,64,256]{2,1,0:T(8,128)(2,1)S(1)} %get-tuple-element.36.own, bf16[2,3,64,256]{3,2,1,0:T(8,128)(2,1)S(1)} %bitcast.9, ...), custom_call_target="tpu_custom_call", output_to_operand_aliasing={{0}: (3, {}), {1}: (4, {})} | custom-call | tf_op jit(solution)/shard_map/merge/pallas_call | solution.py:348
  (2 shorter events, 0.0 us)
Async XLA Ops:
  0.6 16.2 %copy-start = (bf16[2,64,4096]{2,1,0:T(8,128)(2,1)S(1)}, bf16[2,64,4096]{2,1,0:T(8,128)(2,1)}, u32[]{:S(2)}) copy-start(bf16[2,64,4096]{2,1,0:T(8,128)(2,1)} %tokens.1) | copy-start | bytes 3145732
  0.6 6.8 %copy-start.6 = (bf16[4096,128]{1,0:T(8,128)(2,1)S(1)}, bf16[4096,128]{1,0:T(8,128)(2,1)}, u32[]{:S(2)}) copy-start(bf16[4096,128]{1,0:T(8,128)(2,1)} %param.12) | copy-start | bytes 3145732
  0.7 35.5 %collective-permute-start = (bf16[2,64,4096]{2,1,0:T(8,128)(2,1)}, bf16[2,64,4096]{2,1,0:T(8,128)(2,1)S(1)}, u32[]{:S(2)}, u32[]{:S(2)}) collective-permute-start(bf16[2,64,4096]{2,1,0:T(8,128)(2,1)} %tokens.1), channel_id=1, source_target_pairs={{0,2},{1,7},{2,4},{3,1},{4,6},{5,3},{6,0},{7,5},{8,10},{9,15},{10,... | collective-permute-start | bytes 3145736 | tf_op jit(solution)/shard_map/ppermute | solution.py:381
  7.4 33.4 %copy-start.7 = (bf16[4096]{0:T(1024)(128)(2,1)S(1)}, bf16[4096]{0:T(1024)(128)(2,1)}, u32[]{:S(2)}) copy-start(bf16[4096]{0:T(1024)(128)(2,1)} %param.10) | copy-start | bytes 24580
  7.4 33.4 %copy-start.1 = (f32[2,512,2]{1,2,0:T(2,128)S(1)}, f32[2,512,2]{1,2,0:T(2,128)}, u32[]{:S(2)}) copy-start(f32[2,512,2]{1,2,0:T(2,128)} %param.13) | copy-start | bytes 24580
  7.4 33.4 %copy-start.2 = (f32[2,2]{1,0:T(2,128)S(1)}, f32[2,2]{1,0:T(2,128)}, u32[]{:S(2)}) copy-start(f32[2,2]{1,0:T(2,128)} %ng.1) | copy-start | bytes 52
  7.4 33.4 %copy-start.3 = (bf16[2,128]{1,0:T(2,128)(2,1)S(1)}, bf16[2,128]{1,0:T(2,128)(2,1)}, u32[]{:S(2)}) copy-start(bf16[2,128]{1,0:T(2,128)(2,1)} %q.1) | copy-start | bytes 1540
  7.5 33.4 %copy-start.4 = (bf16[2,128]{1,0:T(2,128)(2,1)S(1)}, bf16[2,128]{1,0:T(2,128)(2,1)}, u32[]{:S(2)}) copy-start(bf16[2,128]{1,0:T(2,128)(2,1)} %fk.1) | copy-start | bytes 1540
  7.5 33.4 %copy-start.5 = (bf16[2,128]{1,0:T(2,128)(2,1)S(1)}, bf16[2,128]{1,0:T(2,128)(2,1)}, u32[]{:S(2)}) copy-start(bf16[2,128]{1,0:T(2,128)(2,1)} %fv.1) | copy-start | bytes 1540
  7.7 33.4 %collective-permute-start.5 = (bf16[4096,256]{1,0:T(8,128)(2,1)S(1)}, bf16[4096,256]{1,0:T(8,128)(2,1)S(1)}, u32[]{:S(2)}, u32[]{:S(2)}) collective-permute-start(bf16[4096,256]{1,0:T(8,128)(2,1)S(1)} %constant_dynamic-update-slice_fusion.refs_3_.refs_4_), channel_id=1, source_target_pairs={{0,1},{1,0},{2,3},{3,2},{4,5},{5,4},{6,7},{7,6},{8,9},{9,8},{10,11... | collective-permute-start | bytes 6291464 | tf_op jit(solution)/shard_map/ppermute | solution.py:381
  16.9 17.3 %collective-permute-start.3 = (bf16[64,4096]{1,0:T(8,128)(2,1)S(1)}, bf16[64,4096]{1,0:T(8,128)(2,1)S(1)}, u32[]{:S(2)}, u32[]{:S(2)}) collective-permute-start(bf16[64,4096]{1,0:T(8,128)(2,1)S(1)} %get-tuple-element.28), channel_id=1, source_target_pairs={{0,6},{1,3},{2,0},{3,5},{4,2},{5,7},{6,4},{7,1},{8,14},{9,11},{10,... | collective-permute-start | bytes 1572872 | tf_op jit(solution)/shard_map/ppermute | solution.py:381
  18.9 27.7 %collective-permute-start.2 = (bf16[64,4096]{1,0:T(8,128)(2,1)S(1)}, bf16[64,4096]{1,0:T(8,128)(2,1)S(1)}, u32[]{:S(2)}, u32[]{:S(2)}) collective-permute-start(bf16[64,4096]{1,0:T(8,128)(2,1)S(1)} %get-tuple-element.27), channel_id=1, source_target_pairs={{0,6},{1,3},{2,0},{3,5},{4,2},{5,7},{6,4},{7,1},{8,14},{9,11},{10,... | collective-permute-start | bytes 1572872 | tf_op jit(solution)/shard_map/ppermute | solution.py:381
  34.3 15.8 %collective-permute-start.4 = (bf16[64,4096]{1,0:T(8,128)(2,1)S(1)}, bf16[64,4096]{1,0:T(8,128)(2,1)S(1)}, u32[]{:S(2)}, u32[]{:S(2)}) collective-permute-start(bf16[64,4096]{1,0:T(8,128)(2,1)S(1)} %collective-permute-done.3.refs_1_), channel_id=1, source_target_pairs={{0,6},{1,3},{2,0},{3,5},{4,2},{5,7},{6,4},{7,1},{8,14},{9,11},{10,... | collective-permute-start | bytes 1572872 | tf_op jit(solution)/shard_map/ppermute | solution.py:381
  36.2 15.2 %collective-permute-start.1 = (bf16[64,4096]{1,0:T(8,128)(2,1)S(1)}, bf16[64,4096]{1,0:T(8,128)(2,1)S(1)}, u32[]{:S(2)}, u32[]{:S(2)}) collective-permute-start(bf16[64,4096]{1,0:T(8,128)(2,1)S(1)} %slice_bitcast_fusion), channel_id=1, source_target_pairs={{0,2},{1,7},{2,4},{3,1},{4,6},{5,3},{6,0},{7,5},{8,10},{9,15},{10,... | collective-permute-start | bytes 1572872 | tf_op jit(solution)/shard_map/ppermute | solution.py:381
  44.7 9.7 %collective-permute-start.6 = (bf16[5,64,256]{2,1,0:T(8,128)(2,1)S(1)}, bf16[5,64,256]{2,1,0:T(8,128)(2,1)S(1)}, u32[]{:S(2)}, u32[]{:S(2)}) collective-permute-start(bf16[5,64,256]{2,1,0:T(8,128)(2,1)S(1)} %get-tuple-element.44), channel_id=1, source_target_pairs={{0,1},{1,0},{2,3},{3,2},{4,5},{5,4},{6,7},{7,6},{8,9},{9,8},{10,11... | collective-permute-start | bytes 491528 | tf_op jit(solution)/shard_map/ppermute | solution.py:381

commit v6 on v5

--- a/solution.py
+++ b/solution.py
@@ -17,7 +17,7 @@
 VMEM = pl.BlockSpec(memory_space=pltpu.VMEM)
 ANY = pl.BlockSpec(memory_space=pl.ANY)
 
-EARLY = ((0, 0), (0, 1), (1, 1), (3, 0), (3, 1))
+EARLY = ((0, 0), (0, 1), (3, 0), (3, 1), (1, 1))
 LATE = ((1, 0), (2, 1), (2, 0))
 
 
@@ -408,9 +408,9 @@
     gates, qm, small = made
 
     rows = (2 * half, width)
-    done = project((tokens.reshape(rows), b_1), gain, wo, wp, half)
+    done = project((tokens.reshape(rows),), gain, wo, wp, half)
     own1, par1 = project(
-        (from_3.reshape(rows),), gain, wo, wp, half, done
+        (from_3.reshape(rows), b_1), gain, wo, wp, half, done
     )
     got1 = shift(par1, swap)
     done = project((a_1, b_2), gain, wo, wp, half)

time: 69.7 us -> 69.8 us (level)
  no operation moved by 1% of the time
where the time goes in v6:
time: 69.8 us; the launch traced here: 69.4 us
  starting transfers between devices  26.7 us (38%)
  waiting for transfers between devices  16.9 us (24%)
  blocking collectives  14.1 us (20%)
  Pallas kernels  9.02 us (13%)
  local copies, waits for them, and re-layouts  1.75 us (3%)
  between operations  0.94 us (1%)
    ppermute x7, starting transfers between devices, shift(): return lax.ppermute(x, 'tp', by)  26.7 us
    ppermute x7, waiting for transfers between devices, shift(): return lax.ppermute(x, 'tp', by)  16.9 us
    all_to_all x1, blocking collectives, body(): parts = lax.all_to_all(part, 'sp', split_axis=0, concat_axis=0, tiled=True)  12.2 us
    pallas_call x3, Pallas kernels, project(): pl.pallas_call(functools.partial(project_kernel, len(xs), bool(before)),...  4.89 us
    all_gather x1, blocking collectives, body(): both2 = lax.all_gather(par2, 'tp', axis_index_groups=pairs)  1.96 us
    unnamed x17, local copies, waits for them, and re-layouts  1.45 us
  transfers between devices with their start and end apart: 7, of which 2 were waited for; matrix products, arithmetic and copies ran while one was open for 2% of the time, Pallas kernels for 9%

profile of v6, /device:TPU:1, one launch (start us, length us, event | category | flops | bytes accessed | tf_op | source)
XLA Modules:
  0.0 69.4 jit_solution(6986696770526364510)
XLA Ops:
  0.6 0.0 copy-start
  0.6 0.0 copy-start.6
  0.7 5.3 %collective-permute-start = (bf16[2,64,4096]{2,1,0:T(8,128)(2,1)}, bf16[2,64,4096]{2,1,0:T(8,128)(2,1)S(1)}, u32[]{:S(2)}, u32[]{:S(2)}) collective-permute-start(bf16[2,64,4096]{2,1,0:T(8,128)(2,1)} %tokens.1), channel_id=1, source_target_pairs={{0,2},{1,7},{2,4},{3,1},{4,6},{5,3},{6,0},{7,5},{8,10},{9,15},{10,... | collective-permute-start | bytes 3145736 | tf_op jit(solution)/shard_map/ppermute | solution.py:381
  6.0 1.4 %constant_dynamic-update-slice_fusion.1 = bf16[4096,256]{1,0:T(8,128)(2,1)S(1)} fusion(bf16[4096,128]{1,0:T(8,128)(2,1)} %param.11), kind=kLoop, calls=%fused_computation.2 | loop fusion | bytes 2097152
  7.4 0.0 copy-done.6
  7.4 0.0 copy-start.7
  7.4 0.0 copy-start.1
  7.4 0.0 copy-start.2
  7.4 0.0 copy-start.3
  7.5 0.0 copy-start.4
  7.5 0.0 copy-start.5
  7.5 0.2 constant_dynamic-update-slice_fusion.refs_3_.refs_4_.refs_2_.refs_5_
  7.7 9.1 %collective-permute-start.5 = (bf16[4096,256]{1,0:T(8,128)(2,1)S(1)}, bf16[4096,256]{1,0:T(8,128)(2,1)S(1)}, u32[]{:S(2)}, u32[]{:S(2)}) collective-permute-start(bf16[4096,256]{1,0:T(8,128)(2,1)S(1)} %constant_dynamic-update-slice_fusion.refs_3_.refs_4_.refs_2_.refs_5_), channel_id=1, source_target_pairs={{0,1},{1,0},{2,3},{3,2},{4,5},{5,4},{6,7},{7,6},{8,9},{9,8},{10,11... | collective-permute-start | bytes 6291464 | tf_op jit(solution)/shard_map/ppermute | solution.py:381
  16.9 0.0 copy-done
  16.9 0.1 split.1
  16.9 1.9 %collective-permute-start.3 = (bf16[64,4096]{1,0:T(8,128)(2,1)S(1)}, bf16[64,4096]{1,0:T(8,128)(2,1)S(1)}, u32[]{:S(2)}, u32[]{:S(2)}) collective-permute-start(bf16[64,4096]{1,0:T(8,128)(2,1)S(1)} %get-tuple-element.28), channel_id=1, source_target_pairs={{0,6},{1,3},{2,0},{3,5},{4,2},{5,7},{6,4},{7,1},{8,14},{9,11},{10,... | collective-permute-start | bytes 1572872 | tf_op jit(solution)/shard_map/ppermute | solution.py:381
  18.9 1.9 %collective-permute-start.2 = (bf16[64,4096]{1,0:T(8,128)(2,1)S(1)}, bf16[64,4096]{1,0:T(8,128)(2,1)S(1)}, u32[]{:S(2)}, u32[]{:S(2)}) collective-permute-start(bf16[64,4096]{1,0:T(8,128)(2,1)S(1)} %get-tuple-element.27), channel_id=1, source_target_pairs={{0,6},{1,3},{2,0},{3,5},{4,2},{5,7},{6,4},{7,1},{8,14},{9,11},{10,... | collective-permute-start | bytes 1572872 | tf_op jit(solution)/shard_map/ppermute | solution.py:381
  20.8 13.5 %collective-permute-done.3.refs_1_ = bf16[64,4096]{1,0:T(8,128)(2,1)S(1)} collective-permute-done((bf16[64,4096]{1,0:T(8,128)(2,1)S(1)}, bf16[64,4096]{1,0:T(8,128)(2,1)S(1)}, u32[]{:S(2)}, u32[]{:S(2)}) %collective-permute-start.3) | collective-permute-done | bytes 524320 | tf_op jit(solution)/shard_map/ppermute | solution.py:381
  34.3 1.9 %collective-permute-start.4 = (bf16[64,4096]{1,0:T(8,128)(2,1)S(1)}, bf16[64,4096]{1,0:T(8,128)(2,1)S(1)}, u32[]{:S(2)}, u32[]{:S(2)}) collective-permute-start(bf16[64,4096]{1,0:T(8,128)(2,1)S(1)} %collective-permute-done.3.refs_1_), channel_id=1, source_target_pairs={{0,6},{1,3},{2,0},{3,5},{4,2},{5,7},{6,4},{7,1},{8,14},{9,11},{10,... | collective-permute-start | bytes 1572872 | tf_op jit(solution)/shard_map/ppermute | solution.py:381
  36.2 0.0 collective-permute-done
  36.2 4.6 %collective-permute-start.1 = (bf16[64,4096]{1,0:T(8,128)(2,1)S(1)}, bf16[64,4096]{1,0:T(8,128)(2,1)S(1)}, u32[]{:S(2)}, u32[]{:S(2)}) collective-permute-start(bf16[64,4096]{1,0:T(8,128)(2,1)S(1)} %slice_bitcast_fusion), channel_id=1, source_target_pairs={{0,2},{1,7},{2,4},{3,1},{4,6},{5,3},{6,0},{7,5},{8,10},{9,15},{10,... | collective-permute-start | bytes 1572872 | tf_op jit(solution)/shard_map/ppermute | solution.py:381
  40.8 0.0 copy-done.7
  40.8 0.0 copy-done.1
  40.9 0.0 copy-done.2
  40.9 0.0 copy-done.3
  40.9 0.0 copy-done.4
  40.9 0.0 copy-done.5
  40.9 0.3 prepare.1
  41.2 0.0 collective-permute-done.5.refs_4_.refs_5_.refs_3_.refs_6_
  41.2 1.4 %project.4 = (bf16[2,64,256]{2,1,0:T(8,128)(2,1)S(1)}, bf16[2,64,256]{2,1,0:T(8,128)(2,1)S(1)}) custom-call(bf16[128,4096]{1,0:T(8,128)(2,1)S(1)} %bitcast.6, bf16[1,4096]{1,0:T(2,128)(2,1)S(1)} %reshape.15.refs_2_.refs_3_.refs_1_.refs_4_, bf16[4096,256]{1,0:T(8,128)(2,1)S(1)} %constant_dynamic-update-slice_fusion.refs_3_.refs_4_.refs_2_.refs_5_, ...), custom_call_target="tpu_custom_call" | custom-call | flops 536870912 | bytes 6291456 | tf_op jit(solution)/shard_map/project/pallas_call | solution.py:119
  42.6 2.0 %project.5 = (bf16[5,64,256]{2,1,0:T(8,128)(2,1)S(1)}, bf16[5,64,256]{2,1,0:T(8,128)(2,1)S(1)}) custom-call(bf16[128,4096]{1,0:T(8,128)(2,1)S(1)} %bitcast.7, bf16[64,4096]{1,0:T(8,128)(2,1)S(1)} %collective-permute-done.3.refs_1_, bf16[2,64,256]{2,1,0:T(8,128)(2,1)S(1)} %get-tuple-element.41.refs_2_, bf16[2,64,256]{2,1,0:T(8,128)(2,1)S(1)} %get-tuple-element.42.refs_3_, ...), custom_call_target="tpu_custom_call" | custom-call | flops 805306368 | bytes 6291456 | tf_op jit(solution)/shard_map/project/pallas_call | solution.py:119
  44.7 1.9 %collective-permute-start.6 = (bf16[5,64,256]{2,1,0:T(8,128)(2,1)S(1)}, bf16[5,64,256]{2,1,0:T(8,128)(2,1)S(1)}, u32[]{:S(2)}, u32[]{:S(2)}) collective-permute-start(bf16[5,64,256]{2,1,0:T(8,128)(2,1)S(1)} %get-tuple-element.44), channel_id=1, source_target_pairs={{0,1},{1,0},{2,3},{3,2},{4,5},{5,4},{6,7},{7,6},{8,9},{9,8},{10,11... | collective-permute-start | bytes 491528 | tf_op jit(solution)/shard_map/ppermute | solution.py:381
  46.6 0.0 collective-permute-done.2.refs_0_
  46.6 3.4 %collective-permute-done.4.refs_1_ = bf16[64,4096]{1,0:T(8,128)(2,1)S(1)} collective-permute-done((bf16[64,4096]{1,0:T(8,128)(2,1)S(1)}, bf16[64,4096]{1,0:T(8,128)(2,1)S(1)}, u32[]{:S(2)}, u32[]{:S(2)}) %collective-permute-start.4) | collective-permute-done | bytes 524320 | tf_op jit(solution)/shard_map/ppermute | solution.py:381
  50.0 1.4 %project.3 = (bf16[2,64,256]{2,1,0:T(8,128)(2,1)S(1)}, bf16[2,64,256]{2,1,0:T(8,128)(2,1)S(1)}) custom-call(bf16[64,4096]{1,0:T(8,128)(2,1)S(1)} %collective-permute-done.2.refs_0_, bf16[64,4096]{1,0:T(8,128)(2,1)S(1)} %collective-permute-done.4.refs_1_, bf16[1,4096]{1,0:T(2,128)(2,1)S(1)} %reshape.15.refs_2_.refs_3_.refs_1_.refs_4_, ...), custom_call_target="tpu_custom_call" | custom-call | flops 536870912 | bytes 6291456 | tf_op jit(solution)/shard_map/project/pallas_call | solution.py:119
  51.5 0.0 collective-permute-done.1.refs_0_
  51.5 1.0 %finish.1 = (bf16[3,64,256]{2,1,0:T(8,128)(2,1)S(1)}, bf16[3,64,256]{2,1,0:T(8,128)(2,1)S(1)}) custom-call(bf16[64,4096]{1,0:T(8,128)(2,1)S(1)} %collective-permute-done.1.refs_0_, bf16[2,64,256]{2,1,0:T(8,128)(2,1)S(1)} %get-tuple-element.34.refs_1_, bf16[2,64,256]{2,1,0:T(8,128)(2,1)S(1)} %get-tuple-element.35.refs_2_, ...), custom_call_target="tpu_custom_call" | custom-call | flops 268435456 | bytes 6291456 | tf_op jit(solution)/shard_map/finish/pallas_call | solution.py:98
  52.4 2.0 %all-gather = bf16[6,64,256]{2,1,0:T(8,128)(2,1)S(1)} all-gather(bf16[3,64,256]{2,1,0:T(8,128)(2,1)S(1)} %get-tuple-element.37), channel_id=2, replica_groups={{0,1},{2,3},{4,5},{6,7},{8,9},{10,11},{12,13},{14,15},{16,17},{18,19},{..., dimensions={0}, use_global_device_ids=true | all-gather | bytes 294912 | tf_op jit(solution)/shard_map/all_gather | solution.py:420
  54.4 0.0 collective-permute-done.6.got
  54.4 1.1 %early.1 = (bf16[2,512,128]{2,1,0:T(8,128)(2,1)}, bf16[2,512,128]{2,1,0:T(8,128)(2,1)}, f32[8,128]{1,0:T(8,128)S(1)}) custom-call(bf16[5,64,256]{2,1,0:T(8,128)(2,1)S(1)} %get-tuple-element.43.own, bf16[5,64,256]{2,1,0:T(8,128)(2,1)S(1)} %collective-permute-done.6.got, f32[2,512,128]{2,1,0:T(8,128)S(1)} %get-tuple-element.38.gates, ...), custom_call_target="tpu_custom_call" | custom-call | flops 67108864 | bytes 2097152 | tf_op jit(solution)/shard_map/early/pallas_call | solution.py:231
  55.5 1.0 %late.1 = (bf16[2,512,128]{2,1,0:T(8,128)(2,1)}, bf16[2,512,128]{2,1,0:T(8,128)(2,1)}, f32[32,1,384]{2,1,0:T(1,128)S(1)}) custom-call(bf16[3,64,256]{2,1,0:T(8,128)(2,1)S(1)} %get-tuple-element.36.own, bf16[2,3,64,256]{3,2,1,0:T(8,128)(2,1)S(1)} %bitcast.8, ...), custom_call_target="tpu_custom_call", output_to_operand_aliasing={{0}: (6, {}), {1}: (7, {})} | custom-call | flops 16777216 | bytes 1048576 | tf_op jit(solution)/shard_map/late/pallas_call | solution.py:301
  56.5 12.2 %all_to_all.5.parts = f32[32,1,384]{2,1,0:T(1,128)S(1)} all-to-all(f32[32,1,384]{2,1,0:T(1,128)S(1)} %get-tuple-element.48), channel_id=1, replica_groups=mesh['gr'=3,'sp'=32,'tp'=8] {'sp'}, dimensions={0} | all-to-all | bytes 98304 | tf_op jit(solution)/shard_map/all_to_all | solution.py:424
  68.6 0.8 %merge.1 = (bf16[2,512,128]{2,1,0:T(8,128)(2,1)}, bf16[2,512,128]{2,1,0:T(8,128)(2,1)}, bf16[2,128]{1,0:T(2,128)(2,1)}) custom-call(f32[32,1,384]{2,1,0:T(1,128)S(1)} %all_to_all.5.parts, bf16[3,64,256]{2,1,0:T(8,128)(2,1)S(1)} %get-tuple-element.36.own, bf16[2,3,64,256]{3,2,1,0:T(8,128)(2,1)S(1)} %bitcast.9, ...), custom_call_target="tpu_custom_call", output_to_operand_aliasing={{0}: (3, {}), {1}: (4, {})} | custom-call | tf_op jit(solution)/shard_map/merge/pallas_call | solution.py:348
  (2 shorter events, 0.0 us)
Async XLA Ops:
  0.6 16.2 %copy-start = (bf16[2,64,4096]{2,1,0:T(8,128)(2,1)S(1)}, bf16[2,64,4096]{2,1,0:T(8,128)(2,1)}, u32[]{:S(2)}) copy-start(bf16[2,64,4096]{2,1,0:T(8,128)(2,1)} %tokens.1) | copy-start | bytes 3145732
  0.6 6.8 %copy-start.6 = (bf16[4096,128]{1,0:T(8,128)(2,1)S(1)}, bf16[4096,128]{1,0:T(8,128)(2,1)}, u32[]{:S(2)}) copy-start(bf16[4096,128]{1,0:T(8,128)(2,1)} %param.12) | copy-start | bytes 3145732
  0.7 35.5 %collective-permute-start = (bf16[2,64,4096]{2,1,0:T(8,128)(2,1)}, bf16[2,64,4096]{2,1,0:T(8,128)(2,1)S(1)}, u32[]{:S(2)}, u32[]{:S(2)}) collective-permute-start(bf16[2,64,4096]{2,1,0:T(8,128)(2,1)} %tokens.1), channel_id=1, source_target_pairs={{0,2},{1,7},{2,4},{3,1},{4,6},{5,3},{6,0},{7,5},{8,10},{9,15},{10,... | collective-permute-start | bytes 3145736 | tf_op jit(solution)/shard_map/ppermute | solution.py:381
  7.4 33.4 %copy-start.7 = (bf16[4096]{0:T(1024)(128)(2,1)S(1)}, bf16[4096]{0:T(1024)(128)(2,1)}, u32[]{:S(2)}) copy-start(bf16[4096]{0:T(1024)(128)(2,1)} %param.10) | copy-start | bytes 24580
  7.4 33.4 %copy-start.1 = (f32[2,512,2]{1,2,0:T(2,128)S(1)}, f32[2,512,2]{1,2,0:T(2,128)}, u32[]{:S(2)}) copy-start(f32[2,512,2]{1,2,0:T(2,128)} %param.13) | copy-start | bytes 24580
  7.4 33.4 %copy-start.2 = (f32[2,2]{1,0:T(2,128)S(1)}, f32[2,2]{1,0:T(2,128)}, u32[]{:S(2)}) copy-start(f32[2,2]{1,0:T(2,128)} %ng.1) | copy-start | bytes 52
  7.4 33.4 %copy-start.3 = (bf16[2,128]{1,0:T(2,128)(2,1)S(1)}, bf16[2,128]{1,0:T(2,128)(2,1)}, u32[]{:S(2)}) copy-start(bf16[2,128]{1,0:T(2,128)(2,1)} %q.1) | copy-start | bytes 1540
  7.5 33.4 %copy-start.4 = (bf16[2,128]{1,0:T(2,128)(2,1)S(1)}, bf16[2,128]{1,0:T(2,128)(2,1)}, u32[]{:S(2)}) copy-start(bf16[2,128]{1,0:T(2,128)(2,1)} %fk.1) | copy-start | bytes 1540
  7.5 33.4 %copy-start.5 = (bf16[2,128]{1,0:T(2,128)(2,1)S(1)}, bf16[2,128]{1,0:T(2,128)(2,1)}, u32[]{:S(2)}) copy-start(bf16[2,128]{1,0:T(2,128)(2,1)} %fv.1) | copy-start | bytes 1540
  7.7 33.4 %collective-permute-start.5 = (bf16[4096,256]{1,0:T(8,128)(2,1)S(1)}, bf16[4096,256]{1,0:T(8,128)(2,1)S(1)}, u32[]{:S(2)}, u32[]{:S(2)}) collective-permute-start(bf16[4096,256]{1,0:T(8,128)(2,1)S(1)} %constant_dynamic-update-slice_fusion.refs_3_.refs_4_.refs_2_.refs_5_), channel_id=1, source_target_pairs={{0,1},{1,0},{2,3},{3,2},{4,5},{5,4},{6,7},{7,6},{8,9},{9,8},{10,11... | collective-permute-start | bytes 6291464 | tf_op jit(solution)/shard_map/ppermute | solution.py:381
  16.9 17.3 %collective-permute-start.3 = (bf16[64,4096]{1,0:T(8,128)(2,1)S(1)}, bf16[64,4096]{1,0:T(8,128)(2,1)S(1)}, u32[]{:S(2)}, u32[]{:S(2)}) collective-permute-start(bf16[64,4096]{1,0:T(8,128)(2,1)S(1)} %get-tuple-element.28), channel_id=1, source_target_pairs={{0,6},{1,3},{2,0},{3,5},{4,2},{5,7},{6,4},{7,1},{8,14},{9,11},{10,... | collective-permute-start | bytes 1572872 | tf_op jit(solution)/shard_map/ppermute | solution.py:381
  18.9 27.7 %collective-permute-start.2 = (bf16[64,4096]{1,0:T(8,128)(2,1)S(1)}, bf16[64,4096]{1,0:T(8,128)(2,1)S(1)}, u32[]{:S(2)}, u32[]{:S(2)}) collective-permute-start(bf16[64,4096]{1,0:T(8,128)(2,1)S(1)} %get-tuple-element.27), channel_id=1, source_target_pairs={{0,6},{1,3},{2,0},{3,5},{4,2},{5,7},{6,4},{7,1},{8,14},{9,11},{10,... | collective-permute-start | bytes 1572872 | tf_op jit(solution)/shard_map/ppermute | solution.py:381
  34.3 15.8 %collective-permute-start.4 = (bf16[64,4096]{1,0:T(8,128)(2,1)S(1)}, bf16[64,4096]{1,0:T(8,128)(2,1)S(1)}, u32[]{:S(2)}, u32[]{:S(2)}) collective-permute-start(bf16[64,4096]{1,0:T(8,128)(2,1)S(1)} %collective-permute-done.3.refs_1_), channel_id=1, source_target_pairs={{0,6},{1,3},{2,0},{3,5},{4,2},{5,7},{6,4},{7,1},{8,14},{9,11},{10,... | collective-permute-start | bytes 1572872 | tf_op jit(solution)/shard_map/ppermute | solution.py:381
  36.2 15.2 %collective-permute-start.1 = (bf16[64,4096]{1,0:T(8,128)(2,1)S(1)}, bf16[64,4096]{1,0:T(8,128)(2,1)S(1)}, u32[]{:S(2)}, u32[]{:S(2)}) collective-permute-start(bf16[64,4096]{1,0:T(8,128)(2,1)S(1)} %slice_bitcast_fusion), channel_id=1, source_target_pairs={{0,2},{1,7},{2,4},{3,1},{4,6},{5,3},{6,0},{7,5},{8,10},{9,15},{10,... | collective-permute-start | bytes 1572872 | tf_op jit(solution)/shard_map/ppermute | solution.py:381
  44.7 9.7 %collective-permute-start.6 = (bf16[5,64,256]{2,1,0:T(8,128)(2,1)S(1)}, bf16[5,64,256]{2,1,0:T(8,128)(2,1)S(1)}, u32[]{:S(2)}, u32[]{:S(2)}) collective-permute-start(bf16[5,64,256]{2,1,0:T(8,128)(2,1)S(1)} %get-tuple-element.44), channel_id=1, source_target_pairs={{0,1},{1,0},{2,3},{3,2},{4,5},{5,4},{6,7},{7,6},{8,9},{9,8},{10,11... | collective-permute-start | bytes 491528 | tf_op jit(solution)/shard_map/ppermute | solution.py:381

commit v7 on v6

--- a/solution.py
+++ b/solution.py
@@ -17,8 +17,8 @@
 VMEM = pl.BlockSpec(memory_space=pltpu.VMEM)
 ANY = pl.BlockSpec(memory_space=pl.ANY)
 
-EARLY = ((0, 0), (0, 1), (3, 0), (3, 1), (1, 1))
-LATE = ((1, 0), (2, 1), (2, 0))
+EARLY = ((0, 0), (0, 1), (1, 0), (1, 1), (3, 1))
+LATE = ((3, 0), (2, 0), (2, 1))
 
 
 def project_kernel(count, prior, *refs):
@@ -386,18 +386,18 @@
 ):
     members = lax.axis_size("sp")
     tps = lax.axis_size("tp")
-    ahead = [(i, (i + 2 - 4 * (i % 2)) % tps) for i in range(tps)]
-    back = [(i, (i - 2 + 4 * (i % 2)) % tps) for i in range(tps)]
+    ahead = [(i, (i - 2 + 4 * (i % 2)) % tps) for i in range(tps)]
+    back = [(i, (i + 2 - 4 * (i % 2)) % tps) for i in range(tps)]
     swap = [(i, i ^ 1) for i in range(tps)]
     gain = norm_gain.reshape(1, -1)
     half, width = tokens.shape[1:]
-    from_3 = shift(tokens, ahead)
+    whole = shift(tokens, ahead)
     a_0, b_0 = split(tokens)
-    b_1 = shift(b_0, back)
-    a_1 = shift(a_0, back)
-    b_2 = shift(b_1, back)
-    a_3 = from_3[0]
-    a_2 = shift(a_3, ahead)
+    b_far = shift(b_0, back)
+    a_far = shift(a_0, back)
+    b_2 = shift(b_far, back)
+    a_half = whole[0]
+    a_2 = shift(a_half, ahead)
     wo = jnp.concatenate([key_weight, value_weight], axis=1)
     wp = shift(wo, swap)
 
@@ -410,12 +410,12 @@
     rows = (2 * half, width)
     done = project((tokens.reshape(rows),), gain, wo, wp, half)
     own1, par1 = project(
-        (from_3.reshape(rows), b_1), gain, wo, wp, half, done
+        (whole.reshape(rows), b_far), gain, wo, wp, half, done
     )
     got1 = shift(par1, swap)
-    done = project((a_1, b_2), gain, wo, wp, half)
+    done = project((a_far, a_2), gain, wo, wp, half)
     keys, values, state = early(own1, got1, gates, qm)
-    own2, par2 = finish((a_2,), *done, gain, wo, wp)
+    own2, par2 = finish((b_2,), *done, gain, wo, wp)
     pairs = [[i, i + 1] for i in range(0, tps, 2)]
     both2 = lax.all_gather(par2, "tp", axis_index_groups=pairs)
     keys, values, part = late(

time: 69.8 us -> 71.4 us (1.023)
  the two profiles are of different devices: /device:TPU:1 before, /device:TPU:6 now
where the time goes in v7:
time: 71.4 us; the launch traced here: 71 us
  starting transfers between devices  28.2 us (39%)
  blocking collectives  18.1 us (25%)
  waiting for transfers between devices  12.9 us (18%)
  Pallas kernels  9.02 us (13%)
  local copies, waits for them, and re-layouts  1.75 us (2%)
  between operations  0.93 us (1%)
    ppermute x7, starting transfers between devices, shift(): return lax.ppermute(x, 'tp', by)  28.2 us
    all_to_all x1, blocking collectives, body(): parts = lax.all_to_all(part, 'sp', split_axis=0, concat_axis=0, tiled=True)  16.2 us
    ppermute x7, waiting for transfers between devices, shift(): return lax.ppermute(x, 'tp', by)  12.9 us
    pallas_call x3, Pallas kernels, project(): pl.pallas_call(functools.partial(project_kernel, len(xs), bool(before)),...  4.89 us
    all_gather x1, blocking collectives, body(): both2 = lax.all_gather(par2, 'tp', axis_index_groups=pairs)  1.95 us
    unnamed x17, local copies, waits for them, and re-layouts  1.45 us
  transfers between devices with their start and end apart: 7, of which 2 were waited for; matrix products, arithmetic and copies ran while one was open for 2% of the time, Pallas kernels for 9%

profile of v7, /device:TPU:6, one launch (start us, length us, event | category | flops | bytes accessed | tf_op | source)
XLA Modules:
  0.0 71.0 jit_solution(18059124163144838091)
XLA Ops:
  0.6 0.0 copy-start
  0.6 0.0 copy-start.6
  0.7 2.9 %collective-permute-start.3 = (bf16[2,64,4096]{2,1,0:T(8,128)(2,1)}, bf16[2,64,4096]{2,1,0:T(8,128)(2,1)S(1)}, u32[]{:S(2)}, u32[]{:S(2)}) collective-permute-start(bf16[2,64,4096]{2,1,0:T(8,128)(2,1)} %tokens.1), channel_id=1, source_target_pairs={{0,6},{1,3},{2,0},{3,5},{4,2},{5,7},{6,4},{7,1},{8,14},{9,11},{10,... | collective-permute-start | bytes 3145736 | tf_op jit(solution)/shard_map/ppermute | solution.py:381
  3.5 1.4 %constant_dynamic-update-slice_fusion.1 = bf16[4096,256]{1,0:T(8,128)(2,1)S(1)} fusion(bf16[4096,128]{1,0:T(8,128)(2,1)} %param.11), kind=kLoop, calls=%fused_computation.2 | loop fusion | bytes 2097152
  4.9 0.0 copy-done.6
  4.9 0.0 copy-start.7
  5.0 0.0 copy-start.1
  5.0 0.0 copy-start.2
  5.0 0.0 copy-start.3
  5.0 0.0 copy-start.4
  5.0 0.0 copy-start.5
  5.0 0.2 constant_dynamic-update-slice_fusion.refs_3_.refs_4_.refs_2_.refs_5_
  5.3 1.9 %collective-permute-start.5 = (bf16[4096,256]{1,0:T(8,128)(2,1)S(1)}, bf16[4096,256]{1,0:T(8,128)(2,1)S(1)}, u32[]{:S(2)}, u32[]{:S(2)}) collective-permute-start(bf16[4096,256]{1,0:T(8,128)(2,1)S(1)} %constant_dynamic-update-slice_fusion.refs_3_.refs_4_.refs_2_.refs_5_), channel_id=1, source_target_pairs={{0,1},{1,0},{2,3},{3,2},{4,5},{5,4},{6,7},{7,6},{8,9},{9,8},{10,11... | collective-permute-start | bytes 6291464 | tf_op jit(solution)/shard_map/ppermute | solution.py:381
  7.2 0.0 copy-done
  7.2 0.1 split.1
  7.3 10.6 %collective-permute-start = (bf16[64,4096]{1,0:T(8,128)(2,1)S(1)}, bf16[64,4096]{1,0:T(8,128)(2,1)S(1)}, u32[]{:S(2)}, u32[]{:S(2)}) collective-permute-start(bf16[64,4096]{1,0:T(8,128)(2,1)S(1)} %get-tuple-element.27), channel_id=1, source_target_pairs={{0,2},{1,7},{2,4},{3,1},{4,6},{5,3},{6,0},{7,5},{8,10},{9,15},{10,... | collective-permute-start | bytes 1572872 | tf_op jit(solution)/shard_map/ppermute | solution.py:381
  17.9 3.9 %collective-permute-start.2 = (bf16[64,4096]{1,0:T(8,128)(2,1)S(1)}, bf16[64,4096]{1,0:T(8,128)(2,1)S(1)}, u32[]{:S(2)}, u32[]{:S(2)}) collective-permute-start(bf16[64,4096]{1,0:T(8,128)(2,1)S(1)} %get-tuple-element.28), channel_id=1, source_target_pairs={{0,2},{1,7},{2,4},{3,1},{4,6},{5,3},{6,0},{7,5},{8,10},{9,15},{10,... | collective-permute-start | bytes 1572872 | tf_op jit(solution)/shard_map/ppermute | solution.py:381
  21.8 9.3 %collective-permute-done.3 = bf16[2,64,4096]{2,1,0:T(8,128)(2,1)S(1)} collective-permute-done((bf16[2,64,4096]{2,1,0:T(8,128)(2,1)}, bf16[2,64,4096]{2,1,0:T(8,128)(2,1)S(1)}, u32[]{:S(2)}, u32[]{:S(2)}) %collective-permute-start.3) | collective-permute-done | bytes 1048608 | tf_op jit(solution)/shard_map/ppermute | solution.py:381
  31.1 1.9 %collective-permute-start.4 = (bf16[64,4096]{1,0:T(8,128)(2,1)S(1)}, bf16[64,4096]{1,0:T(8,128)(2,1)S(1)}, u32[]{:S(2)}, u32[]{:S(2)}) collective-permute-start(bf16[64,4096]{1,0:T(8,128)(2,1)S(1)} %slice_bitcast_fusion), channel_id=1, source_target_pairs={{0,6},{1,3},{2,0},{3,5},{4,2},{5,7},{6,4},{7,1},{8,14},{9,11},{10,... | collective-permute-start | bytes 1572872 | tf_op jit(solution)/shard_map/ppermute | solution.py:381
  33.0 0.0 collective-permute-done.refs_1_
  33.1 5.1 %collective-permute-start.1 = (bf16[64,4096]{1,0:T(8,128)(2,1)S(1)}, bf16[64,4096]{1,0:T(8,128)(2,1)S(1)}, u32[]{:S(2)}, u32[]{:S(2)}) collective-permute-start(bf16[64,4096]{1,0:T(8,128)(2,1)S(1)} %collective-permute-done.refs_1_), channel_id=1, source_target_pairs={{0,2},{1,7},{2,4},{3,1},{4,6},{5,3},{6,0},{7,5},{8,10},{9,15},{10,... | collective-permute-start | bytes 1572872 | tf_op jit(solution)/shard_map/ppermute | solution.py:381
  38.2 0.0 copy-done.7
  38.2 0.0 copy-done.1
  38.2 0.0 copy-done.2
  38.2 0.0 copy-done.3
  38.3 0.0 copy-done.4
  38.3 0.0 copy-done.5
  38.3 0.3 prepare.1
  38.5 0.0 collective-permute-done.5.refs_4_.refs_5_.refs_3_.refs_6_
  38.6 1.4 %project.4 = (bf16[2,64,256]{2,1,0:T(8,128)(2,1)S(1)}, bf16[2,64,256]{2,1,0:T(8,128)(2,1)S(1)}) custom-call(bf16[128,4096]{1,0:T(8,128)(2,1)S(1)} %bitcast.6, bf16[1,4096]{1,0:T(2,128)(2,1)S(1)} %reshape.15.refs_2_.refs_3_.refs_1_.refs_4_, bf16[4096,256]{1,0:T(8,128)(2,1)S(1)} %constant_dynamic-update-slice_fusion.refs_3_.refs_4_.refs_2_.refs_5_, ...), custom_call_target="tpu_custom_call" | custom-call | flops 536870912 | bytes 6291456 | tf_op jit(solution)/shard_map/project/pallas_call | solution.py:119
  40.0 2.0 %project.5 = (bf16[5,64,256]{2,1,0:T(8,128)(2,1)S(1)}, bf16[5,64,256]{2,1,0:T(8,128)(2,1)S(1)}) custom-call(bf16[128,4096]{1,0:T(8,128)(2,1)S(1)} %bitcast.7, bf16[64,4096]{1,0:T(8,128)(2,1)S(1)} %collective-permute-done.refs_1_, bf16[2,64,256]{2,1,0:T(8,128)(2,1)S(1)} %get-tuple-element.41.refs_2_, bf16[2,64,256]{2,1,0:T(8,128)(2,1)S(1)} %get-tuple-element.42.refs_3_, ...), custom_call_target="tpu_custom_call" | custom-call | flops 805306368 | bytes 6291456 | tf_op jit(solution)/shard_map/project/pallas_call | solution.py:119
  42.0 1.9 %collective-permute-start.6 = (bf16[5,64,256]{2,1,0:T(8,128)(2,1)S(1)}, bf16[5,64,256]{2,1,0:T(8,128)(2,1)S(1)}, u32[]{:S(2)}, u32[]{:S(2)}) collective-permute-start(bf16[5,64,256]{2,1,0:T(8,128)(2,1)S(1)} %get-tuple-element.44), channel_id=1, source_target_pairs={{0,1},{1,0},{2,3},{3,2},{4,5},{5,4},{6,7},{7,6},{8,9},{9,8},{10,11... | collective-permute-start | bytes 491528 | tf_op jit(solution)/shard_map/ppermute | solution.py:381
  44.0 0.0 collective-permute-done.2.refs_0_
  44.0 3.6 %collective-permute-done.4.refs_1_ = bf16[64,4096]{1,0:T(8,128)(2,1)S(1)} collective-permute-done((bf16[64,4096]{1,0:T(8,128)(2,1)S(1)}, bf16[64,4096]{1,0:T(8,128)(2,1)S(1)}, u32[]{:S(2)}, u32[]{:S(2)}) %collective-permute-start.4) | collective-permute-done | bytes 524320 | tf_op jit(solution)/shard_map/ppermute | solution.py:381
  47.6 1.4 %project.3 = (bf16[2,64,256]{2,1,0:T(8,128)(2,1)S(1)}, bf16[2,64,256]{2,1,0:T(8,128)(2,1)S(1)}) custom-call(bf16[64,4096]{1,0:T(8,128)(2,1)S(1)} %collective-permute-done.2.refs_0_, bf16[64,4096]{1,0:T(8,128)(2,1)S(1)} %collective-permute-done.4.refs_1_, bf16[1,4096]{1,0:T(2,128)(2,1)S(1)} %reshape.15.refs_2_.refs_3_.refs_1_.refs_4_, ...), custom_call_target="tpu_custom_call" | custom-call | flops 536870912 | bytes 6291456 | tf_op jit(solution)/shard_map/project/pallas_call | solution.py:119
  49.0 0.0 collective-permute-done.1.refs_0_
  49.0 1.0 %finish.1 = (bf16[3,64,256]{2,1,0:T(8,128)(2,1)S(1)}, bf16[3,64,256]{2,1,0:T(8,128)(2,1)S(1)}) custom-call(bf16[64,4096]{1,0:T(8,128)(2,1)S(1)} %collective-permute-done.1.refs_0_, bf16[2,64,256]{2,1,0:T(8,128)(2,1)S(1)} %get-tuple-element.34.refs_1_, bf16[2,64,256]{2,1,0:T(8,128)(2,1)S(1)} %get-tuple-element.35.refs_2_, ...), custom_call_target="tpu_custom_call" | custom-call | flops 268435456 | bytes 6291456 | tf_op jit(solution)/shard_map/finish/pallas_call | solution.py:98
  50.0 1.9 %all-gather = bf16[6,64,256]{2,1,0:T(8,128)(2,1)S(1)} all-gather(bf16[3,64,256]{2,1,0:T(8,128)(2,1)S(1)} %get-tuple-element.37), channel_id=2, replica_groups={{0,1},{2,3},{4,5},{6,7},{8,9},{10,11},{12,13},{14,15},{16,17},{18,19},{..., dimensions={0}, use_global_device_ids=true | all-gather | bytes 294912 | tf_op jit(solution)/shard_map/all_gather | solution.py:420
  52.0 0.0 collective-permute-done.6.got
  52.0 1.1 %early.1 = (bf16[2,512,128]{2,1,0:T(8,128)(2,1)}, bf16[2,512,128]{2,1,0:T(8,128)(2,1)}, f32[8,128]{1,0:T(8,128)S(1)}) custom-call(bf16[5,64,256]{2,1,0:T(8,128)(2,1)S(1)} %get-tuple-element.43.own, bf16[5,64,256]{2,1,0:T(8,128)(2,1)S(1)} %collective-permute-done.6.got, f32[2,512,128]{2,1,0:T(8,128)S(1)} %get-tuple-element.38.gates, ...), custom_call_target="tpu_custom_call" | custom-call | flops 67108864 | bytes 2097152 | tf_op jit(solution)/shard_map/early/pallas_call | solution.py:231
  53.1 1.0 %late.1 = (bf16[2,512,128]{2,1,0:T(8,128)(2,1)}, bf16[2,512,128]{2,1,0:T(8,128)(2,1)}, f32[32,1,384]{2,1,0:T(1,128)S(1)}) custom-call(bf16[3,64,256]{2,1,0:T(8,128)(2,1)S(1)} %get-tuple-element.36.own, bf16[2,3,64,256]{3,2,1,0:T(8,128)(2,1)S(1)} %bitcast.8, ...), custom_call_target="tpu_custom_call", output_to_operand_aliasing={{0}: (6, {}), {1}: (7, {})} | custom-call | flops 16777216 | bytes 1048576 | tf_op jit(solution)/shard_map/late/pallas_call | solution.py:301
  54.0 16.2 %all_to_all.5.parts = f32[32,1,384]{2,1,0:T(1,128)S(1)} all-to-all(f32[32,1,384]{2,1,0:T(1,128)S(1)} %get-tuple-element.48), channel_id=1, replica_groups=mesh['gr'=3,'sp'=32,'tp'=8] {'sp'}, dimensions={0} | all-to-all | bytes 98304 | tf_op jit(solution)/shard_map/all_to_all | solution.py:424
  70.2 0.8 %merge.1 = (bf16[2,512,128]{2,1,0:T(8,128)(2,1)}, bf16[2,512,128]{2,1,0:T(8,128)(2,1)}, bf16[2,128]{1,0:T(2,128)(2,1)}) custom-call(f32[32,1,384]{2,1,0:T(1,128)S(1)} %all_to_all.5.parts, bf16[3,64,256]{2,1,0:T(8,128)(2,1)S(1)} %get-tuple-element.36.own, bf16[2,3,64,256]{3,2,1,0:T(8,128)(2,1)S(1)} %bitcast.9, ...), custom_call_target="tpu_custom_call", output_to_operand_aliasing={{0}: (3, {}), {1}: (4, {})} | custom-call | tf_op jit(solution)/shard_map/merge/pallas_call | solution.py:348
  (2 shorter events, 0.0 us)
Async XLA Ops:
  0.6 6.6 %copy-start = (bf16[2,64,4096]{2,1,0:T(8,128)(2,1)S(1)}, bf16[2,64,4096]{2,1,0:T(8,128)(2,1)}, u32[]{:S(2)}) copy-start(bf16[2,64,4096]{2,1,0:T(8,128)(2,1)} %tokens.1) | copy-start | bytes 3145732
  0.6 4.3 %copy-start.6 = (bf16[4096,128]{1,0:T(8,128)(2,1)S(1)}, bf16[4096,128]{1,0:T(8,128)(2,1)}, u32[]{:S(2)}) copy-start(bf16[4096,128]{1,0:T(8,128)(2,1)} %param.12) | copy-start | bytes 3145732
  0.7 30.4 %collective-permute-start.3 = (bf16[2,64,4096]{2,1,0:T(8,128)(2,1)}, bf16[2,64,4096]{2,1,0:T(8,128)(2,1)S(1)}, u32[]{:S(2)}, u32[]{:S(2)}) collective-permute-start(bf16[2,64,4096]{2,1,0:T(8,128)(2,1)} %tokens.1), channel_id=1, source_target_pairs={{0,6},{1,3},{2,0},{3,5},{4,2},{5,7},{6,4},{7,1},{8,14},{9,11},{10,... | collective-permute-start | bytes 3145736 | tf_op jit(solution)/shard_map/ppermute | solution.py:381
  4.9 33.2 %copy-start.7 = (bf16[4096]{0:T(1024)(128)(2,1)S(1)}, bf16[4096]{0:T(1024)(128)(2,1)}, u32[]{:S(2)}) copy-start(bf16[4096]{0:T(1024)(128)(2,1)} %param.10) | copy-start | bytes 24580
  5.0 33.3 %copy-start.1 = (f32[2,512,2]{1,2,0:T(2,128)S(1)}, f32[2,512,2]{1,2,0:T(2,128)}, u32[]{:S(2)}) copy-start(f32[2,512,2]{1,2,0:T(2,128)} %param.13) | copy-start | bytes 24580
  5.0 33.3 %copy-start.2 = (f32[2,2]{1,0:T(2,128)S(1)}, f32[2,2]{1,0:T(2,128)}, u32[]{:S(2)}) copy-start(f32[2,2]{1,0:T(2,128)} %ng.1) | copy-start | bytes 52
  5.0 33.3 %copy-start.3 = (bf16[2,128]{1,0:T(2,128)(2,1)S(1)}, bf16[2,128]{1,0:T(2,128)(2,1)}, u32[]{:S(2)}) copy-start(bf16[2,128]{1,0:T(2,128)(2,1)} %q.1) | copy-start | bytes 1540
  5.0 33.3 %copy-start.4 = (bf16[2,128]{1,0:T(2,128)(2,1)S(1)}, bf16[2,128]{1,0:T(2,128)(2,1)}, u32[]{:S(2)}) copy-start(bf16[2,128]{1,0:T(2,128)(2,1)} %fk.1) | copy-start | bytes 1540
  5.0 33.3 %copy-start.5 = (bf16[2,128]{1,0:T(2,128)(2,1)S(1)}, bf16[2,128]{1,0:T(2,128)(2,1)}, u32[]{:S(2)}) copy-start(bf16[2,128]{1,0:T(2,128)(2,1)} %fv.1) | copy-start | bytes 1540
  5.3 33.3 %collective-permute-start.5 = (bf16[4096,256]{1,0:T(8,128)(2,1)S(1)}, bf16[4096,256]{1,0:T(8,128)(2,1)S(1)}, u32[]{:S(2)}, u32[]{:S(2)}) collective-permute-start(bf16[4096,256]{1,0:T(8,128)(2,1)S(1)} %constant_dynamic-update-slice_fusion.refs_3_.refs_4_.refs_2_.refs_5_), channel_id=1, source_target_pairs={{0,1},{1,0},{2,3},{3,2},{4,5},{5,4},{6,7},{7,6},{8,9},{9,8},{10,11... | collective-permute-start | bytes 6291464 | tf_op jit(solution)/shard_map/ppermute | solution.py:381
  7.3 25.8 %collective-permute-start = (bf16[64,4096]{1,0:T(8,128)(2,1)S(1)}, bf16[64,4096]{1,0:T(8,128)(2,1)S(1)}, u32[]{:S(2)}, u32[]{:S(2)}) collective-permute-start(bf16[64,4096]{1,0:T(8,128)(2,1)S(1)} %get-tuple-element.27), channel_id=1, source_target_pairs={{0,2},{1,7},{2,4},{3,1},{4,6},{5,3},{6,0},{7,5},{8,10},{9,15},{10,... | collective-permute-start | bytes 1572872 | tf_op jit(solution)/shard_map/ppermute | solution.py:381
  17.9 26.1 %collective-permute-start.2 = (bf16[64,4096]{1,0:T(8,128)(2,1)S(1)}, bf16[64,4096]{1,0:T(8,128)(2,1)S(1)}, u32[]{:S(2)}, u32[]{:S(2)}) collective-permute-start(bf16[64,4096]{1,0:T(8,128)(2,1)S(1)} %get-tuple-element.28), channel_id=1, source_target_pairs={{0,2},{1,7},{2,4},{3,1},{4,6},{5,3},{6,0},{7,5},{8,10},{9,15},{10,... | collective-permute-start | bytes 1572872 | tf_op jit(solution)/shard_map/ppermute | solution.py:381
  31.1 16.5 %collective-permute-start.4 = (bf16[64,4096]{1,0:T(8,128)(2,1)S(1)}, bf16[64,4096]{1,0:T(8,128)(2,1)S(1)}, u32[]{:S(2)}, u32[]{:S(2)}) collective-permute-start(bf16[64,4096]{1,0:T(8,128)(2,1)S(1)} %slice_bitcast_fusion), channel_id=1, source_target_pairs={{0,6},{1,3},{2,0},{3,5},{4,2},{5,7},{6,4},{7,1},{8,14},{9,11},{10,... | collective-permute-start | bytes 1572872 | tf_op jit(solution)/shard_map/ppermute | solution.py:381
  33.1 16.0 %collective-permute-start.1 = (bf16[64,4096]{1,0:T(8,128)(2,1)S(1)}, bf16[64,4096]{1,0:T(8,128)(2,1)S(1)}, u32[]{:S(2)}, u32[]{:S(2)}) collective-permute-start(bf16[64,4096]{1,0:T(8,128)(2,1)S(1)} %collective-permute-done.refs_1_), channel_id=1, source_target_pairs={{0,2},{1,7},{2,4},{3,1},{4,6},{5,3},{6,0},{7,5},{8,10},{9,15},{10,... | collective-permute-start | bytes 1572872 | tf_op jit(solution)/shard_map/ppermute | solution.py:381
  42.0 9.9 %collective-permute-start.6 = (bf16[5,64,256]{2,1,0:T(8,128)(2,1)S(1)}, bf16[5,64,256]{2,1,0:T(8,128)(2,1)S(1)}, u32[]{:S(2)}, u32[]{:S(2)}) collective-permute-start(bf16[5,64,256]{2,1,0:T(8,128)(2,1)S(1)} %get-tuple-element.44), channel_id=1, source_target_pairs={{0,1},{1,0},{2,3},{3,2},{4,5},{5,4},{6,7},{7,6},{8,9},{9,8},{10,11... | collective-permute-start | bytes 491528 | tf_op jit(solution)/shard_map/ppermute | solution.py:381

commit v8 on v6

--- a/solution.py
+++ b/solution.py
@@ -18,7 +18,7 @@
 ANY = pl.BlockSpec(memory_space=pl.ANY)
 
 EARLY = ((0, 0), (0, 1), (3, 0), (3, 1), (1, 1))
-LATE = ((1, 0), (2, 1), (2, 0))
+LATE = ((1, 0), (2, 0), (2, 1))
 
 
 def project_kernel(count, prior, *refs):
@@ -413,9 +413,9 @@
         (from_3.reshape(rows), b_1), gain, wo, wp, half, done
     )
     got1 = shift(par1, swap)
-    done = project((a_1, b_2), gain, wo, wp, half)
+    done = project((a_1, a_2), gain, wo, wp, half)
     keys, values, state = early(own1, got1, gates, qm)
-    own2, par2 = finish((a_2,), *done, gain, wo, wp)
+    own2, par2 = finish((b_2,), *done, gain, wo, wp)
     pairs = [[i, i + 1] for i in range(0, tps, 2)]
     both2 = lax.all_gather(par2, "tp", axis_index_groups=pairs)
     keys, values, part = late(

time: 69.8 us -> 71.2 us (1.020)
  waiting for transfers between devices: 16.9 us -> 8.95 us
  starting transfers between devices: 26.7 us -> 33.2 us
  blocking collectives: 14.1 us -> 17 us
    ppermute x7, waiting for transfers between devices: 16.9 us -> 8.95 us  [shift(): return lax.ppermute(x, 'tp', by)]
    ppermute x7, starting transfers between devices: 26.7 us -> 33.2 us  [shift(): return lax.ppermute(x, 'tp', by)]
    all_gather x1, blocking collectives: 1.96 us -> 4.84 us  [body(): both2 = lax.all_gather(par2, 'tp', axis_index_groups=pairs)]
where the time goes in v8:
time: 71.2 us; the launch traced here: 70.8 us
  starting transfers between devices  33.2 us (47%)
  blocking collectives  17 us (24%)
  Pallas kernels  9.02 us (13%)
  waiting for transfers between devices  8.95 us (13%)
  local copies, waits for them, and re-layouts  1.75 us (2%)
  between operations  0.94 us (1%)
    ppermute x7, starting transfers between devices, shift(): return lax.ppermute(x, 'tp', by)  33.2 us
    all_to_all x1, blocking collectives, body(): parts = lax.all_to_all(part, 'sp', split_axis=0, concat_axis=0, tiled=True)  12.1 us
    ppermute x7, waiting for transfers between devices, shift(): return lax.ppermute(x, 'tp', by)  8.95 us
    pallas_call x3, Pallas kernels, project(): pl.pallas_call(functools.partial(project_kernel, len(xs), bool(before)),...  4.9 us
    all_gather x1, blocking collectives, body(): both2 = lax.all_gather(par2, 'tp', axis_index_groups=pairs)  4.84 us
    unnamed x17, local copies, waits for them, and re-layouts  1.45 us
  transfers between devices with their start and end apart: 7, of which 2 were waited for; matrix products, arithmetic and copies ran while one was open for 2% of the time, Pallas kernels for 9%

profile of v8, /device:TPU:1, one launch (start us, length us, event | category | flops | bytes accessed | tf_op | source)
XLA Modules:
  0.0 70.8 jit_solution(324349607738334302)
XLA Ops:
  0.6 0.0 copy-start
  0.6 0.0 copy-start.6
  0.7 5.3 %collective-permute-start.3 = (bf16[2,64,4096]{2,1,0:T(8,128)(2,1)}, bf16[2,64,4096]{2,1,0:T(8,128)(2,1)S(1)}, u32[]{:S(2)}, u32[]{:S(2)}) collective-permute-start(bf16[2,64,4096]{2,1,0:T(8,128)(2,1)} %tokens.1), channel_id=1, source_target_pairs={{0,2},{1,7},{2,4},{3,1},{4,6},{5,3},{6,0},{7,5},{8,10},{9,15},{10,... | collective-permute-start | bytes 3145736 | tf_op jit(solution)/shard_map/ppermute | solution.py:381
  6.0 1.4 %constant_dynamic-update-slice_fusion.1 = bf16[4096,256]{1,0:T(8,128)(2,1)S(1)} fusion(bf16[4096,128]{1,0:T(8,128)(2,1)} %param.11), kind=kLoop, calls=%fused_computation.2 | loop fusion | bytes 2097152
  7.4 0.0 copy-done.6
  7.4 0.0 copy-start.7
  7.4 0.0 copy-start.1
  7.4 0.0 copy-start.2
  7.4 0.0 copy-start.3
  7.5 0.0 copy-start.4
  7.5 0.0 copy-start.5
  7.5 0.2 constant_dynamic-update-slice_fusion.refs_3_.refs_4_.refs_2_.refs_5_
  7.7 9.1 %collective-permute-start.5 = (bf16[4096,256]{1,0:T(8,128)(2,1)S(1)}, bf16[4096,256]{1,0:T(8,128)(2,1)S(1)}, u32[]{:S(2)}, u32[]{:S(2)}) collective-permute-start(bf16[4096,256]{1,0:T(8,128)(2,1)S(1)} %constant_dynamic-update-slice_fusion.refs_3_.refs_4_.refs_2_.refs_5_), channel_id=1, source_target_pairs={{0,1},{1,0},{2,3},{3,2},{4,5},{5,4},{6,7},{7,6},{8,9},{9,8},{10,11... | collective-permute-start | bytes 6291464 | tf_op jit(solution)/shard_map/ppermute | solution.py:381
  16.9 0.0 copy-done
  16.9 0.1 split.1
  16.9 1.9 %collective-permute-start = (bf16[64,4096]{1,0:T(8,128)(2,1)S(1)}, bf16[64,4096]{1,0:T(8,128)(2,1)S(1)}, u32[]{:S(2)}, u32[]{:S(2)}) collective-permute-start(bf16[64,4096]{1,0:T(8,128)(2,1)S(1)} %get-tuple-element.27), channel_id=1, source_target_pairs={{0,6},{1,3},{2,0},{3,5},{4,2},{5,7},{6,4},{7,1},{8,14},{9,11},{10,... | collective-permute-start | bytes 1572872 | tf_op jit(solution)/shard_map/ppermute | solution.py:381
  18.9 1.9 %collective-permute-start.2 = (bf16[64,4096]{1,0:T(8,128)(2,1)S(1)}, bf16[64,4096]{1,0:T(8,128)(2,1)S(1)}, u32[]{:S(2)}, u32[]{:S(2)}) collective-permute-start(bf16[64,4096]{1,0:T(8,128)(2,1)S(1)} %get-tuple-element.28), channel_id=1, source_target_pairs={{0,6},{1,3},{2,0},{3,5},{4,2},{5,7},{6,4},{7,1},{8,14},{9,11},{10,... | collective-permute-start | bytes 1572872 | tf_op jit(solution)/shard_map/ppermute | solution.py:381
  20.8 0.0 collective-permute-done.3
  20.9 4.9 %collective-permute-start.4 = (bf16[64,4096]{1,0:T(8,128)(2,1)S(1)}, bf16[64,4096]{1,0:T(8,128)(2,1)S(1)}, u32[]{:S(2)}, u32[]{:S(2)}) collective-permute-start(bf16[64,4096]{1,0:T(8,128)(2,1)S(1)} %slice_bitcast_fusion), channel_id=1, source_target_pairs={{0,2},{1,7},{2,4},{3,1},{4,6},{5,3},{6,0},{7,5},{8,10},{9,15},{10,... | collective-permute-start | bytes 1572872 | tf_op jit(solution)/shard_map/ppermute | solution.py:381
  25.7 8.6 %collective-permute-done.refs_1_ = bf16[64,4096]{1,0:T(8,128)(2,1)S(1)} collective-permute-done((bf16[64,4096]{1,0:T(8,128)(2,1)S(1)}, bf16[64,4096]{1,0:T(8,128)(2,1)S(1)}, u32[]{:S(2)}, u32[]{:S(2)}) %collective-permute-start) | collective-permute-done | bytes 524320 | tf_op jit(solution)/shard_map/ppermute | solution.py:381
  34.3 1.9 %collective-permute-start.1 = (bf16[64,4096]{1,0:T(8,128)(2,1)S(1)}, bf16[64,4096]{1,0:T(8,128)(2,1)S(1)}, u32[]{:S(2)}, u32[]{:S(2)}) collective-permute-start(bf16[64,4096]{1,0:T(8,128)(2,1)S(1)} %collective-permute-done.refs_1_), channel_id=1, source_target_pairs={{0,6},{1,3},{2,0},{3,5},{4,2},{5,7},{6,4},{7,1},{8,14},{9,11},{10,... | collective-permute-start | bytes 1572872 | tf_op jit(solution)/shard_map/ppermute | solution.py:381
  36.2 0.0 copy-done.7
  36.2 0.0 copy-done.1
  36.2 0.0 copy-done.2
  36.2 0.0 copy-done.3
  36.2 0.0 copy-done.4
  36.3 0.0 copy-done.5
  36.3 0.3 prepare.1
  36.5 0.0 collective-permute-done.5.refs_4_.refs_5_.refs_3_.refs_6_
  36.5 1.4 %project.4 = (bf16[2,64,256]{2,1,0:T(8,128)(2,1)S(1)}, bf16[2,64,256]{2,1,0:T(8,128)(2,1)S(1)}) custom-call(bf16[128,4096]{1,0:T(8,128)(2,1)S(1)} %bitcast.6, bf16[1,4096]{1,0:T(2,128)(2,1)S(1)} %reshape.15.refs_2_.refs_3_.refs_1_.refs_4_, bf16[4096,256]{1,0:T(8,128)(2,1)S(1)} %constant_dynamic-update-slice_fusion.refs_3_.refs_4_.refs_2_.refs_5_, ...), custom_call_target="tpu_custom_call" | custom-call | flops 536870912 | bytes 6291456 | tf_op jit(solution)/shard_map/project/pallas_call | solution.py:119
  38.0 2.0 %project.5 = (bf16[5,64,256]{2,1,0:T(8,128)(2,1)S(1)}, bf16[5,64,256]{2,1,0:T(8,128)(2,1)S(1)}) custom-call(bf16[128,4096]{1,0:T(8,128)(2,1)S(1)} %bitcast.7, bf16[64,4096]{1,0:T(8,128)(2,1)S(1)} %collective-permute-done.refs_1_, bf16[2,64,256]{2,1,0:T(8,128)(2,1)S(1)} %get-tuple-element.41.refs_2_, bf16[2,64,256]{2,1,0:T(8,128)(2,1)S(1)} %get-tuple-element.42.refs_3_, ...), custom_call_target="tpu_custom_call" | custom-call | flops 805306368 | bytes 6291456 | tf_op jit(solution)/shard_map/project/pallas_call | solution.py:119
  40.0 8.2 %collective-permute-start.6 = (bf16[5,64,256]{2,1,0:T(8,128)(2,1)S(1)}, bf16[5,64,256]{2,1,0:T(8,128)(2,1)S(1)}, u32[]{:S(2)}, u32[]{:S(2)}) collective-permute-start(bf16[5,64,256]{2,1,0:T(8,128)(2,1)S(1)} %get-tuple-element.44), channel_id=1, source_target_pairs={{0,1},{1,0},{2,3},{3,2},{4,5},{5,4},{6,7},{7,6},{8,9},{9,8},{10,11... | collective-permute-start | bytes 491528 | tf_op jit(solution)/shard_map/ppermute | solution.py:381
  48.2 0.0 collective-permute-done.2.refs_0_
  48.2 0.0 collective-permute-done.4.refs_1_
  48.2 1.4 %project.3 = (bf16[2,64,256]{2,1,0:T(8,128)(2,1)S(1)}, bf16[2,64,256]{2,1,0:T(8,128)(2,1)S(1)}) custom-call(bf16[64,4096]{1,0:T(8,128)(2,1)S(1)} %collective-permute-done.2.refs_0_, bf16[64,4096]{1,0:T(8,128)(2,1)S(1)} %collective-permute-done.4.refs_1_, bf16[1,4096]{1,0:T(2,128)(2,1)S(1)} %reshape.15.refs_2_.refs_3_.refs_1_.refs_4_, ...), custom_call_target="tpu_custom_call" | custom-call | flops 536870912 | bytes 6291456 | tf_op jit(solution)/shard_map/project/pallas_call | solution.py:119
  49.7 0.4 collective-permute-done.1.refs_0_
  50.0 1.0 %finish.1 = (bf16[3,64,256]{2,1,0:T(8,128)(2,1)S(1)}, bf16[3,64,256]{2,1,0:T(8,128)(2,1)S(1)}) custom-call(bf16[64,4096]{1,0:T(8,128)(2,1)S(1)} %collective-permute-done.1.refs_0_, bf16[2,64,256]{2,1,0:T(8,128)(2,1)S(1)} %get-tuple-element.34.refs_1_, bf16[2,64,256]{2,1,0:T(8,128)(2,1)S(1)} %get-tuple-element.35.refs_2_, ...), custom_call_target="tpu_custom_call" | custom-call | flops 268435456 | bytes 6291456 | tf_op jit(solution)/shard_map/finish/pallas_call | solution.py:98
  51.0 4.8 %all-gather = bf16[6,64,256]{2,1,0:T(8,128)(2,1)S(1)} all-gather(bf16[3,64,256]{2,1,0:T(8,128)(2,1)S(1)} %get-tuple-element.37), channel_id=2, replica_groups={{0,1},{2,3},{4,5},{6,7},{8,9},{10,11},{12,13},{14,15},{16,17},{18,19},{..., dimensions={0}, use_global_device_ids=true | all-gather | bytes 294912 | tf_op jit(solution)/shard_map/all_gather | solution.py:420
  55.8 0.0 collective-permute-done.6.got
  55.8 1.1 %early.1 = (bf16[2,512,128]{2,1,0:T(8,128)(2,1)}, bf16[2,512,128]{2,1,0:T(8,128)(2,1)}, f32[8,128]{1,0:T(8,128)S(1)}) custom-call(bf16[5,64,256]{2,1,0:T(8,128)(2,1)S(1)} %get-tuple-element.43.own, bf16[5,64,256]{2,1,0:T(8,128)(2,1)S(1)} %collective-permute-done.6.got, f32[2,512,128]{2,1,0:T(8,128)S(1)} %get-tuple-element.38.gates, ...), custom_call_target="tpu_custom_call" | custom-call | flops 67108864 | bytes 2097152 | tf_op jit(solution)/shard_map/early/pallas_call | solution.py:231
  57.0 1.0 %late.1 = (bf16[2,512,128]{2,1,0:T(8,128)(2,1)}, bf16[2,512,128]{2,1,0:T(8,128)(2,1)}, f32[32,1,384]{2,1,0:T(1,128)S(1)}) custom-call(bf16[3,64,256]{2,1,0:T(8,128)(2,1)S(1)} %get-tuple-element.36.own, bf16[2,3,64,256]{3,2,1,0:T(8,128)(2,1)S(1)} %bitcast.8, ...), custom_call_target="tpu_custom_call", output_to_operand_aliasing={{0}: (6, {}), {1}: (7, {})} | custom-call | flops 16777216 | bytes 1048576 | tf_op jit(solution)/shard_map/late/pallas_call | solution.py:301
  57.9 12.1 %all_to_all.5.parts = f32[32,1,384]{2,1,0:T(1,128)S(1)} all-to-all(f32[32,1,384]{2,1,0:T(1,128)S(1)} %get-tuple-element.48), channel_id=1, replica_groups=mesh['gr'=3,'sp'=32,'tp'=8] {'sp'}, dimensions={0} | all-to-all | bytes 98304 | tf_op jit(solution)/shard_map/all_to_all | solution.py:424
  70.0 0.8 %merge.1 = (bf16[2,512,128]{2,1,0:T(8,128)(2,1)}, bf16[2,512,128]{2,1,0:T(8,128)(2,1)}, bf16[2,128]{1,0:T(2,128)(2,1)}) custom-call(f32[32,1,384]{2,1,0:T(1,128)S(1)} %all_to_all.5.parts, bf16[3,64,256]{2,1,0:T(8,128)(2,1)S(1)} %get-tuple-element.36.own, bf16[2,3,64,256]{3,2,1,0:T(8,128)(2,1)S(1)} %bitcast.9, ...), custom_call_target="tpu_custom_call", output_to_operand_aliasing={{0}: (3, {}), {1}: (4, {})} | custom-call | tf_op jit(solution)/shard_map/merge/pallas_call | solution.py:348
  (2 shorter events, 0.0 us)
Async XLA Ops:
  0.6 16.2 %copy-start = (bf16[2,64,4096]{2,1,0:T(8,128)(2,1)S(1)}, bf16[2,64,4096]{2,1,0:T(8,128)(2,1)}, u32[]{:S(2)}) copy-start(bf16[2,64,4096]{2,1,0:T(8,128)(2,1)} %tokens.1) | copy-start | bytes 3145732
  0.6 6.8 %copy-start.6 = (bf16[4096,128]{1,0:T(8,128)(2,1)S(1)}, bf16[4096,128]{1,0:T(8,128)(2,1)}, u32[]{:S(2)}) copy-start(bf16[4096,128]{1,0:T(8,128)(2,1)} %param.12) | copy-start | bytes 3145732
  0.7 20.1 %collective-permute-start.3 = (bf16[2,64,4096]{2,1,0:T(8,128)(2,1)}, bf16[2,64,4096]{2,1,0:T(8,128)(2,1)S(1)}, u32[]{:S(2)}, u32[]{:S(2)}) collective-permute-start(bf16[2,64,4096]{2,1,0:T(8,128)(2,1)} %tokens.1), channel_id=1, source_target_pairs={{0,2},{1,7},{2,4},{3,1},{4,6},{5,3},{6,0},{7,5},{8,10},{9,15},{10,... | collective-permute-start | bytes 3145736 | tf_op jit(solution)/shard_map/ppermute | solution.py:381
  7.4 28.8 %copy-start.7 = (bf16[4096]{0:T(1024)(128)(2,1)S(1)}, bf16[4096]{0:T(1024)(128)(2,1)}, u32[]{:S(2)}) copy-start(bf16[4096]{0:T(1024)(128)(2,1)} %param.10) | copy-start | bytes 24580
  7.4 28.8 %copy-start.1 = (f32[2,512,2]{1,2,0:T(2,128)S(1)}, f32[2,512,2]{1,2,0:T(2,128)}, u32[]{:S(2)}) copy-start(f32[2,512,2]{1,2,0:T(2,128)} %param.13) | copy-start | bytes 24580
  7.4 28.8 %copy-start.2 = (f32[2,2]{1,0:T(2,128)S(1)}, f32[2,2]{1,0:T(2,128)}, u32[]{:S(2)}) copy-start(f32[2,2]{1,0:T(2,128)} %ng.1) | copy-start | bytes 52
  7.4 28.8 %copy-start.3 = (bf16[2,128]{1,0:T(2,128)(2,1)S(1)}, bf16[2,128]{1,0:T(2,128)(2,1)}, u32[]{:S(2)}) copy-start(bf16[2,128]{1,0:T(2,128)(2,1)} %q.1) | copy-start | bytes 1540
  7.5 28.8 %copy-start.4 = (bf16[2,128]{1,0:T(2,128)(2,1)S(1)}, bf16[2,128]{1,0:T(2,128)(2,1)}, u32[]{:S(2)}) copy-start(bf16[2,128]{1,0:T(2,128)(2,1)} %fk.1) | copy-start | bytes 1540
  7.5 28.8 %copy-start.5 = (bf16[2,128]{1,0:T(2,128)(2,1)S(1)}, bf16[2,128]{1,0:T(2,128)(2,1)}, u32[]{:S(2)}) copy-start(bf16[2,128]{1,0:T(2,128)(2,1)} %fv.1) | copy-start | bytes 1540
  7.7 28.8 %collective-permute-start.5 = (bf16[4096,256]{1,0:T(8,128)(2,1)S(1)}, bf16[4096,256]{1,0:T(8,128)(2,1)S(1)}, u32[]{:S(2)}, u32[]{:S(2)}) collective-permute-start(bf16[4096,256]{1,0:T(8,128)(2,1)S(1)} %constant_dynamic-update-slice_fusion.refs_3_.refs_4_.refs_2_.refs_5_), channel_id=1, source_target_pairs={{0,1},{1,0},{2,3},{3,2},{4,5},{5,4},{6,7},{7,6},{8,9},{9,8},{10,11... | collective-permute-start | bytes 6291464 | tf_op jit(solution)/shard_map/ppermute | solution.py:381
  16.9 17.3 %collective-permute-start = (bf16[64,4096]{1,0:T(8,128)(2,1)S(1)}, bf16[64,4096]{1,0:T(8,128)(2,1)S(1)}, u32[]{:S(2)}, u32[]{:S(2)}) collective-permute-start(bf16[64,4096]{1,0:T(8,128)(2,1)S(1)} %get-tuple-element.27), channel_id=1, source_target_pairs={{0,6},{1,3},{2,0},{3,5},{4,2},{5,7},{6,4},{7,1},{8,14},{9,11},{10,... | collective-permute-start | bytes 1572872 | tf_op jit(solution)/shard_map/ppermute | solution.py:381
  18.9 29.3 %collective-permute-start.2 = (bf16[64,4096]{1,0:T(8,128)(2,1)S(1)}, bf16[64,4096]{1,0:T(8,128)(2,1)S(1)}, u32[]{:S(2)}, u32[]{:S(2)}) collective-permute-start(bf16[64,4096]{1,0:T(8,128)(2,1)S(1)} %get-tuple-element.28), channel_id=1, source_target_pairs={{0,6},{1,3},{2,0},{3,5},{4,2},{5,7},{6,4},{7,1},{8,14},{9,11},{10,... | collective-permute-start | bytes 1572872 | tf_op jit(solution)/shard_map/ppermute | solution.py:381
  20.9 27.4 %collective-permute-start.4 = (bf16[64,4096]{1,0:T(8,128)(2,1)S(1)}, bf16[64,4096]{1,0:T(8,128)(2,1)S(1)}, u32[]{:S(2)}, u32[]{:S(2)}) collective-permute-start(bf16[64,4096]{1,0:T(8,128)(2,1)S(1)} %slice_bitcast_fusion), channel_id=1, source_target_pairs={{0,2},{1,7},{2,4},{3,1},{4,6},{5,3},{6,0},{7,5},{8,10},{9,15},{10,... | collective-permute-start | bytes 1572872 | tf_op jit(solution)/shard_map/ppermute | solution.py:381
  34.3 15.8 %collective-permute-start.1 = (bf16[64,4096]{1,0:T(8,128)(2,1)S(1)}, bf16[64,4096]{1,0:T(8,128)(2,1)S(1)}, u32[]{:S(2)}, u32[]{:S(2)}) collective-permute-start(bf16[64,4096]{1,0:T(8,128)(2,1)S(1)} %collective-permute-done.refs_1_), channel_id=1, source_target_pairs={{0,6},{1,3},{2,0},{3,5},{4,2},{5,7},{6,4},{7,1},{8,14},{9,11},{10,... | collective-permute-start | bytes 1572872 | tf_op jit(solution)/shard_map/ppermute | solution.py:381
  40.0 15.8 %collective-permute-start.6 = (bf16[5,64,256]{2,1,0:T(8,128)(2,1)S(1)}, bf16[5,64,256]{2,1,0:T(8,128)(2,1)S(1)}, u32[]{:S(2)}, u32[]{:S(2)}) collective-permute-start(bf16[5,64,256]{2,1,0:T(8,128)(2,1)S(1)} %get-tuple-element.44), channel_id=1, source_target_pairs={{0,1},{1,0},{2,3},{3,2},{4,5},{5,4},{6,7},{7,6},{8,9},{9,8},{10,11... | collective-permute-start | bytes 491528 | tf_op jit(solution)/shard_map/ppermute | solution.py:381
